TPU v7x, 128 devices: a whole 4x4x4 slice. The times are simulated.
128 devices in a mesh: sp: 32 (over z, y, core), tp: 4 (over x).
Axes of the slice: x: 4, y: 4, z: 4, core: 2. Of those that a mesh axis runs over, the one named last changes fastest.
Arguments:
- stream: bfloat16 [32768, 2048], P('sp'), may hold values from -6 to 6
- queries: bfloat16 [32768, 1024], P('sp', 'tp'), may hold values from -6 to 6
- projected_keys: bfloat16 [32768, 1024], P('sp', 'tp'), may hold values from -6 to 6
- values: bfloat16 [32768, 2048], P('sp', 'tp'), may hold values from -6 to 6
- decay_gate_logits: bfloat16 [32768, 1024], P('sp', 'tp'), may hold values from -7 to 7
- decay_gate_bias: float32 [1024], P('tp')
- extra_log_decay: float32 [32768, 8], P('sp', 'tp'), may hold values from -0.7 to 0
- document_index: int32 [32768], P('sp'), may hold values from 0 to 7, never falling along the last dimension, each value on 1 to 16384 neighbouring positions
- output_gate: bfloat16 [32768, 2048], P('sp', 'tp'), may hold values from -6 to 6
- head_norm_gain: bfloat16 [256], replicated, may hold values from 0.099609375 to 1.8984375
- output_weight: bfloat16 [2048, 2048], P('tp'), may hold values from -0.125 to 0.125
- feedforward_norm_gain: bfloat16 [2048], replicated, may hold values from 0.099609375 to 1.8984375
- gate_weight: bfloat16 [2048, 5632], P('sp', 'tp'), may hold values from -0.125 to 0.125
- up_weight: bfloat16 [2048, 5632], P('sp', 'tp'), may hold values from -0.125 to 0.125
- down_weight: bfloat16 [5632, 2048], P('tp', 'sp'), may hold values from -0.078125 to 0.078125
Outputs:
- updated: bfloat16 [32768, 2048], P(('sp', 'tp'))
All inputs are finite; a program needn't handle non-finite values.
Results may differ from a plain program's by a relative error of at most 0.015.
Values may be sent and summed in bfloat16 or wider, within the bound.
A program may use at most 128 MiB of HBM per device.

v0:
```python
import jax
import jax.numpy as jnp
from jax import lax
from jax.sharding import Mesh
from jax.sharding import PartitionSpec as P

BLOCK_LENGTH = 64
SP = ("sp_0", "sp_1", "sp_2")
SP_TP = ("sp_0", "sp_1", "sp_2", "tp")


TAU = 16.0
EPS = 1e-06


def side_by_side(arrays, axis, dim, along):
    widths = [a.shape[along] for a in arrays]
    both = jnp.concatenate(arrays, axis=along)
    result = lax.all_gather(both, axis, axis=dim, tiled=True)
    return tuple(jnp.split(result, [sum(widths[:k]) for k in range(1, len(widths))], axis=along))


def laid_out(tiles, dim):
    dims = list(tiles.shape[1:])
    dims[dim] *= tiles.shape[0]
    return jnp.moveaxis(tiles, 0, dim).reshape(dims)


def stacked_from(shard, axes, order):
    tiles = shard
    for k in order:
        tiles = lax.all_gather(tiles, axes[k])
    done = order[::-1]
    back = [done.index(k) for k in range(len(axes))]
    tiles = tiles.transpose(*back, *range(len(axes), tiles.ndim))
    return tiles.reshape(-1, *shard.shape)


def gather_axes(shard, axes, order, dim):
    return laid_out(stacked_from(shard, axes, order), dim)


def filled_with(shard, identity):
    return jax.tree.map(
        lambda part, zero: jnp.zeros_like(part) + jnp.asarray(zero, part.dtype), shard, identity
    )


def collected_together(shard, axis):
    leaves = jax.tree.leaves(shard)
    order = sorted(range(len(leaves)), key=lambda k: -leaves[k].size)
    width = (1, *leaves[order[0]].shape)[-1]
    lines = [
        jnp.pad(leaves[k].reshape(-1), (0, -leaves[k].size % width)).reshape(-1, width)
        for k in order
    ]
    both, at, found = (lax.all_gather(jnp.concatenate(lines), axis), 0, {})
    for k, line in zip(order, lines):
        slab = both[:, at : at + len(line)].reshape(len(both), -1)
        found[k] = slab[:, : leaves[k].size].reshape(-1, *leaves[k].shape)
        at += len(line)
    numbers = iter(range(len(leaves)))
    return jax.tree.map(lambda _: found[next(numbers)], shard)


def entering(shard, axes, combine, identity, reverse):
    before = start = filled_with(shard, identity)
    subtotal = shard
    for axis in reversed(axes):
        size, here = (lax.axis_size(axis), lax.axis_index(axis))
        pieces = collected_together(
            jax.tree.map(
                lambda part, kind: part.astype(kind),
                subtotal,
                (jnp.bfloat16, jnp.bfloat16, jnp.bfloat16, jnp.bfloat16),
            ),
            axis,
        )
        inside, subtotal = (start, start)
        for k in reversed(range(size)) if reverse else range(size):
            passed = k > here if reverse else k < here
            subtotal = combine(
                subtotal, jax.tree.map(lambda part, own: part[k].astype(own.dtype), pieces, shard)
            )
            inside = jax.tree.map(lambda new, old: jnp.where(passed, new, old), subtotal, inside)
        before = combine(inside, before)
    return before


def cut_along(shard, dim, size):
    before, after = (shard.shape[:dim], shard.shape[dim + 1 :])
    return jnp.moveaxis(shard.reshape(*before, size, -1, *after), dim, 0)


def sum_at_owner(shard, axis, dim):
    tiles = cut_along(shard, dim, lax.axis_size(axis))
    arrived = lax.all_to_all(tiles, axis, split_axis=0, concat_axis=0, tiled=True)
    return arrived.astype(jnp.float32).sum(axis=0)


def combine(earlier, later):
    decay_e, state_e, entry_e, exit_e = earlier
    decay_l, state_l, entry_l, exit_l = later
    joined = (exit_e == entry_l) | (exit_e < 0.0) | (entry_l < 0.0)
    passing = decay_l * joined.astype(decay_l.dtype)[..., None, None]
    merged_state = state_l + passing[..., None] * state_e
    merged_decay = decay_e * passing
    entry_doc = jnp.where(entry_e < 0.0, entry_l, entry_e)
    exit_doc = jnp.where(exit_l < 0.0, exit_e, exit_l)
    return (merged_decay, merged_state, entry_doc, exit_doc)


def neutral(head_number, key_channels, val_dim):
    return (
        jnp.ones((head_number, key_channels), jnp.float32),
        jnp.zeros((head_number, key_channels, val_dim), jnp.float32),
        jnp.full((), -1.0, jnp.float32),
        jnp.full((), -1.0, jnp.float32),
    )


def block_prefix(elements, initial, reverse_dir):

    def advance(running, element):
        return (combine(running, element), running)

    totals, before = lax.scan(advance, initial, elements, reverse=reverse_dir)
    return (before, totals)


def attention_variant(
    queries,
    projected_keys,
    values,
    decay_gate_logits,
    decay_gate_bias,
    extra_log_decay,
    document_index,
    block_length,
):
    head_number = extra_log_decay.shape[1]
    row_number = queries.shape[0]
    blocks = row_number // block_length
    key_channels = queries.shape[1] // head_number
    val_dim = values.shape[1] // head_number
    query_f = queries.astype(jnp.float32).reshape(
        blocks, block_length, head_number, key_channels
    ) * key_channels ** (-0.5)
    key_f = projected_keys.astype(jnp.float32).reshape(
        blocks, block_length, head_number, key_channels
    )
    value_b = values.reshape(blocks, block_length, head_number, val_dim)
    decay_logarithm = (
        jax.nn.log_sigmoid(decay_gate_logits.astype(jnp.float32) + decay_gate_bias) / TAU
    )
    decay_logarithm = (
        decay_logarithm.reshape(row_number, head_number, key_channels) + extra_log_decay[:, :, None]
    )
    cumulative = jnp.cumsum(
        decay_logarithm.reshape(blocks, block_length, head_number, key_channels), axis=1
    )
    document_float = document_index.astype(jnp.float32).reshape(blocks, block_length)
    middle = cumulative[:, block_length // 2 - 1 : block_length // 2]
    rising = jnp.exp(cumulative - middle)
    falling = jnp.exp(middle - cumulative)
    forward = jnp.einsum(
        "bihc,bjhc->bhij",
        (query_f * rising).astype(jnp.bfloat16),
        (key_f * falling).astype(jnp.bfloat16),
        preferred_element_type=jnp.float32,
    )
    backward = jnp.einsum(
        "bihc,bjhc->bhij",
        (query_f * falling).astype(jnp.bfloat16),
        (key_f * rising).astype(jnp.bfloat16),
        preferred_element_type=jnp.float32,
    )
    offsets = jnp.arange(block_length)
    same_doc = (document_float[:, :, None] == document_float[:, None, :])[:, None]
    below_mask = offsets[None, :] <= offsets[:, None]
    above_mask = offsets[None, :] >= offsets[:, None]
    scores = jnp.where(same_doc & below_mask, forward, 0.0) + jnp.where(
        same_doc & above_mask, backward, 0.0
    )
    within_block = jnp.einsum(
        "bhij,bjhv->bihv", scores.astype(jnp.bfloat16), value_b, preferred_element_type=jnp.float32
    )
    block_end = cumulative[:, block_length - 1]
    first_doc = document_float[:, 0]
    last_doc = document_float[:, block_length - 1]
    through = jnp.exp(block_end) * (first_doc == last_doc).astype(jnp.float32)[:, None, None]
    tail_mask = (document_float == last_doc[:, None]).astype(jnp.float32)[:, :, None, None]
    head_mask = (document_float == first_doc[:, None]).astype(jnp.float32)[:, :, None, None]
    tail_keys = (key_f * jnp.exp(block_end[:, None] - cumulative) * tail_mask).astype(jnp.bfloat16)
    head_keys = (key_f * jnp.exp(cumulative) * head_mask).astype(jnp.bfloat16)
    fwd_state = jnp.einsum(
        "bjhc,bjhv->bhcv", tail_keys, value_b, preferred_element_type=jnp.float32
    )
    bwd_state = jnp.einsum(
        "bjhc,bjhv->bhcv", head_keys, value_b, preferred_element_type=jnp.float32
    )
    forward_elements = (through, fwd_state, first_doc, last_doc)
    backward_elements = (through, bwd_state, last_doc, first_doc)
    forward_query = query_f * jnp.exp(cumulative)
    backward_query = query_f * jnp.exp(block_end[:, None] - cumulative)
    return (
        within_block,
        forward_elements,
        backward_elements,
        forward_query,
        backward_query,
        document_float,
    )


def carried(inflow, factor, document_float):
    hit_mask = (document_float == inflow[3][:, None]).astype(jnp.float32)[:, :, None, None]
    return jnp.einsum("bihc,bhcv->bihv", factor, inflow[1]) * hit_mask


def head_mix(
    within_block,
    fwd_in,
    bwd_in,
    forward_query,
    backward_query,
    document_float,
    output_gate,
    head_norm_gain,
    head_number,
):
    total_out = (
        within_block
        + carried(fwd_in, forward_query, document_float)
        + carried(bwd_in, backward_query, document_float)
    )
    row_number = output_gate.shape[0]
    total_out = total_out.reshape(row_number, head_number, -1)
    scaled = total_out * lax.rsqrt(jnp.mean(total_out * total_out, axis=-1, keepdims=True) + EPS)
    scaled = scaled * head_norm_gain.astype(jnp.float32)
    return (scaled.reshape(row_number, -1) * jax.nn.silu(output_gate.astype(jnp.float32))).astype(
        jnp.bfloat16
    )


def row_norm(rows_f, gain):
    factor = lax.rsqrt(jnp.mean(rows_f * rows_f, axis=-1, keepdims=True) + EPS)
    return (rows_f * factor * gain.astype(jnp.float32)).astype(jnp.bfloat16)


def per_device(
    stream,
    queries,
    projected_keys,
    values,
    decay_gate_logits,
    decay_gate_bias,
    extra_log_decay,
    document_index,
    output_gate,
    head_norm_gain,
    output_weight,
    feedforward_norm_gain,
    gate_weight,
    up_weight,
    down_weight,
):
    whole_gate, whole_up = side_by_side((gate_weight, up_weight), SP, 0, 1)
    whole_down = gather_axes(down_weight, (("sp_0", "sp_1"), "sp_2"), (0, 1), 1)
    head_number = extra_log_decay.shape[1]
    key_channels = queries.shape[1] // head_number
    val_dim = values.shape[1] // head_number
    (
        within_block,
        forward_elements,
        backward_elements,
        forward_query,
        backward_query,
        document_float,
    ) = attention_variant(
        queries,
        projected_keys,
        values,
        decay_gate_logits,
        decay_gate_bias,
        extra_log_decay,
        document_index,
        BLOCK_LENGTH,
    )
    initial = neutral(head_number, key_channels, val_dim)
    fwd_before, fwd_totals = block_prefix(forward_elements, initial, False)
    bwd_before, bwd_totals = block_prefix(backward_elements, initial, True)
    fwd_carry = entering(
        (fwd_totals[0], fwd_totals[1], fwd_totals[2], fwd_totals[3]),
        SP,
        combine,
        (initial[0], initial[1], initial[2], initial[3]),
        False,
    )
    bwd_carry = entering(
        (bwd_totals[0], bwd_totals[1], bwd_totals[2], bwd_totals[3]),
        SP,
        combine,
        (initial[0], initial[1], initial[2], initial[3]),
        True,
    )
    head_mixed = head_mix(
        within_block,
        combine(fwd_carry, fwd_before),
        combine(bwd_carry, bwd_before),
        forward_query,
        backward_query,
        document_float,
        output_gate,
        head_norm_gain,
        head_number,
    )
    tp_rows = stream.shape[0] // lax.axis_size("tp")
    tp_start = lax.axis_index("tp") * tp_rows
    attended = lax.psum(
        jnp.dot(head_mixed, output_weight, preferred_element_type=jnp.float32).astype(jnp.bfloat16),
        "tp",
    ).astype(jnp.float32)
    resid_all = stream.astype(jnp.float32) + attended
    normed = row_norm(resid_all, feedforward_norm_gain)
    resid_own = lax.dynamic_slice_in_dim(resid_all, tp_start, tp_rows, 0)
    gate_act = jnp.dot(normed, whole_gate, preferred_element_type=jnp.float32)
    up_act = jnp.dot(normed, whole_up, preferred_element_type=jnp.float32)
    hidden = (jax.nn.silu(gate_act) * up_act).astype(jnp.bfloat16)
    partial_value = jnp.dot(hidden, whole_down, preferred_element_type=jnp.float32)
    mlp_out = sum_at_owner(partial_value.astype(jnp.bfloat16), "tp", 0)
    return (resid_own + mlp_out).astype(jnp.bfloat16)


def solution(mesh):
    torus = Mesh(mesh.devices.reshape(4, 4, 2, mesh.shape["tp"]), ("sp_0", "sp_1", "sp_2", "tp"))
    placed = (
        P(SP, None),
        P(SP, "tp"),
        P(SP, "tp"),
        P(SP, "tp"),
        P(SP, "tp"),
        P("tp"),
        P(SP, "tp"),
        P(SP),
        P(SP, "tp"),
        P(),
        P("tp", None),
        P(),
        P(SP, "tp"),
        P(SP, "tp"),
        P("tp", SP),
    )
    return jax.shard_map(
        per_device, mesh=torus, in_specs=placed, out_specs=P(SP_TP, None), check_vma=False
    )
```

profile of v0, /device:TPU:6, one launch (start us, length us, event | category | flops | bytes accessed | tf_op | source)
XLA Modules:
  0.0 613.6 jit_solution(16095509793635452447)
XLA Ops:
  10.3 2.2 reshape.1402
  12.4 2.1 convert_multiply_fusion.1
  14.5 2.7 mul.1173
  18.8 2.7 fusion.34
  21.5 2.8 reshape.1399
  26.0 4.5 multiply_convert_fusion.7
  30.6 2.7 fusion.41
  33.3 2.5 broadcast.749.clone
  35.8 102.6 %while.55 = (s32[]{:T(128)}, f32[2,128]{1,0:T(2,128)S(1)}, f32[2,128,256]{2,1,0:T(8,128)S(1)}, f32[]{:T(128)}, f32[]{:T(128)}, /*index=5*/f32[16,2,128]{2,1,0:T(...) while((s32[]{:T(128)}, f32[2,128]{1,0:T(2,128)S(1)}, ...), condition=%wide.region_4.5_spmd.clone, body=%wide.region_3.4_spmd.clone.sunk | while | flops 263182 | bytes 1318244 | solution.py:127
  138.5 2.0 all-gather.11
  148.4 13.3 %all-gather.12 = bf16[4,259,256]{2,1,0:T(8,128)(2,1)S(1)} all-gather(bf16[1,259,256]{2,1,0:T(8,128)(2,1)S(1)} %maximum_bitcast_fusion.4), channel_id=6, replica_groups=mesh['sp_0'=4,'sp_1'=4,'sp_2'=2,'tp'=4] {'sp_1'}, dimensions={0}, use_global_device_ids=true | all-gather | bytes 663040 | tf_op jit(solution)/shard_map/all_gather | solution.py:57
  161.7 4.0 fusion.43
  165.7 2.6 broadcast.749.clone.1
  168.3 106.0 %while.54 = (s32[]{:T(128)}, f32[2,128]{1,0:T(2,128)S(1)}, f32[2,128,256]{2,1,0:T(8,128)S(1)}, f32[]{:T(128)}, f32[]{:T(128)}, /*index=5*/f32[16,2,128]{2,1,0:T(...) while((s32[]{:T(128)}, f32[2,128]{1,0:T(2,128)S(1)}, ...), condition=%wide.region_2.3_spmd.clone, body=%wide.region_1.2_spmd.clone.sunk | while | flops 263181 | bytes 1318224 | solution.py:127
  274.4 2.0 all-gather.8
  284.3 13.1 %all-gather.9 = bf16[4,259,256]{2,1,0:T(8,128)(2,1)S(1)} all-gather(bf16[1,259,256]{2,1,0:T(8,128)(2,1)S(1)} %maximum_bitcast_fusion.1), channel_id=3, replica_groups=mesh['sp_0'=4,'sp_1'=4,'sp_2'=2,'tp'=4] {'sp_1'}, dimensions={0}, use_global_device_ids=true | all-gather | bytes 663040 | tf_op jit(solution)/shard_map/all_gather | solution.py:57
  311.6 14.1 %all-gather.13 = bf16[4,259,256]{2,1,0:T(8,128)(2,1)S(1)} all-gather(bf16[1,259,256]{2,1,0:T(8,128)(2,1)S(1)} %maximum_bitcast_fusion.5), channel_id=7, replica_groups=mesh['sp_0'=4,'sp_1'=4,'sp_2'=2,'tp'=4] {'sp_0'}, dimensions={0}, use_global_device_ids=true | all-gather | bytes 663040 | tf_op jit(solution)/shard_map/all_gather | solution.py:57
  351.0 13.5 %all-gather.10 = bf16[4,259,256]{2,1,0:T(8,128)(2,1)S(1)} all-gather(bf16[1,259,256]{2,1,0:T(8,128)(2,1)S(1)} %maximum_bitcast_fusion.2), channel_id=4, replica_groups=mesh['sp_0'=4,'sp_1'=4,'sp_2'=2,'tp'=4] {'sp_0'}, dimensions={0}, use_global_device_ids=true | all-gather | bytes 663040 | tf_op jit(solution)/shard_map/all_gather | solution.py:57
  386.2 2.0 fusion.11
  388.8 2.0 fusion.14
  390.8 5.3 multiply_reduce_fusion.1
  399.8 4.7 convolution_convert_fusion
  404.6 3.8 copy.222
  409.5 86.9 %all-reduce.14.cloned.1.call-done = bf16[1024,2048]{1,0:T(8,128)(2,1)} async-done(((bf16[1024,2048]{1,0:T(8,128)(2,1)}), bf16[1024,2048]{1,0:T(8,128)(2,1)}) %all-reduce.14.cloned.1.call-update) | async-done | bytes 4194320 | tf_op jit(solution)/shard_map/psum | solution.py:320
  496.4 8.0 %convert_add_fusion = (f32[1024,2048]{1,0:T(8,128)}, f32[1024]{0:T(1024)S(1)}) fusion(bf16[1024,2048]{1,0:T(8,128)(2,1)} %all-reduce.14.cloned.1.call-done, bf16[1024,2048]{1,0:T(8,128)(2,1)} %param.19), kind=kLoop, calls=%fused_computation.15 | loop fusion | flops 10484736 | bytes 16781312 | tf_op jit(solution)/shard_map/add | solution.py:324
  504.4 7.1 %copy.202 = bf16[16,2,1408,64]{2,3,1,0:T(8,128)(2,1)} copy(bf16[16,2,1408,64]{2,0,1,3:T(8,128)(2,1)} %bitcast.375) | data formatting | bytes 11534336 | tf_op jit(solution)/shard_map/transpose | solution.py:35
  511.5 12.7 %fusion.4 = f32[1024,1408]{1,0:T(8,128)} fusion(bf16[2048,2816]{1,0:T(8,128)(2,1)} %all-gather.18.cloned.1.call-done, f32[2048]{0:T(1024)S(1)} %convert_element_type.1376, f32[1024]{0:T(1024)S(1)} %add_rsqrt_fusion, bf16[1024,2048]{1,0:T(8,128)(2,1)} %all-reduce.14.cloned.1.call-done, bf16[1024,2048]{1,0:T(8,128)(2,1)} %param.19), kind=kOutput, calls=%fused_computation.18 | convolution fusion | flops 5918162944 | bytes 19935232 | tf_op jit(solution)/shard_map/dot_general | solution.py:327
  524.1 22.0 %fusion.17 = bf16[1024,2048]{1,0:T(8,128)(2,1)} fusion(bf16[1408,2048]{0,1:T(8,128)(2,1)} %bitcast.376, f32[1024,1408]{1,0:T(8,128)} %fusion.4, bf16[2048,2816]{1,0:T(8,128)(2,1)} %all-gather.18.cloned.1.call-done, f32[2048]{0:T(1024)S(1)} %convert_element_type.1376, f32[1024]{0:T(1024)S(1)} %add_rsqrt_fusion, ...), kind=kOutput, calls=%fused_computation.28 | convolution fusion | flops 11834490880 | bytes 29896704 | tf_op jit(solution)/shard_map/dot_general | solution.py:330
  546.1 7.2 %all-to-all-start = ((bf16[4,256,2048]{2,1,0:T(8,128)(2,1)}), bf16[4,256,2048]{2,1,0:T(8,128)(2,1)}, u32[]{:S(2)}, u32[]{:S(2)}) async-start(bf16[4,256,2048]{2,1,0:T(8,128)(2,1)} %bitcast.377), calls=%async_computation | async-start | bytes 8388608 | tf_op jit(solution)/shard_map/all_to_all | solution.py:97
  553.4 46.9 %all-to-all-done = bf16[4,256,2048]{2,1,0:T(8,128)(2,1)} async-done(((bf16[4,256,2048]{2,1,0:T(8,128)(2,1)}), bf16[4,256,2048]{2,1,0:T(8,128)(2,1)}, u32[]{:S(2)}, u32[]{:S(2)}) %all-to-all-start) | async-done | bytes 4194336 | tf_op jit(solution)/shard_map/all_to_all | solution.py:97
  600.3 3.4 convert_reduce_fusion
  603.6 2.9 add_convert_fusion
  (458 shorter events, 137.1 us)
Async XLA Ops:
  7.4 392.4 %copy-start = (bf16[512,2048]{1,0:T(8,128)(2,1)S(1)}, bf16[512,2048]{1,0:T(8,128)(2,1)}, u32[]{:S(2)}) copy-start(bf16[512,2048]{1,0:T(8,128)(2,1)} %param.29) | copy-start | bytes 6291460
  7.4 9.9 %copy-start.17 = (bf16[1024,256]{1,0:T(8,128)(2,1)S(1)}, bf16[1024,256]{1,0:T(8,128)(2,1)}, u32[]{:S(2)}) copy-start(bf16[1024,256]{1,0:T(8,128)(2,1)} %param.21) | copy-start | bytes 1572868
  7.4 11.4 %copy-start.21 = (f32[256]{0:T(256)S(1)}, f32[256]{0:T(256)}, u32[]{:S(2)}) copy-start(f32[256]{0:T(256)} %param.24) | copy-start | bytes 3076
  7.4 397.2 %all-gather.20.cloned.1.call-start = ((), (), s32[]{:S(2)}) async-start(), calls=%async_computation.3 | async-start | bytes 3063808 | tf_op jit(solution)/shard_map/all_gather | solution.py:32
  8.1 488.3 %all-reduce.14.cloned.1.call-start = ((), (), s32[]{:S(2)}) async-start(), calls=%async_computation.1 | async-start | bytes 8388608 | tf_op jit(solution)/shard_map/psum | solution.py:320
  24.3 6.3 %copy-start.4 = (bf16[16,64,2,256]{3,2,1,0:T(2,128)(2,1)S(1)}, bf16[16,64,2,256]{3,2,1,0:T(2,128)(2,1)}, u32[]{:S(2)}) copy-start(bf16[16,64,2,256]{3,2,1,0:T(2,128)(2,1)} %reshape.1402) | copy-start | bytes 3145732
  25.9 7.4 %copy-start.6 = (f32[16,64,2,128]{3,0,1,2:T(8,128)}, f32[16,64,2,128]{3,0,1,2:T(8,128)S(1)}, u32[]{:S(2)}) copy-start(f32[16,64,2,128]{3,0,1,2:T(8,128)S(1)} %fusion.37) | copy-start | bytes 3145732
  138.4 2.2 copy-start.24
  140.5 7.8 %copy-start.10 = (bf16[2,259,256]{2,1,0:T(8,128)(2,1)}, bf16[2,259,256]{2,1,0:T(8,128)(2,1)S(1)}, u32[]{:S(2)}) copy-start(bf16[2,259,256]{2,1,0:T(8,128)(2,1)S(1)} %all-gather.11) | copy-start | bytes 795652
  168.2 129.2 %copy-start.23 = (bf16[256]{0:T(256)(128)(2,1)S(1)}, bf16[256]{0:T(256)(128)(2,1)}, u32[]{:S(2)}) copy-start(bf16[256]{0:T(256)(128)(2,1)} %param.28) | copy-start | bytes 1540
  274.3 9.9 %copy-start.26 = (f32[16]{0:T(128)}, f32[16]{0:T(128)S(1)}, u32[]{:S(2)}) copy-start(f32[16]{0:T(128)S(1)} %get-tuple-element.348) | copy-start | bytes 196
  274.3 62.3 %copy-start.25 = (f32[16]{0:T(128)S(1)}, f32[16]{0:T(128)}, u32[]{:S(2)}) copy-start(f32[16]{0:T(128)} %copy-done.24) | copy-start | bytes 196
  276.4 7.8 %copy-start.11 = (bf16[2,259,256]{2,1,0:T(8,128)(2,1)}, bf16[2,259,256]{2,1,0:T(8,128)(2,1)S(1)}, u32[]{:S(2)}) copy-start(bf16[2,259,256]{2,1,0:T(8,128)(2,1)S(1)} %all-gather.8) | copy-start | bytes 795652
  284.2 91.1 %copy-start.27 = (f32[16]{0:T(128)S(1)}, f32[16]{0:T(128)}, u32[]{:S(2)}) copy-start(f32[16]{0:T(128)} %copy-done.26) | copy-start | bytes 196
  325.7 0.8 copy-start.12
  375.3 7.2 %copy-start.14 = (bf16[16,64,2,128]{3,0,1,2:T(8,128)(2,1)S(1)}, bf16[16,64,2,128]{3,0,1,2:T(8,128)(2,1)}, u32[]{:S(2)}) copy-start(bf16[16,64,2,128]{3,0,1,2:T(8,128)(2,1)} %get-tuple-element.700) | copy-start | bytes 1572868
  375.4 7.2 %copy-start.15 = (bf16[16,64,2,128]{3,0,1,2:T(8,128)(2,1)S(1)}, bf16[16,64,2,128]{3,0,1,2:T(8,128)(2,1)}, u32[]{:S(2)}) copy-start(bf16[16,64,2,128]{3,0,1,2:T(8,128)(2,1)} %get-tuple-element.709) | copy-start | bytes 1572868
  382.5 2.5 copy-start.7
  382.5 2.5 copy-start.8
  384.0 2.2 copy-start.2
  385.8 3.0 copy-start.3
  388.2 2.6 copy-start.5
  388.2 2.6 copy-start.16
  396.3 1.6 copy-start.9
  397.9 1.8 copy-start.22
  404.5 99.9 %all-gather.22.cloned.1.call-start = ((), (), s32[]{:S(2)}) async-start(), calls=%async_computation.4 | async-start | bytes 8650752 | tf_op jit(solution)/shard_map/all_gather | solution.py:32
  404.5 4.1 copy-start.18
  404.6 4.1 copy-start.19
  404.6 4.9 copy-start.20
  408.4 103.1 %all-gather.18.cloned.1.call-start = ((), (), s32[]{:S(2)}) async-start(), calls=%async_computation.2 | async-start | bytes 11894784 | tf_op jit(solution)/shard_map/all_gather | solution.py:19
  546.1 54.1 %all-to-all-start = ((bf16[4,256,2048]{2,1,0:T(8,128)(2,1)}), bf16[4,256,2048]{2,1,0:T(8,128)(2,1)}, u32[]{:S(2)}, u32[]{:S(2)}) async-start(bf16[4,256,2048]{2,1,0:T(8,128)(2,1)} %bitcast.377), calls=%async_computation | async-start | bytes 8388608 | tf_op jit(solution)/shard_map/all_to_all | solution.py:97
  600.3 6.2 %copy-start.1 = (bf16[512,2048]{1,0:T(8,128)(2,1)S(1)}, bf16[512,2048]{1,0:T(8,128)(2,1)}, u32[]{:S(2)}) copy-start(bf16[512,2048]{1,0:T(8,128)(2,1)} %param.29) | copy-start | bytes 6291460
  (1 other events, 0.8 us)
Sparse Core Ops, SparseCore 0:
  10.4 49.2 all-gather.19
  408.5 19.8 all-gather.21
  430.7 61.5 all-gather.17
Sparse Core Ops, SparseCore 1:
  404.5 91.8 all-reduce.13
where the time goes:
time: 619 us; the launch traced here: 614 us
  waiting for transfers between devices  135 us (22%)
  loops' own time  103 us (17%)
  other arithmetic  92.3 us (15%)
  local copies, waits for them, and re-layouts  89.4 us (14%)
  between operations  71.5 us (12%)
  blocking collectives  58.1 us (9%)
  matrix products  56.7 us (9%)
  starting transfers between devices  7.58 us (1%)
    another operation x2, loops' own time, block_prefix(): totals, before = lax.scan(advance, initial, elements, reverse=reverse_dir)  103 us
    psum x1, waiting for transfers between devices, per_device(): lax.psum(jnp.dot(head_mixed, output_weight, preferred_element_type=jnp.fl...  86.9 us
    all_gather x6, blocking collectives, collected_together(): both, at, found = (lax.all_gather(jnp.concatenate(lines), axis), 0, {})  58.1 us
    all_to_all x1, waiting for transfers between devices, sum_at_owner(): lax.all_to_all(tiles, axis, split_axis=0, concat_axis=0, tiled=True)  46.9 us
    dynamic_slice x64, local copies, waits for them, and re-layouts, block_prefix(): totals, before = lax.scan(advance, initial, elements, reverse=reverse_dir)  40.2 us
    add x34, other arithmetic, combine(): merged_state = state_l + passing[..., None] * state_e  35 us
    dynamic_update_slice x64, other arithmetic, block_prefix(): totals, before = lax.scan(advance, initial, elements, reverse=reverse_dir)  23.5 us
    dot_general x1, matrix products, per_device(): jnp.dot(hidden, whole_down, preferred_element_type=jnp.float32)  22 us
  transfers between devices with their start and end apart: 5, of which 2 were waited for; matrix products, arithmetic and copies ran while one was open for 32% of the time, Pallas kernels for 0%

commit v1 on v0

v1 whole, which is shorter than its diff:
```python
import functools
import jax
import jax.numpy as jnp
from jax import lax
from jax.experimental import pallas as pl
from jax.experimental.pallas import tpu as pltpu
from jax.sharding import Mesh
from jax.sharding import PartitionSpec as P

SP = ("sp_0", "sp_1", "sp_2")
SP_TP = ("sp_0", "sp_1", "sp_2", "tp")
MESH = pl.DeviceIdType.MESH
F32 = jnp.float32
BF16 = jnp.bfloat16
TAU = 16.0
EPS = 1e-06
BL = 64
GR = 256
DK = 128
DV = 256
NZ, NY = 4, 4
NCHIP = NZ * NY


def nt_dot(a, b):
    return lax.dot_general(a, b, (((1,), (1,)), ((), ())), preferred_element_type=F32)


def tn_dot(a, b):
    return lax.dot_general(a, b, (((0,), (0,)), ((), ())), preferred_element_type=F32)


def nn_dot(a, b):
    return lax.dot_general(a, b, (((1,), (0,)), ((), ())), preferred_element_type=F32)


def attention_kernel(
    q_ref, k_ref, v_ref, lg_ref, bias_ref, aux_ref, docrow_ref, gate_ref, gain_ref,
    mixed_ref,
    cum_ref, glob_ref, blk_ref, states_ref, before_ref, run_ref, local_ref,
    own_t, own_e, part_t, part_e, chip_t, chip_e, recv_t, recv_e, mine_c, send_c, part_c, sum_ref,
    core_send, core_recv, t_send, t_recv, e_send, e_recv,
):
    rows = q_ref.shape[0]
    blocks = rows // BL
    groups = rows // GR
    per = GR // BL
    z, y = lax.axis_index("sp_0"), lax.axis_index("sp_1")
    core, x = lax.axis_index("sp_2"), lax.axis_index("tp")
    chip = z * NY + y
    scale = DK ** (-0.5)

    def chip_peer(k):
        other = lax.rem(chip + k, NCHIP)
        return other, (other // NY, lax.rem(other, NY), core, x)

    partner = (z, y, 1 - core, x)

    recv_t[pl.ds(chip, 1)] = jnp.zeros((1, DV, DK), BF16)

    barrier = pltpu.get_barrier_semaphore()
    pl.semaphore_signal(barrier, inc=1, device_id=partner, device_id_type=MESH)
    for k in range(1, NCHIP):
        pl.semaphore_signal(barrier, inc=1, device_id=chip_peer(k)[1], device_id_type=MESH)

    ri = lax.broadcasted_iota(jnp.int32, (GR, GR), 0)
    ci = lax.broadcasted_iota(jnp.int32, (GR, GR), 1)

    def first(g, base):
        at = pl.multiple_of(g * GR, GR)
        same_block = (ri & (GR - BL)) == (ci & (GR - BL))
        tri = jnp.where(same_block & (ci <= ri), 1.0, 0.0).astype(BF16)
        logits = lg_ref[pl.ds(at, GR), :].astype(F32) + bias_ref[...]
        ld = (jnp.minimum(logits, 0.0) - jnp.log1p(jnp.exp(-jnp.abs(logits)))) / TAU
        extra0 = jnp.broadcast_to(aux_ref[pl.ds(at, GR), 0:1], (GR, DK))
        extra1 = jnp.broadcast_to(aux_ref[pl.ds(at, GR), 1:2], (GR, DK))
        ld = ld + jnp.concatenate([extra0, extra1], axis=1)
        hi = ld.astype(BF16)
        rest = ld - hi.astype(F32)
        mid = rest.astype(BF16)
        low = (rest - mid.astype(F32)).astype(BF16)
        cum = nn_dot(tri, hi) + nn_dot(tri, mid) + nn_dot(tri, low)
        cum_ref[pl.ds(at, GR), :] = cum
        cum3 = cum.reshape(per, BL, 2 * DK)
        ends = cum3[:, BL - 1 : BL, :]
        off, offs = base, []
        for b in range(per):
            offs.append(off)
            blk_ref[pl.ds(g * per + b, 1)] = ends[b : b + 1]
            off = off + ends[b]
        for b in range(per):
            glob_ref[pl.ds(pl.multiple_of(at + b * BL, BL), BL), :] = cum3[b] + offs[b]
        doc = aux_ref[pl.ds(at, GR), 2:3].reshape(per, BL, 1)
        tail_mask = jnp.where(doc == doc[:, BL - 1 : BL], 1.0, 0.0)
        head_mask = jnp.where(doc == doc[:, 0:1], 1.0, 0.0)
        kf = k_ref[pl.ds(at, GR), :].astype(F32).reshape(per, BL, 2 * DK)
        tail = (kf * jnp.exp(ends - cum3) * tail_mask).astype(BF16)
        head = (kf * jnp.exp(cum3) * head_mask).astype(BF16)
        for b in range(per):
            for h in range(2):
                keys = jnp.concatenate(
                    [tail[b][:, h * DK : (h + 1) * DK], head[b][:, h * DK : (h + 1) * DK]], axis=1
                )
                vals = v_ref[pl.ds(pl.multiple_of(at + b * BL, BL), BL), h * DV : (h + 1) * DV]
                states_ref[pl.ds((g * per + b) * 2 + h, 1)] = tn_dot(vals, keys)[None]
        return off

    total = lax.fori_loop(0, groups, first, jnp.zeros((1, 2 * DK), F32))
    sum_ref[...] = total

    run_ref[...] = jnp.zeros_like(run_ref)

    def doc_at(r):
        return aux_ref[pl.ds(r, 1), 2:3]

    def step(b, _):
        lo = jnp.maximum(b * BL - 1, 0)
        keep = jnp.where(doc_at(lo) == doc_at(b * BL + BL - 1), 1.0, 0.0)
        decay = jnp.exp(blk_ref[pl.ds(b, 1)][0]) * keep
        r = blocks - 1 - b
        hi = jnp.minimum(r * BL + BL, rows - 1)
        keep_b = jnp.where(doc_at(hi) == doc_at(r * BL), 1.0, 0.0)
        decay_b = jnp.exp(blk_ref[pl.ds(r, 1)][0]) * keep_b
        for h in range(2):
            fw = run_ref[h, :, :DK]
            before_ref[pl.ds(b * 2 + h, 1), :, :DK] = fw.astype(BF16)[None]
            run_ref[h, :, :DK] = fw * decay[:, h * DK : (h + 1) * DK] + states_ref[b * 2 + h, :, :DK]
            bw = run_ref[h, :, DK:]
            before_ref[pl.ds(r * 2 + h, 1), :, DK:] = bw.astype(BF16)[None]
            run_ref[h, :, DK:] = bw * decay_b[:, h * DK : (h + 1) * DK] + states_ref[r * 2 + h, :, DK:]
        return 0

    lax.fori_loop(0, blocks, step, 0)
    first_doc = jnp.broadcast_to(doc_at(0), (1, DK))
    last_doc = jnp.broadcast_to(doc_at(rows - 1), (1, DK))
    for h in range(2):
        own_t[h, :DV] = run_ref[h, :, :DK].astype(BF16)
        own_t[h, DV:] = run_ref[h, :, DK:].astype(BF16)
        own_e[h, 0:1] = total[:, h * DK : (h + 1) * DK]
        own_e[h, 1:2] = first_doc
        own_e[h, 2:3] = last_doc
        own_e[h, 3:8] = jnp.zeros((5, DK), F32)

    pl.semaphore_wait(barrier, NCHIP)
    swap_t = pltpu.make_async_remote_copy(
        own_t.at[1 - core], part_t, core_send.at[0], core_recv.at[0],
        device_id=partner, device_id_type=MESH)
    swap_e = pltpu.make_async_remote_copy(
        own_e.at[1 - core], part_e, core_send.at[1], core_recv.at[1],
        device_id=partner, device_id_type=MESH)
    swap_t.start()
    swap_e.start()
    swap_t.wait()
    swap_e.wait()
    is0 = core == 0
    mine_e = own_e[pl.ds(core, 1)][0]
    other_e = part_e[...]
    e0 = jnp.where(is0, mine_e, other_e)
    e1 = jnp.where(is0, other_e, mine_e)
    mine_t = own_t[pl.ds(core, 1)][0].astype(F32)
    other_t = part_t[...].astype(F32)
    t0 = jnp.where(is0, mine_t, other_t)
    t1 = jnp.where(is0, other_t, mine_t)
    through1 = jnp.exp(e1[0:1]) * jnp.where(e0[2:3] == e1[2:3], 1.0, 0.0)
    through0 = jnp.exp(e0[0:1]) * jnp.where(e1[1:2] == e0[1:2], 1.0, 0.0)
    chip_t[0] = (t1[:DV] + through1 * t0[:DV]).astype(BF16)
    chip_t[1] = (t0[DV:] + through0 * t1[DV:]).astype(BF16)
    chip_row = jnp.concatenate(
        [e0[0:1] + e1[0:1], e0[1:2], e1[2:3], jnp.zeros((5, DK), F32)], axis=0)
    chip_e[...] = chip_row
    recv_e[pl.ds(chip, 1)] = chip_row[None]

    sends = []
    for k in range(1, NCHIP):
        other, target = chip_peer(k)
        back = jnp.where(other > chip, 0, 1)
        sends.append(pltpu.make_async_remote_copy(
            chip_e, recv_e.at[chip], e_send.at[k], e_recv.at[k],
            device_id=target, device_id_type=MESH))
        sends.append(pltpu.make_async_remote_copy(
            chip_t.at[back], recv_t.at[chip], t_send.at[k], t_recv.at[k],
            device_id=target, device_id_type=MESH))
    for s in sends:
        s.start()

    def inside(g, _):
        at = pl.multiple_of(g * GR, GR)
        same_block = (ri & (GR - BL)) == (ci & (GR - BL))
        doc = aux_ref[pl.ds(at, GR), 2:3]
        same = same_block & (doc == docrow_ref[pl.ds(g, 1), :])
        below = same & (ci <= ri)
        above = same & (ci >= ri)
        cum3 = cum_ref[pl.ds(at, GR), :].reshape(per, BL, 2 * DK)
        middle = cum3[:, BL // 2 - 1 : BL // 2]
        ends = cum3[:, BL - 1 : BL]
        rising = jnp.exp(cum3 - middle)
        falling = jnp.exp(middle - cum3)
        qf = q_ref[pl.ds(at, GR), :].astype(F32).reshape(per, BL, 2 * DK) * scale
        kf = k_ref[pl.ds(at, GR), :].astype(F32).reshape(per, BL, 2 * DK)
        q_rise = (qf * rising).astype(BF16).reshape(GR, 2 * DK)
        q_fall = (qf * falling).astype(BF16).reshape(GR, 2 * DK)
        k_rise = (kf * rising).astype(BF16).reshape(GR, 2 * DK)
        k_fall = (kf * falling).astype(BF16).reshape(GR, 2 * DK)
        q_fwd = qf * jnp.exp(cum3)
        q_bwd = qf * jnp.exp(ends - cum3)
        for h in range(2):
            c = slice(h * DK, (h + 1) * DK)
            fw = nt_dot(q_rise[:, c], k_fall[:, c])
            bw = nt_dot(q_fall[:, c], k_rise[:, c])
            scores = jnp.where(below, fw, 0.0) + jnp.where(above, bw, 0.0)
            vals = v_ref[pl.ds(at, GR), h * DV : (h + 1) * DV]
            local_ref[pl.ds(at, GR), h * DV : (h + 1) * DV] = nn_dot(scores.astype(BF16), vals)
        for b in range(per):
            start = at + b * BL
            prev = doc_at(jnp.maximum(start - 1, 0))
            following = doc_at(jnp.minimum(start + BL, rows - 1))
            rows_doc = doc[b * BL : (b + 1) * BL]
            hit_f = jnp.where(rows_doc == prev, 1.0, 0.0)
            hit_b = jnp.where(rows_doc == following, 1.0, 0.0)
            for h in range(2):
                c = slice(h * DK, (h + 1) * DK)
                both = jnp.concatenate([q_fwd[b][:, c] * hit_f, q_bwd[b][:, c] * hit_b], axis=1)
                here = pl.ds(pl.multiple_of(start, BL), BL)
                local_ref[here, h * DV : (h + 1) * DV] += nt_dot(
                    both.astype(BF16), before_ref[(g * per + b) * 2 + h])
        return 0

    lax.fori_loop(0, groups, inside, 0)

    for s in sends:
        s.wait()
    run_ref[0] = jnp.zeros_like(run_ref[0])

    def earlier(j, _):
        e = recv_e[j]
        p = recv_e[jnp.maximum(j - 1, 0)]
        keep = jnp.exp(e[0:1]) * jnp.where(e[2:3] == p[2:3], 1.0, 0.0)
        run_ref[0, :, :DK] = recv_t[j].astype(F32) + run_ref[0, :, :DK] * keep
        return 0

    def later(i, _):
        j = NCHIP - 1 - i
        e = recv_e[j]
        p = recv_e[jnp.minimum(j + 1, NCHIP - 1)]
        keep = jnp.exp(e[0:1]) * jnp.where(e[1:2] == p[1:2], 1.0, 0.0)
        run_ref[0, :, DK:] = recv_t[j].astype(F32) + run_ref[0, :, DK:] * keep
        return 0

    lax.fori_loop(0, chip, earlier, 0)
    lax.fori_loop(0, NCHIP - 1 - chip, later, 0)
    cf, cb = run_ref[0, :, :DK], run_ref[0, :, DK:]
    before_doc = jnp.where(chip > 0, recv_e[jnp.maximum(chip - 1, 0)][2:3], -1.0)
    after_doc = jnp.where(
        chip < NCHIP - 1, recv_e[jnp.minimum(chip + 1, NCHIP - 1)][1:2], -1.0)
    pass0 = jnp.exp(e0[0:1]) * jnp.where(before_doc == e0[2:3], 1.0, 0.0)
    pass1 = jnp.exp(e1[0:1]) * jnp.where(after_doc == e1[1:2], 1.0, 0.0)
    mine_t = own_t[pl.ds(core, 1)][0].astype(F32)
    other_t = part_t[...].astype(F32)
    t0f = jnp.where(is0, mine_t[:DV], other_t[:DV])
    t1b = jnp.where(is0, other_t[DV:], mine_t[DV:])
    c0 = jnp.concatenate([cf, t1b + pass1 * cb], axis=1)
    c1 = jnp.concatenate([t0f + pass0 * cf, cb], axis=1)
    mine_c[...] = jnp.where(is0, c0, c1).astype(BF16)
    send_c[...] = jnp.where(is0, c1, c0).astype(BF16)
    swap_c = pltpu.make_async_remote_copy(
        send_c, part_c, core_send.at[2], core_recv.at[2],
        device_id=partner, device_id_type=MESH)
    swap_c.start()
    enter_f = jnp.where(is0, before_doc, e0[2:3])[:, 0:1]
    enter_b = jnp.where(is0, e1[1:2], after_doc)[:, 0:1]
    swap_c.wait()

    def last(g, _):
        at = pl.multiple_of(g * GR, GR)
        doc = aux_ref[pl.ds(at, GR), 2:3]
        hit_f = jnp.where(doc == enter_f, 1.0, 0.0)
        hit_b = jnp.where(doc == enter_b, 1.0, 0.0)
        glob = glob_ref[pl.ds(at, GR), :]
        qf = q_ref[pl.ds(at, GR), :].astype(F32) * scale
        q_fwd = (qf * jnp.exp(glob) * hit_f).astype(BF16)
        q_bwd = (qf * jnp.exp(sum_ref[...] - glob) * hit_b).astype(BF16)
        gain = gain_ref[...].astype(F32)
        for h in range(2):
            c = slice(h * DK, (h + 1) * DK)
            both = jnp.concatenate([q_fwd[:, c], q_bwd[:, c]], axis=1)
            carry = jnp.where(h == core, mine_c[...], part_c[...])
            out = local_ref[pl.ds(at, GR), h * DV : (h + 1) * DV] + nt_dot(both, carry)
            out = out * lax.rsqrt(jnp.mean(out * out, axis=-1, keepdims=True) + EPS) * gain
            u = gate_ref[pl.ds(at, GR), h * DV : (h + 1) * DV].astype(F32)
            mixed_ref[pl.ds(at, GR), h * DV : (h + 1) * DV] = (
                out * (u / (1.0 + jnp.exp(-u)))).astype(BF16)
        return 0

    lax.fori_loop(0, groups, last, 0)


def attention(q, k, v, lg, bias, extra, doc, gate, gain):
    rows = q.shape[0]
    doc_f = doc.astype(F32)
    aux = jnp.concatenate([extra, doc_f[:, None]], axis=1)
    docrow = doc_f.reshape(rows // GR, GR)
    vm = pl.BlockSpec(memory_space=pltpu.VMEM)
    blocks = rows // BL
    return pl.pallas_call(
        attention_kernel,
        out_shape=jax.ShapeDtypeStruct((rows, 2 * DV), BF16),
        in_specs=[vm] * 9,
        out_specs=vm,
        scratch_shapes=[
            pltpu.VMEM((rows, 2 * DK), F32),
            pltpu.VMEM((rows, 2 * DK), F32),
            pltpu.VMEM((blocks, 1, 2 * DK), F32),
            pltpu.VMEM((blocks * 2, DV, 2 * DK), F32),
            pltpu.VMEM((blocks * 2, DV, 2 * DK), BF16),
            pltpu.VMEM((2, DV, 2 * DK), F32),
            pltpu.VMEM((rows, 2 * DV), F32),
            pltpu.VMEM((2, 2 * DV, DK), BF16),
            pltpu.VMEM((2, 8, DK), F32),
            pltpu.VMEM((2 * DV, DK), BF16),
            pltpu.VMEM((8, DK), F32),
            pltpu.VMEM((2, DV, DK), BF16),
            pltpu.VMEM((8, DK), F32),
            pltpu.VMEM((NCHIP, DV, DK), BF16),
            pltpu.VMEM((NCHIP, 8, DK), F32),
            pltpu.VMEM((DV, 2 * DK), BF16),
            pltpu.VMEM((DV, 2 * DK), BF16),
            pltpu.VMEM((DV, 2 * DK), BF16),
            pltpu.VMEM((1, 2 * DK), F32),
            pltpu.SemaphoreType.DMA((3,)),
            pltpu.SemaphoreType.DMA((3,)),
            pltpu.SemaphoreType.DMA((NCHIP,)),
            pltpu.SemaphoreType.DMA((NCHIP,)),
            pltpu.SemaphoreType.DMA((NCHIP,)),
            pltpu.SemaphoreType.DMA((NCHIP,)),
        ],
        compiler_params=pltpu.CompilerParams(
            collective_id=0, has_side_effects=True, vmem_limit_bytes=48 * 2**20),
        cost_estimate=pl.CostEstimate(flops=3_000_000_000, bytes_accessed=8_000_000, transcendentals=0),
        name="attention",
    )(q, k, v, lg, bias.reshape(1, -1), aux, docrow, gate, gain.reshape(1, -1))


def row_norm(rows_f, gain):
    factor = lax.rsqrt(jnp.mean(rows_f * rows_f, axis=-1, keepdims=True) + EPS)
    return (rows_f * factor * gain.astype(F32)).astype(BF16)


def per_device(
    stream, queries, projected_keys, values, decay_gate_logits, decay_gate_bias, extra_log_decay,
    document_index, output_gate, head_norm_gain, output_weight, feedforward_norm_gain,
    gate_weight, up_weight, down_weight,
):
    both = lax.all_gather(jnp.concatenate([gate_weight, up_weight], axis=1), SP, axis=0, tiled=True)
    width = gate_weight.shape[1]
    whole_gate, whole_up = both[:, :width], both[:, width:]
    down = lax.all_gather(down_weight, SP)
    whole_down = jnp.moveaxis(down, 0, 1).reshape(down_weight.shape[0], -1)
    head_mixed = attention(
        queries, projected_keys, values, decay_gate_logits, decay_gate_bias, extra_log_decay,
        document_index, output_gate, head_norm_gain)
    tp_rows = stream.shape[0] // lax.axis_size("tp")
    tp_start = lax.axis_index("tp") * tp_rows
    partial = jnp.dot(head_mixed, output_weight, preferred_element_type=F32).astype(BF16)
    attended = lax.psum(partial, "tp").astype(F32)
    resid_all = stream.astype(F32) + attended
    normed = row_norm(resid_all, feedforward_norm_gain)
    resid_own = lax.dynamic_slice_in_dim(resid_all, tp_start, tp_rows, 0)
    gate_act = jnp.dot(normed, whole_gate, preferred_element_type=F32)
    up_act = jnp.dot(normed, whole_up, preferred_element_type=F32)
    hidden = (jax.nn.silu(gate_act) * up_act).astype(BF16)
    partial = jnp.dot(hidden, whole_down, preferred_element_type=F32).astype(BF16)
    tiles = partial.reshape(lax.axis_size("tp"), tp_rows, -1)
    arrived = lax.all_to_all(tiles, "tp", split_axis=0, concat_axis=0, tiled=True)
    return (resid_own + arrived.astype(F32).sum(axis=0)).astype(BF16)


def solution(mesh):
    torus = Mesh(mesh.devices.reshape(4, 4, 2, mesh.shape["tp"]), ("sp_0", "sp_1", "sp_2", "tp"))
    placed = (
        P(SP, None), P(SP, "tp"), P(SP, "tp"), P(SP, "tp"), P(SP, "tp"), P("tp"), P(SP, "tp"),
        P(SP), P(SP, "tp"), P(), P("tp", None), P(), P(SP, "tp"), P(SP, "tp"), P("tp", SP),
    )
    return jax.shard_map(
        per_device, mesh=torus, in_specs=placed, out_specs=P(SP_TP, None), check_vma=False
    )
```

time: 619 us -> 268 us (0.43)
  loops' own time: 103 us -> 0 us
  other arithmetic: 92.3 us -> 16.8 us
  local copies, waits for them, and re-layouts: 89.4 us -> 15.4 us
  blocking collectives: 58.1 us -> 0 us
  between operations: 71.5 us -> 15 us
  Pallas kernels: 0 us -> 32.1 us
  matrix products: 56.7 us -> 39.2 us
  waiting for transfers between devices: 135 us -> 142 us
    another operation x2 -> x0, loops' own time: 103 us -> none  [block_prefix(): totals, before = lax.scan(advance, initial, elements, reverse=reverse_dir)]
    all_gather x6 -> x0, blocking collectives: 58.1 us -> none  [collected_together(): both, at, found = (lax.all_gather(jnp.concatenate(lines), axis), 0, {})]
    dynamic_slice x64 -> x0, local copies, waits for them, and re-layouts: 40.2 us -> none  [block_prefix(): totals, before = lax.scan(advance, initial, elements, reverse=reverse_dir)]
    add x35 -> x1, other arithmetic: 43 us -> 8.34 us  [per_device(): resid_all = stream.astype(F32) + attended]
    pallas_call x0 -> x1, Pallas kernels: none -> 32.1 us  [attention(): pl.pallas_call(attention_kernel, out_shape=jax.ShapeDtypeStruct((rows, 2...]
    dynamic_update_slice x64 -> x0, other arithmetic: 23.5 us -> none  [block_prefix(): totals, before = lax.scan(advance, initial, elements, reverse=reverse_dir)]
    dot_general x9 -> x3, matrix products: 56.7 us -> 39.2 us  [the longest x1 22.2 us: per_device(): jnp.dot(hidden, whole_down, preferred_element_type=F32).astype(BF16)]
    slice x21 -> x0, local copies, waits for them, and re-layouts: 9.64 us -> none  [the longest x14 9.4 us: entering(): part[k].astype(own.dtype)]
  transfers between devices with their start and end apart: 5 -> 4, of which waited for: 2 -> 3; matrix products, arithmetic and copies ran while one was open for 32% -> 7% of each run, Pallas kernels for 0% -> 0%
where the time goes in v1:
time: 268 us; the launch traced here: 266 us
  waiting for transfers between devices  142 us (53%)
  matrix products  39.2 us (15%)
  Pallas kernels  32.1 us (12%)
  other arithmetic  16.8 us (6%)
  local copies, waits for them, and re-layouts  15.4 us (6%)
  between operations  15 us (6%)
  starting transfers between devices  5.61 us (2%)
    psum x1, waiting for transfers between devices, per_device(): attended = lax.psum(partial, 'tp').astype(F32)  88.9 us
    all_to_all x1, waiting for transfers between devices, per_device(): lax.all_to_all(tiles, 'tp', split_axis=0, concat_axis=0, tiled=True)  47.6 us
    pallas_call x1, Pallas kernels, attention(): pl.pallas_call(attention_kernel, out_shape=jax.ShapeDtypeStruct((rows, 2...  32.1 us
    dot_general x1, matrix products, per_device(): jnp.dot(hidden, whole_down, preferred_element_type=F32).astype(BF16)  22.2 us
    dot_general x1, matrix products, per_device(): gate_act = jnp.dot(normed, whole_gate, preferred_element_type=F32)  12.6 us
    unnamed x23, local copies, waits for them, and re-layouts  10.1 us
    add x1, other arithmetic, per_device(): resid_all = stream.astype(F32) + attended  8.34 us
  transfers between devices with their start and end apart: 4, of which 3 were waited for; matrix products, arithmetic and copies ran while one was open for 7% of the time, Pallas kernels for 0%

profile of v1, /device:TPU:6, one launch (start us, length us, event | category | flops | bytes accessed | tf_op | source)
XLA Modules:
  0.0 265.7 jit_solution(7373183576628583284)
XLA Ops:
  7.4 0.8 convert_element_type.31
  8.2 0.7 pad_maximum_fusion.1
  8.9 0.2 copy.22.aux_ref
  9.2 0.7 reshape.26.gain_ref
  9.8 1.2 copy-done.2
  11.1 1.2 copy-done.3
  12.3 1.0 copy-done.4
  13.3 1.0 copy-done.5
  14.4 1.0 copy-done.6
  15.4 0.7 copy-done.7
  16.1 32.1 %attention.1 = bf16[1024,512]{1,0:T(8,128)(2,1)S(1)} custom-call(bf16[1024,256]{1,0:T(8,128)(2,1)S(1)} %copy-done.4, bf16[1024,256]{1,0:T(8,128)(2,1)S(1)} %copy-done.5, bf16[1024,512]{1,0:T(8,128)(2,1)S(1)} %copy-done.2, bf16[1024,256]{1,0:T(8,128)(2,1)S(1)} %copy-done.6, f32[1,256]{1,0:T(1,128)S(1)} %bitcast.13, f32[1024,3]{1,0:T(8,128)S(1)} %copy.22.aux_ref, ...), custom_call_target="tpu_custom_call" | custom-call | flops 3000000000 | bytes 8000000 | tf_op jit(solution)/shard_map/attention/pallas_call | solution.py:304
  48.2 0.0 copy-start.8
  48.2 0.0 copy-start.9
  48.2 0.0 copy-start.10
  48.2 4.4 %convolution_convert_fusion = bf16[1024,2048]{1,0:T(8,128)(2,1)} fusion(bf16[1024,512]{1,0:T(8,128)(2,1)S(1)} %attention.1, bf16[512,2048]{1,0:T(8,128)(2,1)S(1)} %copy-done), kind=kOutput, calls=%fused_computation.11 | convolution fusion | flops 2149580800 | bytes 7340032 | tf_op jit(solution)/shard_map/dot_general | solution.py:363
  52.7 0.0 all-reduce.2.cloned.1.call-update
  52.7 0.0 all-gather.6.cloned.1.call-start
  52.8 0.5 all-gather.6.cloned.1.call-update
  53.3 0.2 all-gather.4.cloned.1.call-start
  53.5 0.8 pad_maximum_fusion
  54.3 0.0 all-gather.4.cloned.1.call-update
  54.3 88.9 %all-reduce.2.cloned.1.call-done = bf16[1024,2048]{1,0:T(8,128)(2,1)} async-done(((bf16[1024,2048]{1,0:T(8,128)(2,1)}), bf16[1024,2048]{1,0:T(8,128)(2,1)}) %all-reduce.2.cloned.1.call-update) | async-done | bytes 4194320 | tf_op jit(solution)/shard_map/psum | solution.py:364
  143.2 8.3 %convert_add_fusion = (f32[1024,2048]{1,0:T(8,128)}, f32[1024]{0:T(1024)S(1)}) fusion(bf16[1024,2048]{1,0:T(8,128)(2,1)} %all-reduce.2.cloned.1.call-done, bf16[1024,2048]{1,0:T(8,128)(2,1)} %param.15), kind=kLoop, calls=%fused_computation.3 | loop fusion | flops 10484736 | bytes 16781312 | tf_op jit(solution)/shard_map/add | solution.py:365
  151.6 3.8 %copy.24 = bf16[8,8,32,1408]{3,2,1,0:T(8,128)(2,1)S(1)} copy(bf16[8,8,32,1408]{3,1,2,0:T(8,128)(2,1)} %bitcast.15) | data formatting | bytes 11534336
  155.4 4.5 %copy.23 = bf16[1408,32,64]{0,2,1:T(8,128)(2,1)} copy(bf16[1408,32,64]{0,1,2:T(8,128)(2,1)S(1)} %bitcast.14) | data formatting | bytes 11534336 | tf_op jit(solution)/shard_map/transpose | solution.py:357
  159.8 4.5 %all-gather.4.cloned.1.call-done = bf16[2048,2816]{1,0:T(8,128)(2,1)} async-done(((bf16[64,2816]{1,0:T(8,128)(2,1)}), bf16[2048,2816]{1,0:T(8,128)(2,1)}) %all-gather.4.cloned.1.call-update) | async-done | bytes 11534352 | tf_op jit(solution)/shard_map/all_gather | solution.py:353
  164.4 12.6 %fusion.2 = f32[1024,1408]{1,0:T(8,128)} fusion(bf16[2048,2816]{1,0:T(8,128)(2,1)} %all-gather.4.cloned.1.call-done, f32[2048]{0:T(1024)S(1)} %convert_element_type.34, f32[1024]{0:T(1024)S(1)} %add_rsqrt_fusion, bf16[1024,2048]{1,0:T(8,128)(2,1)} %all-reduce.2.cloned.1.call-done, bf16[1024,2048]{1,0:T(8,128)(2,1)} %param.15), kind=kOutput, calls=%fused_computation.6 | convolution fusion | flops 5918162944 | bytes 19935232 | tf_op jit(solution)/shard_map/dot_general | solution.py:368
  177.0 22.2 %fusion.9 = bf16[1024,2048]{1,0:T(8,128)(2,1)} fusion(bf16[1408,2048]{0,1:T(8,128)(2,1)} %bitcast.16, f32[1024,1408]{1,0:T(8,128)} %fusion.2, bf16[2048,2816]{1,0:T(8,128)(2,1)} %all-gather.4.cloned.1.call-done, f32[2048]{0:T(1024)S(1)} %convert_element_type.34, f32[1024]{0:T(1024)S(1)} %add_rsqrt_fusion, ...), kind=kOutput, calls=%fused_computation.10 | convolution fusion | flops 11834490880 | bytes 29896704 | tf_op jit(solution)/shard_map/dot_general | solution.py:371
  199.2 5.3 %all-to-all-start = ((bf16[4,256,2048]{2,1,0:T(8,128)(2,1)}), bf16[4,256,2048]{2,1,0:T(8,128)(2,1)}, u32[]{:S(2)}, u32[]{:S(2)}) async-start(bf16[4,256,2048]{2,1,0:T(8,128)(2,1)} %bitcast.17), calls=%async_computation | async-start | bytes 8388608 | tf_op jit(solution)/shard_map/all_to_all | solution.py:373
  204.5 47.6 %all-to-all-done = bf16[4,256,2048]{2,1,0:T(8,128)(2,1)} async-done(((bf16[4,256,2048]{2,1,0:T(8,128)(2,1)}), bf16[4,256,2048]{2,1,0:T(8,128)(2,1)}, u32[]{:S(2)}, u32[]{:S(2)}) %all-to-all-start) | async-done | bytes 4194336 | tf_op jit(solution)/shard_map/all_to_all | solution.py:373
  252.1 3.3 %convert_reduce_fusion = f32[256,2048]{1,0:T(8,128)S(1)} fusion(bf16[4,256,2048]{2,1,0:T(8,128)(2,1)} %all-to-all-done), kind=kLoop, calls=%fused_computation | loop fusion | flops 3670016 | bytes 6291456 | tf_op jit(solution)/shard_map/reduce_sum | solution.py:374
  255.4 2.9 %add_convert_fusion = bf16[256,2048]{1,0:T(8,128)(2,1)} fusion(f32[256,2048]{1,0:T(8,128)S(1)} %convert_reduce_fusion, f32[1024,2048]{1,0:T(8,128)} %get-tuple-element.5, s32[]{:T(128)S(6)} %select_n.3), kind=kLoop, calls=%fused_computation.13 | loop fusion | flops 1048576 | bytes 5242884 | tf_op jit(solution)/shard_map/convert_element_type | solution.py:374
  (18 shorter events, 0.0 us)
Async XLA Ops:
  7.4 40.8 %copy-start = (bf16[512,2048]{1,0:T(8,128)(2,1)S(1)}, bf16[512,2048]{1,0:T(8,128)(2,1)}, u32[]{:S(2)}) copy-start(bf16[512,2048]{1,0:T(8,128)(2,1)} %param.25) | copy-start | bytes 6291460
  7.4 135.8 %all-reduce.2.cloned.1.call-start = ((), (), s32[]{:S(2)}) async-start(), calls=%async_computation.1 | async-start | bytes 8388608 | tf_op jit(solution)/shard_map/psum | solution.py:364
  9.8 1.2 copy-start.2
  11.1 1.2 copy-start.3
  12.3 1.0 copy-start.4
  13.3 1.0 copy-start.5
  14.4 1.0 copy-start.6
  15.4 0.7 copy-start.7
  48.2 5.3 %copy-start.8 = (bf16[64,1408]{1,0:T(8,128)(2,1)S(1)}, bf16[64,1408]{1,0:T(8,128)(2,1)}, u32[]{:S(2)}) copy-start(bf16[64,1408]{1,0:T(8,128)(2,1)} %param.28) | copy-start | bytes 540676
  48.2 5.3 %copy-start.9 = (bf16[64,1408]{1,0:T(8,128)(2,1)S(1)}, bf16[64,1408]{1,0:T(8,128)(2,1)}, u32[]{:S(2)}) copy-start(bf16[64,1408]{1,0:T(8,128)(2,1)} %param.27) | copy-start | bytes 540676
  48.2 6.1 %copy-start.10 = (bf16[2048]{0:T(1024)(128)(2,1)S(1)}, bf16[2048]{0:T(1024)(128)(2,1)}, u32[]{:S(2)}) copy-start(bf16[2048]{0:T(1024)(128)(2,1)} %param.26) | copy-start | bytes 12292
  52.7 98.9 %all-gather.6.cloned.1.call-start = ((), (), s32[]{:S(2)}) async-start(), calls=%async_computation.3 | async-start | bytes 5947392 | tf_op jit(solution)/shard_map/all_gather | solution.py:356
  53.3 111.1 %all-gather.4.cloned.1.call-start = ((), (), s32[]{:S(2)}) async-start(), calls=%async_computation.2 | async-start | bytes 11894784 | tf_op jit(solution)/shard_map/all_gather | solution.py:353
  199.2 52.9 %all-to-all-start = ((bf16[4,256,2048]{2,1,0:T(8,128)(2,1)}), bf16[4,256,2048]{2,1,0:T(8,128)(2,1)}, u32[]{:S(2)}, u32[]{:S(2)}) async-start(bf16[4,256,2048]{2,1,0:T(8,128)(2,1)} %bitcast.17), calls=%async_computation | async-start | bytes 8388608 | tf_op jit(solution)/shard_map/all_to_all | solution.py:373
  204.5 53.7 %copy-start.1 = (bf16[512,2048]{1,0:T(8,128)(2,1)S(1)}, bf16[512,2048]{1,0:T(8,128)(2,1)}, u32[]{:S(2)}) copy-start(bf16[512,2048]{1,0:T(8,128)(2,1)} %param.25) | copy-start | bytes 6291460
Sparse Core Ops, SparseCore 0:
  52.8 90.3 all-reduce.1
Sparse Core Ops, SparseCore 1:
  55.5 47.6 all-gather.5
  105.3 59.0 all-gather.3

commit v2 on v1

--- a/solution.py
+++ b/solution.py
@@ -340,9 +340,244 @@
     )(q, k, v, lg, bias.reshape(1, -1), aux, docrow, gate, gain.reshape(1, -1))
 
 
-def row_norm(rows_f, gain):
-    factor = lax.rsqrt(jnp.mean(rows_f * rows_f, axis=-1, keepdims=True) + EPS)
-    return (rows_f * factor * gain.astype(F32)).astype(BF16)
+def ffn_kernel(
+    mixed_ref, stream_ref, wo_ref, w_ref, gain_ref,
+    out_ref,
+    hm, st, wo_v, w_v, resid, keep, normed, hidden, s2, s1, s3, ra, rb, rl, rr,
+    local_sem, own_rs, own_ls, fwd_rs, fwd_ls, left_in, right_in, opp_l, opp_r,
+    rs_send, rs_recv,
+):
+    z, y, core = lax.axis_index("sp_0"), lax.axis_index("sp_1"), lax.axis_index("sp_2")
+    me = lax.axis_index("tp")
+    n = 4
+    q_rows = GR
+    half = q_rows // 2
+    d = out_ref.shape[1]
+    units = hidden.shape[1]
+    ix_r, ix_l = lax.rem(me + 1, n), lax.rem(me + n - 1, n)
+    right, left = (z, y, core, ix_r), (z, y, core, ix_l)
+
+    own = pltpu.make_async_copy(mixed_ref, hm.at[me], local_sem.at[0])
+    load_wo = pltpu.make_async_copy(wo_ref, wo_v, local_sem.at[1])
+    load_st = pltpu.make_async_copy(stream_ref, st, local_sem.at[2])
+    load_w = pltpu.make_async_copy(w_ref, w_v, local_sem.at[3])
+    own.start()
+    load_wo.start()
+    load_st.start()
+    load_w.start()
+    barrier = pltpu.get_barrier_semaphore()
+    pl.semaphore_signal(barrier, inc=1, device_id=right, device_id_type=MESH)
+    pl.semaphore_signal(barrier, inc=1, device_id=left, device_id_type=MESH)
+    pl.semaphore_wait(barrier, 2)
+    own.wait()
+
+    def piece(slot, r, part):
+        return hm.at[slot, pl.ds(pl.multiple_of(r * q_rows + part * half, half), half)]
+
+    def remote(ref, send, recv, target, dst=None):
+        return pltpu.make_async_remote_copy(
+            ref, ref if dst is None else dst, send, recv, device_id=target, device_id_type=MESH)
+
+    def own_right(r, p):
+        return remote(piece(me, r, p), own_rs.at[r * 2 + p], left_in.at[r * 2 + p], right)
+
+    def own_left(r, p):
+        return remote(piece(me, r, p), own_ls.at[r * 2 + p], right_in.at[r * 2 + p], left)
+
+    def fwd_right(r):
+        return remote(piece(ix_l, r, 0), fwd_rs.at[r], opp_l.at[r], right)
+
+    def fwd_left(r):
+        return remote(piece(ix_r, r, 1), fwd_ls.at[r], opp_r.at[r], left)
+
+    def came_left(r, p):
+        return remote(piece(ix_l, r, p), own_rs.at[r * 2 + p], left_in.at[r * 2 + p], right)
+
+    def came_right(r, p):
+        return remote(piece(ix_r, r, p), own_ls.at[r * 2 + p], right_in.at[r * 2 + p], left)
+
+    opposite = lax.rem(me + 2, n)
+
+    def came_opp_l(r):
+        return remote(piece(opposite, r, 0), fwd_rs.at[r], opp_l.at[r], right)
+
+    def came_opp_r(r):
+        return remote(piece(opposite, r, 1), fwd_ls.at[r], opp_r.at[r], left)
+
+    def send_own(r):
+        own_right(r, 0).start()
+        own_left(r, 1).start()
+        own_right(r, 1).start()
+        own_left(r, 0).start()
+
+    def pump(r):
+        came_left(r, 0).wait_recv()
+        fwd_right(r).start()
+        came_right(r, 1).wait_recv()
+        fwd_left(r).start()
+
+    send_own(0)
+    pump(0)
+    send_own(1)
+    load_wo.wait()
+    load_st.wait()
+
+    dh = d // 2
+    to_r_a = remote(s2.at[:, pl.ds(0, dh)], rs_send.at[0], rs_recv.at[0], right, ra)
+    to_l_b = remote(s2.at[:, pl.ds(dh, dh)], rs_send.at[1], rs_recv.at[1], left, rb)
+    to_r = remote(s1, rs_send.at[2], rs_recv.at[2], right, rl)
+    to_l = remote(s3, rs_send.at[3], rs_recv.at[3], left, rr)
+
+    def pass_on(role):
+        @pl.when(role == 1)
+        def _():
+            to_r_a.wait_recv()
+            s1[:, :dh] = (s1[:, :dh].astype(F32) + ra[...].astype(F32)).astype(BF16)
+            to_r.start()
+
+        @pl.when(role == 3)
+        def _():
+            to_l_b.wait_recv()
+            s3[:, dh:] = (s3[:, dh:].astype(F32) + rb[...].astype(F32)).astype(BF16)
+            to_l.start()
+
+    def quarter(q, _):
+        role = lax.rem(q - me + n, n)
+        at = pl.multiple_of(q * q_rows, q_rows)
+        rows = pl.ds(at, q_rows)
+        came_left(q, 1).wait_recv()
+        came_right(q, 0).wait_recv()
+        came_opp_l(q).wait_recv()
+        came_opp_r(q).wait_recv()
+
+        def project(j, total):
+            cols = pl.ds(pl.multiple_of(j * 512, 512), 512)
+            acc = st[rows, cols].astype(F32)
+            for k in range(n):
+                acc = acc + nn_dot(hm[k, rows, :], wo_v[k * 512 : (k + 1) * 512, cols])
+            resid[:, cols] = acc
+            return total + jnp.sum(acc * acc, axis=-1, keepdims=True)
+
+        squares = lax.fori_loop(0, d // 512, project, jnp.zeros((q_rows, 1), F32))
+
+        @pl.when(q < n - 1)
+        def _():
+            pump(q + 1)
+
+        @pl.when(q < n - 2)
+        def _():
+            send_own(q + 2)
+
+        @pl.when(q == 0)
+        def _():
+            load_w.wait()
+
+        factor = lax.rsqrt(squares / d + EPS)
+        normed[...] = (resid[...] * factor * gain_ref[...].astype(F32)).astype(BF16)
+
+        @pl.when(role == 0)
+        def _():
+            keep[...] = resid[...]
+
+        def gate_up(j, _):
+            both = nn_dot(normed[...], w_v[:, pl.ds(pl.multiple_of(j * 256, 256), 256)])
+            g, u = both[:, :128], both[:, 128:]
+            hidden[:, pl.ds(pl.multiple_of(j * 128, 128), 128)] = (
+                g / (1.0 + jnp.exp(-g)) * u).astype(BF16)
+            return 0
+
+        lax.fori_loop(0, units // 128, gate_up, 0)
+
+        @pl.when(q > 0)
+        def _():
+            pass_on(lax.rem(q - 1 - me + n, n))
+
+        def down(j, _):
+            at_col = pl.multiple_of(j * 256, 256)
+            cols = pl.ds(at_col, 256)
+            part = nt_dot(hidden[...], w_v[cols, 2 * units : 3 * units]).astype(BF16)
+
+            @pl.when(role == 0)
+            def _():
+                keep[:, cols] = keep[:, cols] + part.astype(F32)
+
+            @pl.when(role == 1)
+            def _():
+                s1[:, cols] = part
+
+            @pl.when(role == 2)
+            def _():
+                s2[:, cols] = part
+
+            @pl.when(role == 3)
+            def _():
+                s3[:, cols] = part
+
+            return 0
+
+        lax.fori_loop(0, d // 256, down, 0)
+
+        @pl.when(role == 2)
+        def _():
+            to_r_a.start()
+            to_l_b.start()
+
+        return 0
+
+    lax.fori_loop(0, n, quarter, 0)
+    pass_on(lax.rem(n - 1 - me + n, n))
+    to_r.wait_recv()
+    to_l.wait_recv()
+    out_ref[...] = (keep[...] + rl[...].astype(F32) + rr[...].astype(F32)).astype(BF16)
+
+    for r in range(n):
+        for p in range(2):
+            own_right(r, p).wait_send()
+            own_left(r, p).wait_send()
+        fwd_right(r).wait_send()
+        fwd_left(r).wait_send()
+    to_r_a.wait_send()
+    to_l_b.wait_send()
+    to_r.wait_send()
+    to_l.wait_send()
+
+
+def feed_forward(mixed, stream, wo, w, gain):
+    rows, d = stream.shape
+    units = w.shape[1] // 3
+    vm = pl.BlockSpec(memory_space=pltpu.VMEM)
+    hbm = pl.BlockSpec(memory_space=pl.ANY)
+    dma = pltpu.SemaphoreType.DMA
+    return pl.pallas_call(
+        ffn_kernel,
+        out_shape=jax.ShapeDtypeStruct((GR, d), BF16),
+        in_specs=[hbm, hbm, hbm, hbm, vm],
+        out_specs=vm,
+        scratch_shapes=[
+            pltpu.VMEM((4, rows, mixed.shape[1]), BF16),
+            pltpu.VMEM((rows, d), BF16),
+            pltpu.VMEM(wo.shape, BF16),
+            pltpu.VMEM(w.shape, BF16),
+            pltpu.VMEM((GR, d), F32),
+            pltpu.VMEM((GR, d), F32),
+            pltpu.VMEM((GR, d), BF16),
+            pltpu.VMEM((GR, units), BF16),
+            pltpu.VMEM((GR, d), BF16),
+            pltpu.VMEM((GR, d), BF16),
+            pltpu.VMEM((GR, d), BF16),
+            pltpu.VMEM((GR, d // 2), BF16),
+            pltpu.VMEM((GR, d // 2), BF16),
+            pltpu.VMEM((GR, d), BF16),
+            pltpu.VMEM((GR, d), BF16),
+            dma((4,)), dma((8,)), dma((8,)), dma((4,)), dma((4,)),
+            dma((8,)), dma((8,)), dma((4,)), dma((4,)), dma((4,)), dma((4,)),
+        ],
+        compiler_params=pltpu.CompilerParams(
+            collective_id=1, has_side_effects=True, vmem_limit_bytes=60 * 2**20),
+        cost_estimate=pl.CostEstimate(
+            flops=26_000_000_000, bytes_accessed=32_000_000, transcendentals=0),
+        name="feed_forward",
+    )(mixed, stream, wo, w, gain.reshape(1, -1))
 
 
 def per_device(
@@ -350,28 +585,16 @@
     document_index, output_gate, head_norm_gain, output_weight, feedforward_norm_gain,
     gate_weight, up_weight, down_weight,
 ):
-    both = lax.all_gather(jnp.concatenate([gate_weight, up_weight], axis=1), SP, axis=0, tiled=True)
-    width = gate_weight.shape[1]
-    whole_gate, whole_up = both[:, :width], both[:, width:]
-    down = lax.all_gather(down_weight, SP)
-    whole_down = jnp.moveaxis(down, 0, 1).reshape(down_weight.shape[0], -1)
+    own_rows, units = gate_weight.shape
+    pair = jnp.stack(
+        [gate_weight.reshape(own_rows, -1, 128), up_weight.reshape(own_rows, -1, 128)], axis=2)
+    shard = jnp.concatenate([pair.reshape(own_rows, 2 * units), down_weight.T], axis=1)
+    weights = lax.all_gather(shard, SP, axis=0, tiled=True)
+    whole_out = lax.all_gather(output_weight, "tp", axis=0, tiled=True)
     head_mixed = attention(
         queries, projected_keys, values, decay_gate_logits, decay_gate_bias, extra_log_decay,
         document_index, output_gate, head_norm_gain)
-    tp_rows = stream.shape[0] // lax.axis_size("tp")
-    tp_start = lax.axis_index("tp") * tp_rows
-    partial = jnp.dot(head_mixed, output_weight, preferred_element_type=F32).astype(BF16)
-    attended = lax.psum(partial, "tp").astype(F32)
-    resid_all = stream.astype(F32) + attended
-    normed = row_norm(resid_all, feedforward_norm_gain)
-    resid_own = lax.dynamic_slice_in_dim(resid_all, tp_start, tp_rows, 0)
-    gate_act = jnp.dot(normed, whole_gate, preferred_element_type=F32)
-    up_act = jnp.dot(normed, whole_up, preferred_element_type=F32)
-    hidden = (jax.nn.silu(gate_act) * up_act).astype(BF16)
-    partial = jnp.dot(hidden, whole_down, preferred_element_type=F32).astype(BF16)
-    tiles = partial.reshape(lax.axis_size("tp"), tp_rows, -1)
-    arrived = lax.all_to_all(tiles, "tp", split_axis=0, concat_axis=0, tiled=True)
-    return (resid_own + arrived.astype(F32).sum(axis=0)).astype(BF16)
+    return feed_forward(head_mixed, stream, whole_out, weights, feedforward_norm_gain)
 
 
 def solution(mesh):

time: 268 us -> 335 us (1.25)
  Pallas kernels: 32.1 us -> 186 us
  matrix products: 39.2 us -> 0 us
  other arithmetic: 16.8 us -> 0.97 us
  waiting for transfers between devices: 142 us -> 127 us
  local copies, waits for them, and re-layouts: 15.4 us -> 7.18 us
  starting transfers between devices: 5.61 us -> 0.04 us
    pallas_call x0 -> x1, Pallas kernels: none -> 154 us  [feed_forward(): pl.pallas_call(ffn_kernel, out_shape=jax.ShapeDtypeStruct((GR, d), BF16),...]
    all_gather x2, waiting for transfers between devices: 4.54 us -> 126 us  [the longest x1 78.3 us: per_device(): weights = lax.all_gather(shard, SP, axis=0, tiled=True)]
    psum x1 -> x0, waiting for transfers between devices: 88.9 us -> none  [per_device(): attended = lax.psum(partial, 'tp').astype(F32)]
    all_to_all x1 -> x0, waiting for transfers between devices: 47.6 us -> none  [per_device(): lax.all_to_all(tiles, 'tp', split_axis=0, concat_axis=0, tiled=True)]
    dot_general x3 -> x0, matrix products: 39.2 us -> none  [the longest x1 22.2 us: per_device(): jnp.dot(hidden, whole_down, preferred_element_type=F32).astype(BF16)]
    add x1 -> x0, other arithmetic: 8.34 us -> none  [per_device(): resid_all = stream.astype(F32) + attended]
    all_to_all x1 -> x0, starting transfers between devices: 5.34 us -> none  [per_device(): lax.all_to_all(tiles, 'tp', split_axis=0, concat_axis=0, tiled=True)]
    unnamed x23 -> x29, local copies, waits for them, and re-layouts: 10.1 us -> 5.55 us
  transfers between devices with their start and end apart: 4 -> 2, of which waited for: 3 -> 2; matrix products, arithmetic and copies ran while one was open for 7% -> 1% of each run, Pallas kernels for 0% -> 10%
where the time goes in v2:
time: 335 us; the launch traced here: 334 us
  Pallas kernels  186 us (56%)
  waiting for transfers between devices  127 us (38%)
  between operations  13.6 us (4%)
  local copies, waits for them, and re-layouts  7.18 us (2%)
    pallas_call x1, Pallas kernels, feed_forward(): pl.pallas_call(ffn_kernel, out_shape=jax.ShapeDtypeStruct((GR, d), BF16),...  154 us
    all_gather x1, waiting for transfers between devices, per_device(): weights = lax.all_gather(shard, SP, axis=0, tiled=True)  78.3 us
    all_gather x1, waiting for transfers between devices, per_device(): whole_out = lax.all_gather(output_weight, 'tp', axis=0, tiled=True)  47.8 us
    pallas_call x1, Pallas kernels, attention(): pl.pallas_call(attention_kernel, out_shape=jax.ShapeDtypeStruct((rows, 2...  32.1 us
  transfers between devices with their start and end apart: 2, of which 2 were waited for; matrix products, arithmetic and copies ran while one was open for 1% of the time, Pallas kernels for 10%

profile of v2, /device:TPU:6, one launch (start us, length us, event | category | flops | bytes accessed | tf_op | source)
XLA Modules:
  0.0 334.5 jit_solution(3184360715633667763)
XLA Ops:
  6.5 0.0 all-gather.3.cloned.1.call-start
  6.5 0.7 all-gather.3.cloned.1.call-update
  7.3 0.0 all-gather.5.cloned.1.call-start
  7.3 0.1 copy-done.7
  7.5 0.1 stack_reshape.6
  7.6 0.0 copy-done.8
  7.6 0.1 stack_reshape.7
  7.7 0.0 copy-start.13
  7.7 0.0 copy-start.12
  7.8 0.0 copy-start.11
  7.8 0.0 copy-start.10
  7.8 0.1 pad_maximum_fusion.1
  7.9 0.0 copy-start
  7.9 0.0 copy-start.1
  7.9 0.0 copy-start.2
  7.9 0.0 copy-start.5
  7.9 0.4 copy.23
  8.3 0.1 reshape.18
  8.5 0.9 pad_maximum_fusion
  9.4 0.0 all-gather.5.cloned.1.call-update
  9.4 0.6 reshape.19.gain_ref
  10.1 0.2 copy.22.aux_ref
  10.3 0.0 copy-start.3
  10.3 1.0 copy-done.3
  11.4 1.0 copy-done.4
  12.4 32.1 %attention.1.mixed_ref = bf16[1024,512]{1,0:T(8,128)(2,1)S(1)} custom-call(bf16[1024,256]{1,0:T(8,128)(2,1)S(1)} %copy-done.2, bf16[1024,256]{1,0:T(8,128)(2,1)S(1)} %copy-done.3, bf16[1024,512]{1,0:T(8,128)(2,1)S(1)} %copy-done, bf16[1024,256]{1,0:T(8,128)(2,1)S(1)} %copy-done.4, f32[1,256]{1,0:T(1,128)S(1)} %bitcast.3, f32[1024,3]{1,0:T(8,128)S(1)} %copy.22.aux_ref, ...), custom_call_target="tpu_custom_call" | custom-call | flops 3000000000 | bytes 8000000 | tf_op jit(solution)/shard_map/attention/pallas_call | solution.py:304
  44.5 0.0 copy-start.6
  44.5 1.0 copy-done.6
  45.5 47.8 %all-gather.3.cloned.1.call-done.wo_ref = bf16[2048,2048]{1,0:T(8,128)(2,1)} async-done(((bf16[512,2048]{1,0:T(8,128)(2,1)}), bf16[2048,2048]{1,0:T(8,128)(2,1)}) %all-gather.3.cloned.1.call-update) | async-done | bytes 8388624 | tf_op jit(solution)/shard_map/all_gather | solution.py:593
  93.2 78.3 %all-gather.5.cloned.1.call-done.w_ref = bf16[2048,4224]{1,0:T(8,128)(2,1)} async-done(((bf16[64,4224]{1,0:T(8,128)(2,1)}), bf16[2048,4224]{1,0:T(8,128)(2,1)}) %all-gather.5.cloned.1.call-update) | async-done | bytes 17301520 | tf_op jit(solution)/shard_map/all_gather | solution.py:592
  171.6 153.7 %feed_forward.1 = bf16[256,2048]{1,0:T(8,128)(2,1)} custom-call(bf16[1024,512]{1,0:T(8,128)(2,1)} %copy-done.6, bf16[1024,2048]{1,0:T(8,128)(2,1)} %stream_ref.1, bf16[2048,2048]{1,0:T(8,128)(2,1)} %all-gather.3.cloned.1.call-done.wo_ref, bf16[2048,4224]{1,0:T(8,128)(2,1)} %all-gather.5.cloned.1.call-done.w_ref, bf16[1,2048]{1,0:T(2,128)(2,1)} %reshape.19.gain_ref), custom_call_target="tpu_custom_call" | custom-call | flops 25999998976 | bytes 32000000 | tf_op jit(solution)/shard_map/feed_forward/pallas_call | solution.py:551
  325.3 2.3 copy.25
  (17 shorter events, 0.1 us)
Async XLA Ops:
  6.5 0.9 copy-start.7
  6.5 1.1 copy-start.8
  6.5 86.7 %all-gather.3.cloned.1.call-start = ((), (), s32[]{:S(2)}) async-start(), calls=%async_computation | async-start | bytes 10485760 | tf_op jit(solution)/shard_map/all_gather | solution.py:593
  7.3 1.2 copy-start.9
  7.3 164.3 %all-gather.5.cloned.1.call-start = ((), (), s32[]{:S(2)}) async-start(), calls=%async_computation.1 | async-start | bytes 17842176 | tf_op jit(solution)/shard_map/all_gather | solution.py:592
  7.7 1.7 copy-start.13
  7.7 1.7 copy-start.12
  7.8 1.7 copy-start.11
  7.8 2.3 copy-start.10
  7.9 2.4 copy-start
  7.9 2.4 copy-start.1
  7.9 2.4 copy-start.2
  7.9 2.4 copy-start.5
  10.3 1.0 copy-start.3
  11.4 1.0 copy-start.4
  44.5 1.0 copy-start.6
Sparse Core Ops, SparseCore 0:
  9.0 84.2 all-gather.2
  95.5 76.0 all-gather.4

commit v3 on v2

--- a/solution.py
+++ b/solution.py
@@ -343,7 +343,7 @@
 def ffn_kernel(
     mixed_ref, stream_ref, wo_ref, w_ref, gain_ref,
     out_ref,
-    hm, st, wo_v, w_v, resid, keep, normed, hidden, s2, s1, s3, ra, rb, rl, rr,
+    hm, st, wo_v, w_v, resid, normed, hidden, s2, s1, s3, ra, rb, rl, rr,
     local_sem, own_rs, own_ls, fwd_rs, fwd_ls, left_in, right_in, opp_l, opp_r,
     rs_send, rs_recv,
 ):
@@ -378,43 +378,60 @@
         return pltpu.make_async_remote_copy(
             ref, ref if dst is None else dst, send, recv, device_id=target, device_id_type=MESH)
 
-    def own_right(r, p):
-        return remote(piece(me, r, p), own_rs.at[r * 2 + p], left_in.at[r * 2 + p], right)
-
-    def own_left(r, p):
-        return remote(piece(me, r, p), own_ls.at[r * 2 + p], right_in.at[r * 2 + p], left)
-
-    def fwd_right(r):
-        return remote(piece(ix_l, r, 0), fwd_rs.at[r], opp_l.at[r], right)
-
-    def fwd_left(r):
-        return remote(piece(ix_r, r, 1), fwd_ls.at[r], opp_r.at[r], left)
-
-    def came_left(r, p):
-        return remote(piece(ix_l, r, p), own_rs.at[r * 2 + p], left_in.at[r * 2 + p], right)
-
-    def came_right(r, p):
-        return remote(piece(ix_r, r, p), own_ls.at[r * 2 + p], right_in.at[r * 2 + p], left)
+    order = (2, 1, 3, 0)
+
+    def quarter_of(owner, offset):
+        return lax.rem(owner + offset, n)
+
+    def wire(slot, quarter, part, send, recv, target):
+        return remote(piece(slot, quarter, part), send, recv, target)
+
+    to_right = (((3, 0), (3, 1), (0, 0)), ((2, 0), (2, 1)), ((0, 1), (1, 0)), ((1, 1),))
+    to_left = (((1, 1), (1, 0), (0, 1)), ((0, 0), (3, 1)), ((2, 1), (2, 0)), ((3, 0),))
+
+    def own_right(o, p):
+        return wire(me, quarter_of(me, o), p, own_rs.at[o * 2 + p], left_in.at[o * 2 + p], right)
+
+    def own_left(o, p):
+        return wire(me, quarter_of(me, o), p, own_ls.at[o * 2 + p], right_in.at[o * 2 + p], left)
+
+    def came_left(o, p):
+        return wire(ix_l, quarter_of(ix_l, o), p, own_rs.at[o * 2 + p], left_in.at[o * 2 + p], right)
+
+    def came_right(o, p):
+        return wire(ix_r, quarter_of(ix_r, o), p, own_ls.at[o * 2 + p], right_in.at[o * 2 + p], left)
+
+    def fwd_right(i):
+        return wire(ix_l, quarter_of(ix_r, order[i]), 0, fwd_rs.at[i], opp_l.at[i], right)
+
+    def fwd_left(i):
+        return wire(ix_r, quarter_of(ix_l, order[i]), 1, fwd_ls.at[i], opp_r.at[i], left)
 
     opposite = lax.rem(me + 2, n)
 
-    def came_opp_l(r):
-        return remote(piece(opposite, r, 0), fwd_rs.at[r], opp_l.at[r], right)
-
-    def came_opp_r(r):
-        return remote(piece(opposite, r, 1), fwd_ls.at[r], opp_r.at[r], left)
-
-    def send_own(r):
-        own_right(r, 0).start()
-        own_left(r, 1).start()
-        own_right(r, 1).start()
-        own_left(r, 0).start()
-
-    def pump(r):
-        came_left(r, 0).wait_recv()
-        fwd_right(r).start()
-        came_right(r, 1).wait_recv()
-        fwd_left(r).start()
+    def came_opp_l(i):
+        return wire(opposite, quarter_of(me, order[i]), 0, fwd_rs.at[i], opp_l.at[i], right)
+
+    def came_opp_r(i):
+        return wire(opposite, quarter_of(me, order[i]), 1, fwd_ls.at[i], opp_r.at[i], left)
+
+    def send_own(i):
+        for k in range(len(to_right[i])):
+            own_right(*to_right[i][k]).start()
+            own_left(*to_left[i][k]).start()
+
+    seen = set()
+
+    def arrived(side, o, p):
+        if (side, o, p) not in seen:
+            seen.add((side, o, p))
+            (came_left if side == "l" else came_right)(o, p).wait_recv()
+
+    def pump(i):
+        arrived("l", (2 + order[i]) % n, 0)
+        fwd_right(i).start()
+        arrived("r", (n - 2 + order[i]) % n, 1)
+        fwd_left(i).start()
 
     send_own(0)
     pump(0)
@@ -428,27 +445,15 @@
     to_r = remote(s1, rs_send.at[2], rs_recv.at[2], right, rl)
     to_l = remote(s3, rs_send.at[3], rs_recv.at[3], left, rr)
 
-    def pass_on(role):
-        @pl.when(role == 1)
-        def _():
-            to_r_a.wait_recv()
-            s1[:, :dh] = (s1[:, :dh].astype(F32) + ra[...].astype(F32)).astype(BF16)
-            to_r.start()
-
-        @pl.when(role == 3)
-        def _():
-            to_l_b.wait_recv()
-            s3[:, dh:] = (s3[:, dh:].astype(F32) + rb[...].astype(F32)).astype(BF16)
-            to_l.start()
-
-    def quarter(q, _):
-        role = lax.rem(q - me + n, n)
+    for i in range(n):
+        q = quarter_of(me, order[i])
         at = pl.multiple_of(q * q_rows, q_rows)
         rows = pl.ds(at, q_rows)
-        came_left(q, 1).wait_recv()
-        came_right(q, 0).wait_recv()
-        came_opp_l(q).wait_recv()
-        came_opp_r(q).wait_recv()
+        for p in range(2):
+            arrived("l", (1 + order[i]) % n, p)
+            arrived("r", (n - 1 + order[i]) % n, p)
+        came_opp_l(i).wait_recv()
+        came_opp_r(i).wait_recv()
 
         def project(j, total):
             cols = pl.ds(pl.multiple_of(j * 512, 512), 512)
@@ -459,25 +464,14 @@
             return total + jnp.sum(acc * acc, axis=-1, keepdims=True)
 
         squares = lax.fori_loop(0, d // 512, project, jnp.zeros((q_rows, 1), F32))
-
-        @pl.when(q < n - 1)
-        def _():
-            pump(q + 1)
-
-        @pl.when(q < n - 2)
-        def _():
-            send_own(q + 2)
-
-        @pl.when(q == 0)
-        def _():
+        if i < n - 1:
+            pump(i + 1)
+        if i < n - 2:
+            send_own(i + 2)
+        if i == 0:
             load_w.wait()
-
         factor = lax.rsqrt(squares / d + EPS)
         normed[...] = (resid[...] * factor * gain_ref[...].astype(F32)).astype(BF16)
-
-        @pl.when(role == 0)
-        def _():
-            keep[...] = resid[...]
 
         def gate_up(j, _):
             both = nn_dot(normed[...], w_v[:, pl.ds(pl.multiple_of(j * 256, 256), 256)])
@@ -487,55 +481,40 @@
             return 0
 
         lax.fori_loop(0, units // 128, gate_up, 0)
-
-        @pl.when(q > 0)
-        def _():
-            pass_on(lax.rem(q - 1 - me + n, n))
+        target = (s2, s1, s3, resid)[i]
 
         def down(j, _):
-            at_col = pl.multiple_of(j * 256, 256)
-            cols = pl.ds(at_col, 256)
+            cols = pl.ds(pl.multiple_of(j * 256, 256), 256)
             part = nt_dot(hidden[...], w_v[cols, 2 * units : 3 * units]).astype(BF16)
-
-            @pl.when(role == 0)
-            def _():
-                keep[:, cols] = keep[:, cols] + part.astype(F32)
-
-            @pl.when(role == 1)
-            def _():
-                s1[:, cols] = part
-
-            @pl.when(role == 2)
-            def _():
-                s2[:, cols] = part
-
-            @pl.when(role == 3)
-            def _():
-                s3[:, cols] = part
-
+            if i < n - 1:
+                target[:, cols] = part
+            else:
+                target[:, cols] = target[:, cols] + part.astype(F32)
             return 0
 
         lax.fori_loop(0, d // 256, down, 0)
-
-        @pl.when(role == 2)
-        def _():
+        if i == 0:
             to_r_a.start()
             to_l_b.start()
-
-        return 0
-
-    lax.fori_loop(0, n, quarter, 0)
-    pass_on(lax.rem(n - 1 - me + n, n))
+        if i == 2:
+            to_r_a.wait_recv()
+            s1[:, :dh] = (s1[:, :dh].astype(F32) + ra[...].astype(F32)).astype(BF16)
+            to_r.start()
+            to_l_b.wait_recv()
+            s3[:, dh:] = (s3[:, dh:].astype(F32) + rb[...].astype(F32)).astype(BF16)
+            to_l.start()
+
     to_r.wait_recv()
     to_l.wait_recv()
-    out_ref[...] = (keep[...] + rl[...].astype(F32) + rr[...].astype(F32)).astype(BF16)
-
-    for r in range(n):
+    out_ref[...] = (resid[...] + rl[...].astype(F32) + rr[...].astype(F32)).astype(BF16)
+
+    for o in range(n):
         for p in range(2):
-            own_right(r, p).wait_send()
-            own_left(r, p).wait_send()
-        fwd_right(r).wait_send()
-        fwd_left(r).wait_send()
+            own_right(o, p).wait_send()
+            own_left(o, p).wait_send()
+    for i in range(n):
+        fwd_right(i).wait_send()
+        fwd_left(i).wait_send()
     to_r_a.wait_send()
     to_l_b.wait_send()
     to_r.wait_send()
@@ -558,7 +537,6 @@
             pltpu.VMEM((rows, d), BF16),
             pltpu.VMEM(wo.shape, BF16),
             pltpu.VMEM(w.shape, BF16),
-            pltpu.VMEM((GR, d), F32),
             pltpu.VMEM((GR, d), F32),
             pltpu.VMEM((GR, d), BF16),
             pltpu.VMEM((GR, units), BF16),

time: 335 us -> 266 us (0.79)
  Pallas kernels: 186 us -> 117 us
    pallas_call x1, Pallas kernels: 154 us -> 85 us  [feed_forward(): pl.pallas_call(ffn_kernel, out_shape=jax.ShapeDtypeStruct((GR, d), BF16),...]
  transfers between devices with their start and end apart: 2 -> 2, of which waited for: 2 -> 2; matrix products, arithmetic and copies ran while one was open for 1% -> 1% of each run, Pallas kernels for 10% -> 12%
where the time goes in v3:
time: 266 us
  waiting for transfers between devices  127 us (48%)
  Pallas kernels  117 us (44%)
  between operations  13.6 us (5%)
  local copies, waits for them, and re-layouts  7.18 us (3%)
    pallas_call x1, Pallas kernels, feed_forward(): pl.pallas_call(ffn_kernel, out_shape=jax.ShapeDtypeStruct((GR, d), BF16),...  85 us
    all_gather x1, waiting for transfers between devices, per_device(): weights = lax.all_gather(shard, SP, axis=0, tiled=True)  78.3 us
    all_gather x1, waiting for transfers between devices, per_device(): whole_out = lax.all_gather(output_weight, 'tp', axis=0, tiled=True)  47.8 us
    pallas_call x1, Pallas kernels, attention(): pl.pallas_call(attention_kernel, out_shape=jax.ShapeDtypeStruct((rows, 2...  32.1 us
    unnamed x29, local copies, waits for them, and re-layouts  5.55 us
  transfers between devices with their start and end apart: 2, of which 2 were waited for; matrix products, arithmetic and copies ran while one was open for 1% of the time, Pallas kernels for 12%

profile of v3, /device:TPU:6, one launch (start us, length us, event | category | flops | bytes accessed | tf_op | source)
XLA Modules:
  0.0 265.7 jit_solution(16310923908381268626)
XLA Ops:
  6.5 0.7 all-gather.3.cloned.1.call-update
  7.3 0.0 all-gather.5.cloned.1.call-start
  7.3 0.1 copy-done.7
  7.5 0.1 stack_reshape.6
  7.6 0.0 copy-done.8
  7.6 0.1 stack_reshape.7
  7.7 0.0 copy-start.13
  7.7 0.0 copy-start.12
  7.8 0.0 copy-start.11
  7.8 0.0 copy-start.10
  7.8 0.1 pad_maximum_fusion.1
  7.9 0.0 copy-start
  7.9 0.0 copy-start.1
  7.9 0.0 copy-start.2
  7.9 0.0 copy-start.5
  7.9 0.4 copy.23
  8.3 0.1 reshape.18
  8.5 0.0 copy-done.9
  8.5 0.9 pad_maximum_fusion
  9.4 0.0 all-gather.5.cloned.1.call-update
  9.4 0.6 reshape.19.gain_ref
  10.1 0.2 copy.22.aux_ref
  10.3 0.0 copy-start.3
  10.3 1.0 copy-done.3
  11.4 1.0 copy-done.4
  12.4 32.1 %attention.1.mixed_ref = bf16[1024,512]{1,0:T(8,128)(2,1)S(1)} custom-call(bf16[1024,256]{1,0:T(8,128)(2,1)S(1)} %copy-done.2, bf16[1024,256]{1,0:T(8,128)(2,1)S(1)} %copy-done.3, bf16[1024,512]{1,0:T(8,128)(2,1)S(1)} %copy-done, bf16[1024,256]{1,0:T(8,128)(2,1)S(1)} %copy-done.4, f32[1,256]{1,0:T(1,128)S(1)} %bitcast.3, f32[1024,3]{1,0:T(8,128)S(1)} %copy.22.aux_ref, ...), custom_call_target="tpu_custom_call" | custom-call | flops 3000000000 | bytes 8000000 | tf_op jit(solution)/shard_map/attention/pallas_call | solution.py:304
  44.5 0.0 copy-start.6
  44.5 1.0 copy-done.6
  45.5 47.8 %all-gather.3.cloned.1.call-done.wo_ref = bf16[2048,2048]{1,0:T(8,128)(2,1)} async-done(((bf16[512,2048]{1,0:T(8,128)(2,1)}), bf16[2048,2048]{1,0:T(8,128)(2,1)}) %all-gather.3.cloned.1.call-update) | async-done | bytes 8388624 | tf_op jit(solution)/shard_map/all_gather | solution.py:571
  93.2 78.3 %all-gather.5.cloned.1.call-done.w_ref = bf16[2048,4224]{1,0:T(8,128)(2,1)} async-done(((bf16[64,4224]{1,0:T(8,128)(2,1)}), bf16[2048,4224]{1,0:T(8,128)(2,1)}) %all-gather.5.cloned.1.call-update) | async-done | bytes 17301520 | tf_op jit(solution)/shard_map/all_gather | solution.py:570
  171.6 85.0 %feed_forward.1 = bf16[256,2048]{1,0:T(8,128)(2,1)} custom-call(bf16[1024,512]{1,0:T(8,128)(2,1)} %copy-done.6, bf16[1024,2048]{1,0:T(8,128)(2,1)} %stream_ref.1, bf16[2048,2048]{1,0:T(8,128)(2,1)} %all-gather.3.cloned.1.call-done.wo_ref, bf16[2048,4224]{1,0:T(8,128)(2,1)} %all-gather.5.cloned.1.call-done.w_ref, bf16[1,2048]{1,0:T(2,128)(2,1)} %reshape.19.gain_ref), custom_call_target="tpu_custom_call" | custom-call | flops 25999998976 | bytes 32000000 | tf_op jit(solution)/shard_map/feed_forward/pallas_call | solution.py:530
  256.6 2.3 copy.25
  (17 shorter events, 0.1 us)
Async XLA Ops:
  6.5 0.9 copy-start.7
  6.5 1.1 copy-start.8
  6.5 86.7 %all-gather.3.cloned.1.call-start = ((), (), s32[]{:S(2)}) async-start(), calls=%async_computation | async-start | bytes 10485760 | tf_op jit(solution)/shard_map/all_gather | solution.py:571
  7.3 1.2 copy-start.9
  7.3 164.3 %all-gather.5.cloned.1.call-start = ((), (), s32[]{:S(2)}) async-start(), calls=%async_computation.1 | async-start | bytes 17842176 | tf_op jit(solution)/shard_map/all_gather | solution.py:570
  7.7 1.7 copy-start.13
  7.7 1.7 copy-start.12
  7.8 1.7 copy-start.11
  7.8 2.3 copy-start.10
  7.9 2.4 copy-start
  7.9 2.4 copy-start.1
  7.9 2.4 copy-start.2
  7.9 2.4 copy-start.5
  10.3 1.0 copy-start.3
  11.4 1.0 copy-start.4
  44.5 1.0 copy-start.6
Sparse Core Ops, SparseCore 0:
  9.0 84.2 all-gather.2
  95.5 76.0 all-gather.4

commit v4 on v3

--- a/solution.py
+++ b/solution.py
@@ -34,12 +34,228 @@
     return lax.dot_general(a, b, (((1,), (0,)), ((), ())), preferred_element_type=F32)
 
 
+def remote_copy(src, dst, send, recv, target):
+    return pltpu.make_async_remote_copy(
+        src, dst, send, recv, device_id=target, device_id_type=MESH)
+
+
+class PlaneGather:
+    SEMS = (40, 40, 32, 32, 1)
+
+    def __init__(self, src, dst, sems):
+        self.src, self.dst = src, dst
+        self.send, self.recv, self.core_send, self.core_recv, self.local = sems
+        self.at = {"z": lax.axis_index("sp_0"), "y": lax.axis_index("sp_1")}
+        self.core, self.x = lax.axis_index("sp_2"), lax.axis_index("tp")
+        self.rows = src.shape[0] // 2
+
+    def shifted(self, moves):
+        at = dict(self.at)
+        for axis, k in moves:
+            at[axis] = lax.rem(at[axis] + (k + 4), 4)
+        return at["z"], at["y"]
+
+    def chip_at(self, axis, k):
+        z, y = self.shifted([(axis, k)])
+        return z, y, self.core, self.x
+
+    def piece(self, hf, ja, jb, sub=None):
+        a, b = ("y", "z") if hf == 0 else ("z", "y")
+        z, y = self.shifted([(a, ja), (b, jb)])
+        row = ((z * NY + y) * 2 + self.core) * (2 * self.rows) + hf * self.rows
+        size = self.rows
+        if sub is not None:
+            size = size // 2
+            row = row + sub * size
+        return self.dst.at[pl.ds(pl.multiple_of(row, 16), size)]
+
+    def axis(self, hf, stage):
+        return ("y", "z")[(hf + stage) % 2]
+
+    OFFS = (0, -1, 1, 2)
+
+    def hop(self, hf, stage, ja, way, forward):
+        axis = self.axis(hf, stage)
+        k = hf * 20 + (0 if stage == 0 else 4 + 4 * self.OFFS.index(ja)) + (0 if way > 0 else 1)
+        k = k + (2 if forward else 0)
+        target = self.chip_at(axis, way)
+        if forward:
+            sub = 0 if way > 0 else 1
+            ref = self.piece(hf, -way, 0, sub) if stage == 0 else self.piece(hf, ja, -way, sub)
+            src = ref
+        else:
+            ref = self.piece(hf, 0, 0) if stage == 0 else self.piece(hf, ja, 0)
+            own = stage == 0 or ja == 0
+            src = self.src.at[pl.ds(hf * self.rows, self.rows)] if own else ref
+        return remote_copy(src, ref, self.send.at[k], self.recv.at[k], target)
+
+    def landing(self, hf, stage, ja, way, forward):
+        axis = self.axis(hf, stage)
+        k = hf * 20 + (0 if stage == 0 else 4 + 4 * self.OFFS.index(ja)) + (0 if way > 0 else 1)
+        k = k + (2 if forward else 0)
+        back = 2 if forward else -way
+        sub = (0 if way > 0 else 1) if forward else None
+        ref = self.piece(hf, back, 0, sub) if stage == 0 else self.piece(hf, ja, back, sub)
+        return remote_copy(ref, ref, self.send.at[k], self.recv.at[k], self.chip_at(axis, way))
+
+    def hand(self, hf, ja, jb):
+        p = hf * 16 + self.OFFS.index(ja) * 4 + self.OFFS.index(jb)
+        ref = self.piece(hf, ja, jb)
+        src = self.src.at[pl.ds(hf * self.rows, self.rows)] if ja == 0 and jb == 0 else ref
+        partner = (self.at["z"], self.at["y"], 1 - self.core, self.x)
+        return remote_copy(src, ref, self.core_send.at[p], self.core_recv.at[p], partner)
+
+    def handed(self, hf, ja, jb):
+        p = hf * 16 + self.OFFS.index(ja) * 4 + self.OFFS.index(jb)
+        a, b = ("y", "z") if hf == 0 else ("z", "y")
+        z, y = self.shifted([(a, ja), (b, jb)])
+        row = ((z * NY + y) * 2 + 1 - self.core) * (2 * self.rows) + hf * self.rows
+        ref = self.dst.at[pl.ds(pl.multiple_of(row, 16), self.rows)]
+        partner = (self.at["z"], self.at["y"], 1 - self.core, self.x)
+        return remote_copy(ref, ref, self.core_send.at[p], self.core_recv.at[p], partner)
+
+    def keep(self):
+        row = ((self.at["z"] * NY + self.at["y"]) * 2 + self.core) * (2 * self.rows)
+        return pltpu.make_async_copy(
+            self.src, self.dst.at[pl.ds(pl.multiple_of(row, 16), 2 * self.rows)], self.local.at[0])
+
+    def start(self):
+        for stage in range(2):
+            for hf in range(2):
+                for way in (1, -1):
+                    self.hop(hf, stage, 0, way, False).start()
+        for hf in range(2):
+            self.hand(hf, 0, 0).start()
+        self.keep().start()
+
+    def second(self, hf, ja):
+        for way in (1, -1):
+            self.hop(hf, 1, ja, way, False).start()
+        self.hand(hf, ja, 0).start()
+
+    def near(self):
+        for way in (1, -1):
+            for hf in range(2):
+                self.landing(hf, 0, 0, way, False).wait_recv()
+                self.hop(hf, 0, 0, way, True).start()
+                self.second(hf, -way)
+
+    def far(self):
+        for hf in range(2):
+            for way in (1, -1):
+                self.landing(hf, 0, 0, way, True).wait_recv()
+            self.second(hf, 2)
+
+    def column(self, ja):
+        for way in (1, -1):
+            for hf in range(2):
+                self.landing(hf, 1, ja, way, False).wait_recv()
+                self.hop(hf, 1, ja, way, True).start()
+                self.hand(hf, ja, -way).start()
+
+    def column_far(self, ja):
+        for hf in range(2):
+            for way in (1, -1):
+                self.landing(hf, 1, ja, way, True).wait_recv()
+            self.hand(hf, ja, 2).start()
+
+    def finish(self):
+        self.keep().wait()
+        for hf in range(2):
+            for ja in self.OFFS:
+                for jb in self.OFFS:
+                    self.handed(hf, ja, jb).wait_recv()
+
+    def drain(self):
+        for hf in range(2):
+            for way in (1, -1):
+                for forward in (False, True):
+                    self.hop(hf, 0, 0, way, forward).wait_send()
+                    for ja in self.OFFS:
+                        self.hop(hf, 1, ja, way, forward).wait_send()
+            for ja in self.OFFS:
+                for jb in self.OFFS:
+                    self.hand(hf, ja, jb).wait_send()
+
+
+class RowGather:
+    SEMS = (4, 4, 3, 3)
+
+    def __init__(self, src, dst, sems):
+        self.src, self.dst = src, dst
+        self.send, self.recv, self.core_send, self.core_recv = sems
+        self.z, self.y = lax.axis_index("sp_0"), lax.axis_index("sp_1")
+        self.core, self.x = lax.axis_index("sp_2"), lax.axis_index("tp")
+        self.rows = src.shape[0]
+
+    def piece(self, k, core, sub=None):
+        size = self.rows // 2
+        row = lax.rem(self.x + (k + 4), 4) * self.rows + core * size
+        if sub is not None:
+            size = size // 2
+            row = row + sub * size
+        return self.dst.at[pl.ds(pl.multiple_of(row, 16), size)]
+
+    def side(self, way):
+        return (self.z, self.y, self.core, lax.rem(self.x + (way + 4), 4))
+
+    def hop(self, way, forward):
+        k = (0 if way > 0 else 1) + (2 if forward else 0)
+        if forward:
+            dst = self.piece(-way, self.core, 0 if way > 0 else 1)
+            src = dst
+        else:
+            dst = self.piece(0, self.core)
+            size = self.rows // 2
+            src = self.src.at[pl.ds(pl.multiple_of(self.core * size, 16), size)]
+        return remote_copy(src, dst, self.send.at[k], self.recv.at[k], self.side(way))
+
+    def landing(self, way, forward):
+        k = (0 if way > 0 else 1) + (2 if forward else 0)
+        ref = self.piece(2, self.core, 0 if way > 0 else 1) if forward else self.piece(-way, self.core)
+        return remote_copy(ref, ref, self.send.at[k], self.recv.at[k], self.side(way))
+
+    def hand(self, i, arriving=False):
+        k = (-1, 1, 2)[i]
+        ref = self.piece(k, 1 - self.core if arriving else self.core)
+        return remote_copy(
+            ref, ref, self.core_send.at[i], self.core_recv.at[i], (self.z, self.y, 1 - self.core, self.x))
+
+    def start(self):
+        for way in (1, -1):
+            self.hop(way, False).start()
+
+    def near(self):
+        for i, way in enumerate((1, -1)):
+            self.landing(way, False).wait_recv()
+            self.hop(way, True).start()
+            self.hand(i).start()
+
+    def far(self):
+        for way in (1, -1):
+            self.landing(way, True).wait_recv()
+        self.hand(2).start()
+
+    def finish(self):
+        for i in range(3):
+            self.hand(i, True).wait_recv()
+        for way in (1, -1):
+            for forward in (False, True):
+                self.hop(way, forward).wait_send()
+        for i in range(3):
+            self.hand(i).wait_send()
+
+
+def plane_sems():
+    return [pltpu.SemaphoreType.DMA((k,)) for k in PlaneGather.SEMS]
+
+
 def attention_kernel(
-    q_ref, k_ref, v_ref, lg_ref, bias_ref, aux_ref, docrow_ref, gate_ref, gain_ref,
-    mixed_ref,
+    q_ref, k_ref, v_ref, lg_ref, bias_ref, aux_ref, docrow_ref, gate_ref, gain_ref, shard_ref, wo_ref,
+    mixed_ref, whole_ref, whole_wo_ref,
     cum_ref, glob_ref, blk_ref, states_ref, before_ref, run_ref, local_ref,
     own_t, own_e, part_t, part_e, chip_t, chip_e, recv_t, recv_e, mine_c, send_c, part_c, sum_ref,
-    core_send, core_recv, t_send, t_recv, e_send, e_recv,
+    core_send, core_recv, t_send, t_recv, e_send, e_recv, *gather_sems,
 ):
     rows = q_ref.shape[0]
     blocks = rows // BL
@@ -62,6 +278,14 @@
     pl.semaphore_signal(barrier, inc=1, device_id=partner, device_id_type=MESH)
     for k in range(1, NCHIP):
         pl.semaphore_signal(barrier, inc=1, device_id=chip_peer(k)[1], device_id_type=MESH)
+    for k in (1, 3):
+        pl.semaphore_signal(
+            barrier, inc=1, device_id=(z, y, core, lax.rem(x + k, 4)), device_id_type=MESH)
+    pl.semaphore_wait(barrier, NCHIP + 2)
+    plane = PlaneGather(shard_ref, whole_ref, gather_sems[:5])
+    ring = RowGather(wo_ref, whole_wo_ref, gather_sems[5:])
+    plane.start()
+    ring.start()
 
     ri = lax.broadcasted_iota(jnp.int32, (GR, GR), 0)
     ci = lax.broadcasted_iota(jnp.int32, (GR, GR), 1)
@@ -141,7 +365,6 @@
         own_e[h, 2:3] = last_doc
         own_e[h, 3:8] = jnp.zeros((5, DK), F32)
 
-    pl.semaphore_wait(barrier, NCHIP)
     swap_t = pltpu.make_async_remote_copy(
         own_t.at[1 - core], part_t, core_send.at[0], core_recv.at[0],
         device_id=partner, device_id_type=MESH)
@@ -182,6 +405,7 @@
             device_id=target, device_id_type=MESH))
     for s in sends:
         s.start()
+    plane.near()
 
     def inside(g, _):
         at = pl.multiple_of(g * GR, GR)
@@ -225,10 +449,16 @@
                     both.astype(BF16), before_ref[(g * per + b) * 2 + h])
         return 0
 
-    lax.fori_loop(0, groups, inside, 0)
+    lax.fori_loop(0, groups // 2, inside, 0)
+    plane.far()
+    plane.column(0)
+    lax.fori_loop(groups // 2, groups, inside, 0)
+    ring.near()
+    plane.column(-1)
 
     for s in sends:
         s.wait()
+    plane.column(1)
     run_ref[0] = jnp.zeros_like(run_ref[0])
 
     def earlier(j, _):
@@ -292,20 +522,32 @@
         return 0
 
     lax.fori_loop(0, groups, last, 0)
-
-
-def attention(q, k, v, lg, bias, extra, doc, gate, gain):
+    plane.column(2)
+    for ja in PlaneGather.OFFS:
+        plane.column_far(ja)
+    ring.far()
+    plane.finish()
+    plane.drain()
+    ring.finish()
+
+
+def attention(q, k, v, lg, bias, extra, doc, gate, gain, shard, wo):
     rows = q.shape[0]
     doc_f = doc.astype(F32)
     aux = jnp.concatenate([extra, doc_f[:, None]], axis=1)
     docrow = doc_f.reshape(rows // GR, GR)
     vm = pl.BlockSpec(memory_space=pltpu.VMEM)
+    hbm = pl.BlockSpec(memory_space=pl.ANY)
     blocks = rows // BL
     return pl.pallas_call(
         attention_kernel,
-        out_shape=jax.ShapeDtypeStruct((rows, 2 * DV), BF16),
-        in_specs=[vm] * 9,
-        out_specs=vm,
+        out_shape=(
+            jax.ShapeDtypeStruct((rows, 2 * DV), BF16),
+            jax.ShapeDtypeStruct((shard.shape[0] * 2 * NCHIP, shard.shape[1]), BF16),
+            jax.ShapeDtypeStruct((wo.shape[0] * 4, wo.shape[1]), BF16),
+        ),
+        in_specs=[vm] * 10 + [hbm],
+        out_specs=(vm, hbm, hbm),
         scratch_shapes=[
             pltpu.VMEM((rows, 2 * DK), F32),
             pltpu.VMEM((rows, 2 * DK), F32),
@@ -332,20 +574,20 @@
             pltpu.SemaphoreType.DMA((NCHIP,)),
             pltpu.SemaphoreType.DMA((NCHIP,)),
             pltpu.SemaphoreType.DMA((NCHIP,)),
-        ],
+        ] + plane_sems() + [pltpu.SemaphoreType.DMA((k,)) for k in RowGather.SEMS],
         compiler_params=pltpu.CompilerParams(
             collective_id=0, has_side_effects=True, vmem_limit_bytes=48 * 2**20),
         cost_estimate=pl.CostEstimate(flops=3_000_000_000, bytes_accessed=8_000_000, transcendentals=0),
         name="attention",
-    )(q, k, v, lg, bias.reshape(1, -1), aux, docrow, gate, gain.reshape(1, -1))
+    )(q, k, v, lg, bias.reshape(1, -1), aux, docrow, gate, gain.reshape(1, -1), shard, wo)
 
 
 def ffn_kernel(
-    mixed_ref, stream_ref, wo_ref, w_ref, gain_ref,
+    mixed_ref, stream_ref, own_wo_ref, wo_ref, w_ref, shard_ref, gain_ref,
     out_ref,
-    hm, st, wo_v, w_v, resid, normed, hidden, s2, s1, s3, ra, rb, rl, rr,
+    hm, st, wo_v, w_v, down_v, resid, normed, hidden, s2, s1, s3, ra, rb, rl, rr,
     local_sem, own_rs, own_ls, fwd_rs, fwd_ls, left_in, right_in, opp_l, opp_r,
-    rs_send, rs_recv,
+    rs_send, rs_recv, *gather_sems,
 ):
     z, y, core = lax.axis_index("sp_0"), lax.axis_index("sp_1"), lax.axis_index("sp_2")
     me = lax.axis_index("tp")
@@ -358,17 +600,33 @@
     right, left = (z, y, core, ix_r), (z, y, core, ix_l)
 
     own = pltpu.make_async_copy(mixed_ref, hm.at[me], local_sem.at[0])
-    load_wo = pltpu.make_async_copy(wo_ref, wo_v, local_sem.at[1])
+    per = own_wo_ref.shape[0]
+
+    def wo_rows(k):
+        return pl.ds(pl.multiple_of(lax.rem(me + k, n) * per, per), per)
+
+    load_wo = [pltpu.make_async_copy(own_wo_ref, wo_v.at[wo_rows(0)], local_sem.at[1])] + [
+        pltpu.make_async_copy(wo_ref.at[wo_rows(k)], wo_v.at[wo_rows(k)], local_sem.at[3 + k])
+        for k in range(1, n)
+    ]
     load_st = pltpu.make_async_copy(stream_ref, st, local_sem.at[2])
     load_w = pltpu.make_async_copy(w_ref, w_v, local_sem.at[3])
     own.start()
-    load_wo.start()
+    for c in load_wo:
+        c.start()
     load_st.start()
     load_w.start()
     barrier = pltpu.get_barrier_semaphore()
     pl.semaphore_signal(barrier, inc=1, device_id=right, device_id_type=MESH)
     pl.semaphore_signal(barrier, inc=1, device_id=left, device_id_type=MESH)
-    pl.semaphore_wait(barrier, 2)
+    partner = (z, y, 1 - core, me)
+    pl.semaphore_signal(barrier, inc=1, device_id=partner, device_id_type=MESH)
+    plane = PlaneGather(shard_ref, down_v, gather_sems)
+    for axis in ("z", "y"):
+        for k in (1, -1):
+            pl.semaphore_signal(
+                barrier, inc=1, device_id=plane.chip_at(axis, k), device_id_type=MESH)
+    pl.semaphore_wait(barrier, 7)
     own.wait()
 
     def piece(slot, r, part):
@@ -434,9 +692,12 @@
         fwd_left(i).start()
 
     send_own(0)
+    plane.start()
     pump(0)
     send_own(1)
-    load_wo.wait()
+    plane.near()
+    for c in load_wo:
+        c.wait()
     load_st.wait()
 
     dh = d // 2
@@ -469,6 +730,8 @@
         if i < n - 2:
             send_own(i + 2)
         if i == 0:
+            plane.far()
+            plane.column(0)
             load_w.wait()
         factor = lax.rsqrt(squares / d + EPS)
         normed[...] = (resid[...] * factor * gain_ref[...].astype(F32)).astype(BF16)
@@ -481,11 +744,17 @@
             return 0
 
         lax.fori_loop(0, units // 128, gate_up, 0)
+        if i == 0:
+            for ja in (-1, 1, 2):
+                plane.column(ja)
+            for ja in PlaneGather.OFFS:
+                plane.column_far(ja)
+            plane.finish()
         target = (s2, s1, s3, resid)[i]
 
         def down(j, _):
             cols = pl.ds(pl.multiple_of(j * 256, 256), 256)
-            part = nt_dot(hidden[...], w_v[cols, 2 * units : 3 * units]).astype(BF16)
+            part = nt_dot(hidden[...], down_v[cols, :]).astype(BF16)
             if i < n - 1:
                 target[:, cols] = part
             else:
@@ -515,28 +784,30 @@
     for i in range(n):
         fwd_right(i).wait_send()
         fwd_left(i).wait_send()
+    plane.drain()
     to_r_a.wait_send()
     to_l_b.wait_send()
     to_r.wait_send()
     to_l.wait_send()
 
 
-def feed_forward(mixed, stream, wo, w, gain):
+def feed_forward(mixed, stream, own_wo, wo, w, shard, gain):
     rows, d = stream.shape
-    units = w.shape[1] // 3
+    units = shard.shape[1]
     vm = pl.BlockSpec(memory_space=pltpu.VMEM)
     hbm = pl.BlockSpec(memory_space=pl.ANY)
     dma = pltpu.SemaphoreType.DMA
     return pl.pallas_call(
         ffn_kernel,
         out_shape=jax.ShapeDtypeStruct((GR, d), BF16),
-        in_specs=[hbm, hbm, hbm, hbm, vm],
+        in_specs=[hbm, hbm, hbm, hbm, hbm, vm, vm],
         out_specs=vm,
         scratch_shapes=[
             pltpu.VMEM((4, rows, mixed.shape[1]), BF16),
             pltpu.VMEM((rows, d), BF16),
             pltpu.VMEM(wo.shape, BF16),
             pltpu.VMEM(w.shape, BF16),
+            pltpu.VMEM((d, units), BF16),
             pltpu.VMEM((GR, d), F32),
             pltpu.VMEM((GR, d), BF16),
             pltpu.VMEM((GR, units), BF16),
@@ -547,15 +818,15 @@
             pltpu.VMEM((GR, d // 2), BF16),
             pltpu.VMEM((GR, d), BF16),
             pltpu.VMEM((GR, d), BF16),
-            dma((4,)), dma((8,)), dma((8,)), dma((4,)), dma((4,)),
+            dma((8,)), dma((8,)), dma((8,)), dma((4,)), dma((4,)),
             dma((8,)), dma((8,)), dma((4,)), dma((4,)), dma((4,)), dma((4,)),
-        ],
+        ] + plane_sems(),
         compiler_params=pltpu.CompilerParams(
             collective_id=1, has_side_effects=True, vmem_limit_bytes=60 * 2**20),
         cost_estimate=pl.CostEstimate(
             flops=26_000_000_000, bytes_accessed=32_000_000, transcendentals=0),
         name="feed_forward",
-    )(mixed, stream, wo, w, gain.reshape(1, -1))
+    )(mixed, stream, own_wo, wo, w, shard, gain.reshape(1, -1))
 
 
 def per_device(
@@ -566,13 +837,12 @@
     own_rows, units = gate_weight.shape
     pair = jnp.stack(
         [gate_weight.reshape(own_rows, -1, 128), up_weight.reshape(own_rows, -1, 128)], axis=2)
-    shard = jnp.concatenate([pair.reshape(own_rows, 2 * units), down_weight.T], axis=1)
-    weights = lax.all_gather(shard, SP, axis=0, tiled=True)
-    whole_out = lax.all_gather(output_weight, "tp", axis=0, tiled=True)
-    head_mixed = attention(
+    shard = pair.reshape(own_rows, 2 * units)
+    head_mixed, weights, whole_out = attention(
         queries, projected_keys, values, decay_gate_logits, decay_gate_bias, extra_log_decay,
-        document_index, output_gate, head_norm_gain)
-    return feed_forward(head_mixed, stream, whole_out, weights, feedforward_norm_gain)
+        document_index, output_gate, head_norm_gain, shard, output_weight)
+    return feed_forward(
+        head_mixed, stream, output_weight, whole_out, weights, down_weight.T, feedforward_norm_gain)
 
 
 def solution(mesh):

time: 266 us -> 172 us (0.65)
  waiting for transfers between devices: 127 us -> 0 us
  Pallas kernels: 117 us -> 154 us
  between operations: 13.6 us -> 0.08 us
  local copies, waits for them, and re-layouts: 7.18 us -> 14.3 us
    all_gather x2 -> x0, waiting for transfers between devices: 126 us -> none  [the longest x1 78.3 us: per_device(): weights = lax.all_gather(shard, SP, axis=0, tiled=True)]
    pallas_call x1, Pallas kernels: 32.1 us -> 59.7 us  [attention(): pl.pallas_call(attention_kernel, out_shape=(jax.ShapeDtypeStruct((rows, 2...]
    pallas_call x1, Pallas kernels: 85 us -> 94.2 us  [feed_forward(): pl.pallas_call(ffn_kernel, out_shape=jax.ShapeDtypeStruct((GR, d), BF16),...]
    unnamed x29 -> x15, local copies, waits for them, and re-layouts: 5.55 us -> 9.52 us
  transfers between devices with their start and end apart: 2 -> 0, of which waited for: 2 -> 0; matrix products, arithmetic and copies ran while one was open for 1% -> 0% of each run, Pallas kernels for 12% -> 0%
where the time goes in v4:
time: 172 us; the launch traced here: 170 us
  Pallas kernels  154 us (90%)
  local copies, waits for them, and re-layouts  14.3 us (8%)
    pallas_call x1, Pallas kernels, feed_forward(): pl.pallas_call(ffn_kernel, out_shape=jax.ShapeDtypeStruct((GR, d), BF16),...  94.2 us
    pallas_call x1, Pallas kernels, attention(): pl.pallas_call(attention_kernel, out_shape=(jax.ShapeDtypeStruct((rows, 2...  59.7 us
    unnamed x15, local copies, waits for them, and re-layouts  9.52 us

profile of v4, /device:TPU:6, one launch (start us, length us, event | category | flops | bytes accessed | tf_op | source)
XLA Modules:
  0.0 169.8 jit_solution(7025146521743329189)
XLA Ops:
  0.0 0.7 reshape.17.gain_ref
  0.7 0.7 convert_element_type.3
  1.4 1.3 reshape.19.gain_ref
  2.6 0.7 pad_maximum_fusion.1
  3.4 1.1 stack_reshape.6
  4.4 1.1 stack_reshape.7
  5.5 0.1 pad_maximum_fusion
  5.6 0.4 copy.22
  6.0 0.1 reshape.18.shard_ref
  6.1 0.2 copy.23.aux_ref
  6.4 0.0 copy-start
  6.4 1.2 copy-done
  7.6 0.0 copy-start.1
  7.6 1.2 copy-done.1
  8.8 0.0 copy-start.2
  8.8 1.0 copy-done.2
  9.9 0.0 copy-start.3
  9.9 1.0 copy-done.3
  10.9 0.0 copy-start.4
  10.9 1.0 copy-done.4
  11.9 0.0 copy-start.5
  11.9 0.7 copy-done.5
  12.6 59.7 %attention.1 = (bf16[1024,512]{1,0:T(8,128)(2,1)S(1)}, bf16[2048,2816]{1,0:T(8,128)(2,1)}, bf16[2048,2048]{1,0:T(8,128)(2,1)}) custom-call(bf16[1024,256]{1,0:T(8,128)(2,1)S(1)} %copy-done.2, bf16[1024,256]{1,0:T(8,128)(2,1)S(1)} %copy-done.3, bf16[1024,512]{1,0:T(8,128)(2,1)S(1)} %copy-done, bf16[1024,256]{1,0:T(8,128)(2,1)S(1)} %copy-done.4, ...), custom_call_target="tpu_custom_call" | custom-call | flops 3000000000 | bytes 8000000 | tf_op jit(solution)/shard_map/attention/pallas_call | solution.py:542
  72.3 0.0 copy-start.6
  72.3 1.0 copy-done.6
  73.3 94.2 %feed_forward.1 = bf16[256,2048]{1,0:T(8,128)(2,1)} custom-call(bf16[1024,512]{1,0:T(8,128)(2,1)} %copy-done.6, bf16[1024,2048]{1,0:T(8,128)(2,1)} %stream_ref.1, bf16[512,2048]{1,0:T(8,128)(2,1)} %own_wo_ref.1, bf16[2048,2048]{1,0:T(8,128)(2,1)} %get-tuple-element.9.wo_ref, bf16[2048,2816]{1,0:T(8,128)(2,1)} %get-tuple-element.10.w_ref, ...), custom_call_target="tpu_custom_call" | custom-call | flops 25999998976 | bytes 32000000 | tf_op jit(solution)/shard_map/feed_forward/pallas_call | solution.py:800
  167.5 2.3 %copy.25 = bf16[256,2048]{1,0:T(8,128)(2,1)} copy(bf16[256,2048]{1,0:T(8,128)(2,1)} %feed_forward.1) | data formatting | bytes 2097152
  (1 shorter events, 0.0 us)
Async XLA Ops:
  6.4 1.2 copy-start
  7.6 1.2 copy-start.1
  8.8 1.0 copy-start.2
  9.9 1.0 copy-start.3
  10.9 1.0 copy-start.4
  11.9 0.7 copy-start.5
  72.3 1.0 copy-start.6

commit v5 on v4

--- a/solution.py
+++ b/solution.py
@@ -181,12 +181,12 @@
 class RowGather:
     SEMS = (4, 4, 3, 3)
 
-    def __init__(self, src, dst, sems):
-        self.src, self.dst = src, dst
+    def __init__(self, rows, dst, sems):
+        self.dst = dst
         self.send, self.recv, self.core_send, self.core_recv = sems
         self.z, self.y = lax.axis_index("sp_0"), lax.axis_index("sp_1")
         self.core, self.x = lax.axis_index("sp_2"), lax.axis_index("tp")
-        self.rows = src.shape[0]
+        self.rows = rows
 
     def piece(self, k, core, sub=None):
         size = self.rows // 2
@@ -206,8 +206,7 @@
             src = dst
         else:
             dst = self.piece(0, self.core)
-            size = self.rows // 2
-            src = self.src.at[pl.ds(pl.multiple_of(self.core * size, 16), size)]
+            src = dst
         return remote_copy(src, dst, self.send.at[k], self.recv.at[k], self.side(way))
 
     def landing(self, way, forward):
@@ -250,45 +249,108 @@
     return [pltpu.SemaphoreType.DMA((k,)) for k in PlaneGather.SEMS]
 
 
-def attention_kernel(
-    q_ref, k_ref, v_ref, lg_ref, bias_ref, aux_ref, docrow_ref, gate_ref, gain_ref, shard_ref, wo_ref,
-    mixed_ref, whole_ref, whole_wo_ref,
-    cum_ref, glob_ref, blk_ref, states_ref, before_ref, run_ref, local_ref,
+def layer_kernel(
+    q_in, k_in, v_in, lg_in, gate_in, wo_in, stream_in, wg_in, wu_in, wd_in,
+    bias_ref, rows_ref, gain_ref, ff_gain_ref,
+    out_ref,
+    q_ref, k_ref, v_ref, lg_ref, gate_ref, aux_ref, wg_ref, wu_ref, shard_ref, wd_ref,
+    cum_ref, blk_ref, off_ref, states_ref, before_ref, run_ref, local_ref,
     own_t, own_e, part_t, part_e, chip_t, chip_e, recv_t, recv_e, mine_c, send_c, part_c, sum_ref,
-    core_send, core_recv, t_send, t_recv, e_send, e_recv, *gather_sems,
+    hm, st, wo_v, w_v, down_v, resid, normed, hidden, s2, s1, s3, ra, rb, rl, rr,
+    local_sem, core_send, core_recv, t_send, t_recv, e_send, e_recv,
+    own_rs, own_ls, fwd_rs, fwd_ls, left_in, right_in, opp_l, opp_r, rs_send, rs_recv,
+    *gather_sems,
 ):
     rows = q_ref.shape[0]
     blocks = rows // BL
     groups = rows // GR
     per = GR // BL
     z, y = lax.axis_index("sp_0"), lax.axis_index("sp_1")
-    core, x = lax.axis_index("sp_2"), lax.axis_index("tp")
+    core, me = lax.axis_index("sp_2"), lax.axis_index("tp")
     chip = z * NY + y
     scale = DK ** (-0.5)
+    n = 4
+    q_rows = GR
+    half = q_rows // 2
+    d = out_ref.shape[1]
+    units = hidden.shape[1]
+    ix_r, ix_l = lax.rem(me + 1, n), lax.rem(me + n - 1, n)
+    right, left = (z, y, core, ix_r), (z, y, core, ix_l)
+    partner = (z, y, 1 - core, me)
+    order = (2, 1, 3, 0)
+
+    def quarter_of(owner, offset):
+        return lax.rem(owner + offset, n)
 
     def chip_peer(k):
         other = lax.rem(chip + k, NCHIP)
-        return other, (other // NY, lax.rem(other, NY), core, x)
-
-    partner = (z, y, 1 - core, x)
+        return other, (other // NY, lax.rem(other, NY), core, me)
+
+    wo_own = wo_in.shape[0]
+    loads = {
+        name: pltpu.make_async_copy(src, dst, local_sem.at[i])
+        for i, (name, src, dst) in enumerate((
+            ("wg", wg_in, wg_ref), ("wu", wu_in, wu_ref), ("wd", wd_in, wd_ref),
+            ("wo", wo_in, wo_v.at[pl.ds(pl.multiple_of(me * wo_own, wo_own), wo_own)]),
+            ("lg", lg_in, lg_ref), ("k", k_in, k_ref), ("v", v_in, v_ref), ("q", q_in, q_ref),
+            ("gate", gate_in, gate_ref),
+        ))
+    }
+    for copy in loads.values():
+        copy.start()
+
+    def load_stream(i):
+        at = pl.multiple_of(quarter_of(me, order[i]) * q_rows, q_rows)
+        return pltpu.make_async_copy(
+            stream_in.at[pl.ds(at, q_rows)], st.at[i % 2], local_sem.at[9 + i])
+
+    load_stream(0).start()
+    load_stream(1).start()
 
     recv_t[pl.ds(chip, 1)] = jnp.zeros((1, DV, DK), BF16)
 
     barrier = pltpu.get_barrier_semaphore()
     pl.semaphore_signal(barrier, inc=1, device_id=partner, device_id_type=MESH)
+    pl.semaphore_signal(barrier, inc=1, device_id=right, device_id_type=MESH)
+    pl.semaphore_signal(barrier, inc=1, device_id=left, device_id_type=MESH)
     for k in range(1, NCHIP):
         pl.semaphore_signal(barrier, inc=1, device_id=chip_peer(k)[1], device_id_type=MESH)
-    for k in (1, 3):
-        pl.semaphore_signal(
-            barrier, inc=1, device_id=(z, y, core, lax.rem(x + k, 4)), device_id_type=MESH)
+
+    loads["wg"].wait()
+    loads["wu"].wait()
+    for j in range(units // 128):
+        shard_ref[:, j * 256 : j * 256 + 128] = wg_ref[:, j * 128 : (j + 1) * 128]
+        shard_ref[:, j * 256 + 128 : (j + 1) * 256] = wu_ref[:, j * 128 : (j + 1) * 128]
+    loads["wd"].wait()
+    loads["wo"].wait()
+
     pl.semaphore_wait(barrier, NCHIP + 2)
-    plane = PlaneGather(shard_ref, whole_ref, gather_sems[:5])
-    ring = RowGather(wo_ref, whole_wo_ref, gather_sems[5:])
-    plane.start()
+    g1 = PlaneGather(shard_ref, w_v, gather_sems[:5])
+    g2 = PlaneGather(wd_ref, down_v, gather_sems[5:10])
+    ring = RowGather(wo_own, wo_v, gather_sems[10:])
     ring.start()
+    g1.start()
+    g2.start()
 
     ri = lax.broadcasted_iota(jnp.int32, (GR, GR), 0)
     ci = lax.broadcasted_iota(jnp.int32, (GR, GR), 1)
+
+    def columns(g, _):
+        at = pl.multiple_of(g * GR, GR)
+        for j in range(3):
+            row = rows_ref[pl.ds(j * groups + g, 1), :]
+            col = jnp.sum(jnp.where(ri == ci, row, 0.0), axis=1, keepdims=True)
+            aux_ref[pl.ds(at, GR), j : j + 1] = col
+        return 0
+
+    lax.fori_loop(0, groups, columns, 0)
+    loads["lg"].wait()
+    loads["k"].wait()
+    loads["v"].wait()
+    run_ref[...] = jnp.zeros_like(run_ref)
+
+    def doc_at(r):
+        return aux_ref[pl.ds(r, 1), 2:3]
 
     def first(g, base):
         at = pl.multiple_of(g * GR, GR)
@@ -307,13 +369,11 @@
         cum_ref[pl.ds(at, GR), :] = cum
         cum3 = cum.reshape(per, BL, 2 * DK)
         ends = cum3[:, BL - 1 : BL, :]
-        off, offs = base, []
+        off = base
         for b in range(per):
-            offs.append(off)
+            off_ref[pl.ds(g * per + b, 1)] = off[None]
             blk_ref[pl.ds(g * per + b, 1)] = ends[b : b + 1]
             off = off + ends[b]
-        for b in range(per):
-            glob_ref[pl.ds(pl.multiple_of(at + b * BL, BL), BL), :] = cum3[b] + offs[b]
         doc = aux_ref[pl.ds(at, GR), 2:3].reshape(per, BL, 1)
         tail_mask = jnp.where(doc == doc[:, BL - 1 : BL], 1.0, 0.0)
         head_mask = jnp.where(doc == doc[:, 0:1], 1.0, 0.0)
@@ -321,37 +381,33 @@
         tail = (kf * jnp.exp(ends - cum3) * tail_mask).astype(BF16)
         head = (kf * jnp.exp(cum3) * head_mask).astype(BF16)
         for b in range(per):
+            start = at + b * BL
+            keep = jnp.where(doc_at(jnp.maximum(start - 1, 0)) == doc_at(start + BL - 1), 1.0, 0.0)
+            decay = jnp.exp(ends[b]) * keep
             for h in range(2):
-                keys = jnp.concatenate(
-                    [tail[b][:, h * DK : (h + 1) * DK], head[b][:, h * DK : (h + 1) * DK]], axis=1
-                )
-                vals = v_ref[pl.ds(pl.multiple_of(at + b * BL, BL), BL), h * DV : (h + 1) * DV]
-                states_ref[pl.ds((g * per + b) * 2 + h, 1)] = tn_dot(vals, keys)[None]
+                c = slice(h * DK, (h + 1) * DK)
+                keys = jnp.concatenate([tail[b][:, c], head[b][:, c]], axis=1)
+                vals = v_ref[pl.ds(pl.multiple_of(start, BL), BL), h * DV : (h + 1) * DV]
+                both = tn_dot(vals, keys)
+                slot = (g * per + b) * 2 + h
+                states_ref[pl.ds(slot, 1)] = both[None, :, DK:]
+                fw = run_ref[h, :, :DK]
+                before_ref[pl.ds(slot, 1), :, :DK] = fw.astype(BF16)[None]
+                run_ref[h, :, :DK] = fw * decay[:, c] + both[:, :DK]
         return off
 
     total = lax.fori_loop(0, groups, first, jnp.zeros((1, 2 * DK), F32))
     sum_ref[...] = total
 
-    run_ref[...] = jnp.zeros_like(run_ref)
-
-    def doc_at(r):
-        return aux_ref[pl.ds(r, 1), 2:3]
-
     def step(b, _):
-        lo = jnp.maximum(b * BL - 1, 0)
-        keep = jnp.where(doc_at(lo) == doc_at(b * BL + BL - 1), 1.0, 0.0)
-        decay = jnp.exp(blk_ref[pl.ds(b, 1)][0]) * keep
         r = blocks - 1 - b
         hi = jnp.minimum(r * BL + BL, rows - 1)
-        keep_b = jnp.where(doc_at(hi) == doc_at(r * BL), 1.0, 0.0)
-        decay_b = jnp.exp(blk_ref[pl.ds(r, 1)][0]) * keep_b
+        keep = jnp.where(doc_at(hi) == doc_at(r * BL), 1.0, 0.0)
+        decay = jnp.exp(blk_ref[pl.ds(r, 1)][0]) * keep
         for h in range(2):
-            fw = run_ref[h, :, :DK]
-            before_ref[pl.ds(b * 2 + h, 1), :, :DK] = fw.astype(BF16)[None]
-            run_ref[h, :, :DK] = fw * decay[:, h * DK : (h + 1) * DK] + states_ref[b * 2 + h, :, :DK]
             bw = run_ref[h, :, DK:]
             before_ref[pl.ds(r * 2 + h, 1), :, DK:] = bw.astype(BF16)[None]
-            run_ref[h, :, DK:] = bw * decay_b[:, h * DK : (h + 1) * DK] + states_ref[r * 2 + h, :, DK:]
+            run_ref[h, :, DK:] = bw * decay[:, h * DK : (h + 1) * DK] + states_ref[r * 2 + h]
         return 0
 
     lax.fori_loop(0, blocks, step, 0)
@@ -405,13 +461,14 @@
             device_id=target, device_id_type=MESH))
     for s in sends:
         s.start()
-    plane.near()
+    g1.near()
+    loads["q"].wait()
 
     def inside(g, _):
         at = pl.multiple_of(g * GR, GR)
         same_block = (ri & (GR - BL)) == (ci & (GR - BL))
         doc = aux_ref[pl.ds(at, GR), 2:3]
-        same = same_block & (doc == docrow_ref[pl.ds(g, 1), :])
+        same = same_block & (doc == rows_ref[pl.ds(2 * groups + g, 1), :])
         below = same & (ci <= ri)
         above = same & (ci >= ri)
         cum3 = cum_ref[pl.ds(at, GR), :].reshape(per, BL, 2 * DK)
@@ -450,15 +507,13 @@
         return 0
 
     lax.fori_loop(0, groups // 2, inside, 0)
-    plane.far()
-    plane.column(0)
+    g2.near()
     lax.fori_loop(groups // 2, groups, inside, 0)
+    g1.far()
     ring.near()
-    plane.column(-1)
 
     for s in sends:
         s.wait()
-    plane.column(1)
     run_ref[0] = jnp.zeros_like(run_ref[0])
 
     def earlier(j, _):
@@ -500,12 +555,15 @@
     enter_b = jnp.where(is0, e1[1:2], after_doc)[:, 0:1]
     swap_c.wait()
 
-    def last(g, _):
+    loads["gate"].wait()
+
+    def last(g):
         at = pl.multiple_of(g * GR, GR)
         doc = aux_ref[pl.ds(at, GR), 2:3]
         hit_f = jnp.where(doc == enter_f, 1.0, 0.0)
         hit_b = jnp.where(doc == enter_b, 1.0, 0.0)
-        glob = glob_ref[pl.ds(at, GR), :]
+        glob = cum_ref[pl.ds(at, GR), :].reshape(per, BL, 2 * DK) + off_ref[pl.ds(g * per, per)]
+        glob = glob.reshape(GR, 2 * DK)
         qf = q_ref[pl.ds(at, GR), :].astype(F32) * scale
         q_fwd = (qf * jnp.exp(glob) * hit_f).astype(BF16)
         q_bwd = (qf * jnp.exp(sum_ref[...] - glob) * hit_b).astype(BF16)
@@ -517,117 +575,14 @@
             out = local_ref[pl.ds(at, GR), h * DV : (h + 1) * DV] + nt_dot(both, carry)
             out = out * lax.rsqrt(jnp.mean(out * out, axis=-1, keepdims=True) + EPS) * gain
             u = gate_ref[pl.ds(at, GR), h * DV : (h + 1) * DV].astype(F32)
-            mixed_ref[pl.ds(at, GR), h * DV : (h + 1) * DV] = (
+            hm[me, pl.ds(at, GR), h * DV : (h + 1) * DV] = (
                 out * (u / (1.0 + jnp.exp(-u)))).astype(BF16)
+
+    def three(i, _):
+        last(quarter_of(me, i + i // 2))
         return 0
 
-    lax.fori_loop(0, groups, last, 0)
-    plane.column(2)
-    for ja in PlaneGather.OFFS:
-        plane.column_far(ja)
-    ring.far()
-    plane.finish()
-    plane.drain()
-    ring.finish()
-
-
-def attention(q, k, v, lg, bias, extra, doc, gate, gain, shard, wo):
-    rows = q.shape[0]
-    doc_f = doc.astype(F32)
-    aux = jnp.concatenate([extra, doc_f[:, None]], axis=1)
-    docrow = doc_f.reshape(rows // GR, GR)
-    vm = pl.BlockSpec(memory_space=pltpu.VMEM)
-    hbm = pl.BlockSpec(memory_space=pl.ANY)
-    blocks = rows // BL
-    return pl.pallas_call(
-        attention_kernel,
-        out_shape=(
-            jax.ShapeDtypeStruct((rows, 2 * DV), BF16),
-            jax.ShapeDtypeStruct((shard.shape[0] * 2 * NCHIP, shard.shape[1]), BF16),
-            jax.ShapeDtypeStruct((wo.shape[0] * 4, wo.shape[1]), BF16),
-        ),
-        in_specs=[vm] * 10 + [hbm],
-        out_specs=(vm, hbm, hbm),
-        scratch_shapes=[
-            pltpu.VMEM((rows, 2 * DK), F32),
-            pltpu.VMEM((rows, 2 * DK), F32),
-            pltpu.VMEM((blocks, 1, 2 * DK), F32),
-            pltpu.VMEM((blocks * 2, DV, 2 * DK), F32),
-            pltpu.VMEM((blocks * 2, DV, 2 * DK), BF16),
-            pltpu.VMEM((2, DV, 2 * DK), F32),
-            pltpu.VMEM((rows, 2 * DV), F32),
-            pltpu.VMEM((2, 2 * DV, DK), BF16),
-            pltpu.VMEM((2, 8, DK), F32),
-            pltpu.VMEM((2 * DV, DK), BF16),
-            pltpu.VMEM((8, DK), F32),
-            pltpu.VMEM((2, DV, DK), BF16),
-            pltpu.VMEM((8, DK), F32),
-            pltpu.VMEM((NCHIP, DV, DK), BF16),
-            pltpu.VMEM((NCHIP, 8, DK), F32),
-            pltpu.VMEM((DV, 2 * DK), BF16),
-            pltpu.VMEM((DV, 2 * DK), BF16),
-            pltpu.VMEM((DV, 2 * DK), BF16),
-            pltpu.VMEM((1, 2 * DK), F32),
-            pltpu.SemaphoreType.DMA((3,)),
-            pltpu.SemaphoreType.DMA((3,)),
-            pltpu.SemaphoreType.DMA((NCHIP,)),
-            pltpu.SemaphoreType.DMA((NCHIP,)),
-            pltpu.SemaphoreType.DMA((NCHIP,)),
-            pltpu.SemaphoreType.DMA((NCHIP,)),
-        ] + plane_sems() + [pltpu.SemaphoreType.DMA((k,)) for k in RowGather.SEMS],
-        compiler_params=pltpu.CompilerParams(
-            collective_id=0, has_side_effects=True, vmem_limit_bytes=48 * 2**20),
-        cost_estimate=pl.CostEstimate(flops=3_000_000_000, bytes_accessed=8_000_000, transcendentals=0),
-        name="attention",
-    )(q, k, v, lg, bias.reshape(1, -1), aux, docrow, gate, gain.reshape(1, -1), shard, wo)
-
-
-def ffn_kernel(
-    mixed_ref, stream_ref, own_wo_ref, wo_ref, w_ref, shard_ref, gain_ref,
-    out_ref,
-    hm, st, wo_v, w_v, down_v, resid, normed, hidden, s2, s1, s3, ra, rb, rl, rr,
-    local_sem, own_rs, own_ls, fwd_rs, fwd_ls, left_in, right_in, opp_l, opp_r,
-    rs_send, rs_recv, *gather_sems,
-):
-    z, y, core = lax.axis_index("sp_0"), lax.axis_index("sp_1"), lax.axis_index("sp_2")
-    me = lax.axis_index("tp")
-    n = 4
-    q_rows = GR
-    half = q_rows // 2
-    d = out_ref.shape[1]
-    units = hidden.shape[1]
-    ix_r, ix_l = lax.rem(me + 1, n), lax.rem(me + n - 1, n)
-    right, left = (z, y, core, ix_r), (z, y, core, ix_l)
-
-    own = pltpu.make_async_copy(mixed_ref, hm.at[me], local_sem.at[0])
-    per = own_wo_ref.shape[0]
-
-    def wo_rows(k):
-        return pl.ds(pl.multiple_of(lax.rem(me + k, n) * per, per), per)
-
-    load_wo = [pltpu.make_async_copy(own_wo_ref, wo_v.at[wo_rows(0)], local_sem.at[1])] + [
-        pltpu.make_async_copy(wo_ref.at[wo_rows(k)], wo_v.at[wo_rows(k)], local_sem.at[3 + k])
-        for k in range(1, n)
-    ]
-    load_st = pltpu.make_async_copy(stream_ref, st, local_sem.at[2])
-    load_w = pltpu.make_async_copy(w_ref, w_v, local_sem.at[3])
-    own.start()
-    for c in load_wo:
-        c.start()
-    load_st.start()
-    load_w.start()
-    barrier = pltpu.get_barrier_semaphore()
-    pl.semaphore_signal(barrier, inc=1, device_id=right, device_id_type=MESH)
-    pl.semaphore_signal(barrier, inc=1, device_id=left, device_id_type=MESH)
-    partner = (z, y, 1 - core, me)
-    pl.semaphore_signal(barrier, inc=1, device_id=partner, device_id_type=MESH)
-    plane = PlaneGather(shard_ref, down_v, gather_sems)
-    for axis in ("z", "y"):
-        for k in (1, -1):
-            pl.semaphore_signal(
-                barrier, inc=1, device_id=plane.chip_at(axis, k), device_id_type=MESH)
-    pl.semaphore_wait(barrier, 7)
-    own.wait()
+    lax.fori_loop(0, 3, three, 0)
 
     def piece(slot, r, part):
         return hm.at[slot, pl.ds(pl.multiple_of(r * q_rows + part * half, half), half)]
@@ -635,11 +590,6 @@
     def remote(ref, send, recv, target, dst=None):
         return pltpu.make_async_remote_copy(
             ref, ref if dst is None else dst, send, recv, device_id=target, device_id_type=MESH)
-
-    order = (2, 1, 3, 0)
-
-    def quarter_of(owner, offset):
-        return lax.rem(owner + offset, n)
 
     def wire(slot, quarter, part, send, recv, target):
         return remote(piece(slot, quarter, part), send, recv, target)
@@ -692,13 +642,17 @@
         fwd_left(i).start()
 
     send_own(0)
-    plane.start()
+    last(quarter_of(me, 2))
+    g1.column(0)
     pump(0)
     send_own(1)
-    plane.near()
-    for c in load_wo:
-        c.wait()
-    load_st.wait()
+    for ja in (-1, 1):
+        g1.column(ja)
+    g2.far()
+    g2.column(0)
+    ring.far()
+    g1.column(2)
+    ring.finish()
 
     dh = d // 2
     to_r_a = remote(s2.at[:, pl.ds(0, dh)], rs_send.at[0], rs_recv.at[0], right, ra)
@@ -716,9 +670,11 @@
         came_opp_l(i).wait_recv()
         came_opp_r(i).wait_recv()
 
+        load_stream(i).wait()
+
         def project(j, total):
             cols = pl.ds(pl.multiple_of(j * 512, 512), 512)
-            acc = st[rows, cols].astype(F32)
+            acc = st[i % 2, :, cols].astype(F32)
             for k in range(n):
                 acc = acc + nn_dot(hm[k, rows, :], wo_v[k * 512 : (k + 1) * 512, cols])
             resid[:, cols] = acc
@@ -729,12 +685,15 @@
             pump(i + 1)
         if i < n - 2:
             send_own(i + 2)
+            load_stream(i + 2).start()
         if i == 0:
-            plane.far()
-            plane.column(0)
-            load_w.wait()
+            for ja in (-1, 1, 2):
+                g2.column(ja)
+            for ja in PlaneGather.OFFS:
+                g1.column_far(ja)
+            g1.finish()
         factor = lax.rsqrt(squares / d + EPS)
-        normed[...] = (resid[...] * factor * gain_ref[...].astype(F32)).astype(BF16)
+        normed[...] = (resid[...] * factor * ff_gain_ref[...].astype(F32)).astype(BF16)
 
         def gate_up(j, _):
             both = nn_dot(normed[...], w_v[:, pl.ds(pl.multiple_of(j * 256, 256), 256)])
@@ -745,11 +704,9 @@
 
         lax.fori_loop(0, units // 128, gate_up, 0)
         if i == 0:
-            for ja in (-1, 1, 2):
-                plane.column(ja)
             for ja in PlaneGather.OFFS:
-                plane.column_far(ja)
-            plane.finish()
+                g2.column_far(ja)
+            g2.finish()
         target = (s2, s1, s3, resid)[i]
 
         def down(j, _):
@@ -784,49 +741,65 @@
     for i in range(n):
         fwd_right(i).wait_send()
         fwd_left(i).wait_send()
-    plane.drain()
+    g1.drain()
+    g2.drain()
     to_r_a.wait_send()
     to_l_b.wait_send()
     to_r.wait_send()
     to_l.wait_send()
 
 
-def feed_forward(mixed, stream, own_wo, wo, w, shard, gain):
+def layer(q, k, v, lg, bias, extra, doc, gate, gain, wo, stream, ff_gain, wg, wu, wd):
     rows, d = stream.shape
-    units = shard.shape[1]
+    units = wg.shape[1]
+    groups = rows // GR
+    table = jnp.concatenate([extra.T, doc.astype(F32)[None]], axis=0).reshape(3 * groups, GR)
     vm = pl.BlockSpec(memory_space=pltpu.VMEM)
     hbm = pl.BlockSpec(memory_space=pl.ANY)
+    blocks = rows // BL
     dma = pltpu.SemaphoreType.DMA
+
+    def buf(*shape, dtype=BF16):
+        return pltpu.VMEM(shape, dtype)
+
     return pl.pallas_call(
-        ffn_kernel,
+        layer_kernel,
         out_shape=jax.ShapeDtypeStruct((GR, d), BF16),
-        in_specs=[hbm, hbm, hbm, hbm, hbm, vm, vm],
+        in_specs=[hbm] * 10 + [vm] * 4,
         out_specs=vm,
         scratch_shapes=[
-            pltpu.VMEM((4, rows, mixed.shape[1]), BF16),
-            pltpu.VMEM((rows, d), BF16),
-            pltpu.VMEM(wo.shape, BF16),
-            pltpu.VMEM(w.shape, BF16),
-            pltpu.VMEM((d, units), BF16),
-            pltpu.VMEM((GR, d), F32),
-            pltpu.VMEM((GR, d), BF16),
-            pltpu.VMEM((GR, units), BF16),
-            pltpu.VMEM((GR, d), BF16),
-            pltpu.VMEM((GR, d), BF16),
-            pltpu.VMEM((GR, d), BF16),
-            pltpu.VMEM((GR, d // 2), BF16),
-            pltpu.VMEM((GR, d // 2), BF16),
-            pltpu.VMEM((GR, d), BF16),
-            pltpu.VMEM((GR, d), BF16),
-            dma((8,)), dma((8,)), dma((8,)), dma((4,)), dma((4,)),
+            buf(rows, 2 * DK), buf(rows, 2 * DK), buf(rows, 2 * DV), buf(rows, 2 * DK),
+            buf(rows, 2 * DV), buf(rows, 3, dtype=F32),
+            buf(*wg.shape), buf(*wu.shape), buf(wg.shape[0], 2 * units), buf(*wd.shape),
+            buf(rows, 2 * DK, dtype=F32),
+            buf(blocks, 1, 2 * DK, dtype=F32),
+            buf(blocks, 1, 2 * DK, dtype=F32),
+            buf(blocks * 2, DV, DK, dtype=F32),
+            buf(blocks * 2, DV, 2 * DK),
+            buf(2, DV, 2 * DK, dtype=F32),
+            buf(rows, 2 * DV, dtype=F32),
+            buf(2, 2 * DV, DK), buf(2, 8, DK, dtype=F32),
+            buf(2 * DV, DK), buf(8, DK, dtype=F32),
+            buf(2, DV, DK), buf(8, DK, dtype=F32),
+            buf(NCHIP, DV, DK), buf(NCHIP, 8, DK, dtype=F32),
+            buf(DV, 2 * DK), buf(DV, 2 * DK), buf(DV, 2 * DK),
+            buf(1, 2 * DK, dtype=F32),
+            buf(4, rows, 2 * DV), buf(2, GR, d), buf(4 * wo.shape[0], d),
+            buf(2 * NCHIP * wg.shape[0], 2 * units), buf(2 * NCHIP * wd.shape[0], units),
+            buf(GR, d, dtype=F32), buf(GR, d), buf(GR, units),
+            buf(GR, d), buf(GR, d), buf(GR, d), buf(GR, d // 2), buf(GR, d // 2), buf(GR, d), buf(GR, d),
+            dma((13,)), dma((3,)), dma((3,)),
+            dma((NCHIP,)), dma((NCHIP,)), dma((NCHIP,)), dma((NCHIP,)),
+            dma((8,)), dma((8,)), dma((4,)), dma((4,)),
             dma((8,)), dma((8,)), dma((4,)), dma((4,)), dma((4,)), dma((4,)),
-        ] + plane_sems(),
+        ] + plane_sems() + plane_sems() + [dma((k,)) for k in RowGather.SEMS],
         compiler_params=pltpu.CompilerParams(
-            collective_id=1, has_side_effects=True, vmem_limit_bytes=60 * 2**20),
+            collective_id=0, has_side_effects=True, vmem_limit_bytes=67_043_328),
         cost_estimate=pl.CostEstimate(
-            flops=26_000_000_000, bytes_accessed=32_000_000, transcendentals=0),
-        name="feed_forward",
-    )(mixed, stream, own_wo, wo, w, shard, gain.reshape(1, -1))
+            flops=29_000_000_000, bytes_accessed=16_000_000, transcendentals=0),
+        name="layer",
+    )(q, k, v, lg, gate, wo, stream, wg, wu, wd,
+      bias.reshape(1, -1), table, gain.reshape(1, -1), ff_gain.reshape(1, -1))
 
 
 def per_device(
@@ -834,15 +807,10 @@
     document_index, output_gate, head_norm_gain, output_weight, feedforward_norm_gain,
     gate_weight, up_weight, down_weight,
 ):
-    own_rows, units = gate_weight.shape
-    pair = jnp.stack(
-        [gate_weight.reshape(own_rows, -1, 128), up_weight.reshape(own_rows, -1, 128)], axis=2)
-    shard = pair.reshape(own_rows, 2 * units)
-    head_mixed, weights, whole_out = attention(
+    return layer(
         queries, projected_keys, values, decay_gate_logits, decay_gate_bias, extra_log_decay,
-        document_index, output_gate, head_norm_gain, shard, output_weight)
-    return feed_forward(
-        head_mixed, stream, output_weight, whole_out, weights, down_weight.T, feedforward_norm_gain)
+        document_index, output_gate, head_norm_gain, output_weight, stream,
+        feedforward_norm_gain, gate_weight, up_weight, down_weight.T)
 
 
 def solution(mesh):

time: 172 us -> 155 us (0.901)
  local copies, waits for them, and re-layouts: 14.3 us -> 5.45 us
  Pallas kernels: 154 us -> 146 us
    pallas_call x2 -> x1, Pallas kernels: 154 us -> 146 us  [layer(): pl.pallas_call(layer_kernel, out_shape=jax.ShapeDtypeStruct((GR, d), BF16...]
    unnamed x15 -> x1, local copies, waits for them, and re-layouts: 9.52 us -> 2.3 us
    another operation x3 -> x0, local copies, waits for them, and re-layouts: 2.49 us -> none  [per_device(): jnp.stack([gate_weight.reshape(own_rows, -1, 128), up_weight.reshape(own_...]
where the time goes in v5:
time: 155 us; the launch traced here: 153 us
  Pallas kernels  146 us (94%)
  local copies, waits for them, and re-layouts  5.45 us (4%)
    pallas_call x1, Pallas kernels, layer(): pl.pallas_call(layer_kernel, out_shape=jax.ShapeDtypeStruct((GR, d), BF16...  146 us

profile of v5, /device:TPU:6, one launch (start us, length us, event | category | flops | bytes accessed | tf_op | source)
XLA Modules:
  0.0 153.2 jit_solution(1559861879393369280)
XLA Ops:
  0.0 1.2 reshape.14.gain_ref
  1.2 0.7 convert_element_type.3
  1.9 1.3 reshape.15.ff_gain_ref
  3.2 0.7 pad_maximum_fusion
  3.9 0.6 reshape.13.rows_ref
  4.5 146.3 %layer.1 = bf16[256,2048]{1,0:T(8,128)(2,1)} custom-call(bf16[1024,256]{1,0:T(8,128)(2,1)} %q_in.1, bf16[1024,256]{1,0:T(8,128)(2,1)} %k_in.1, bf16[1024,512]{1,0:T(8,128)(2,1)} %v_in.1, bf16[1024,256]{1,0:T(8,128)(2,1)} %lg_in.1, bf16[1024,512]{1,0:T(8,128)(2,1)} %gate_in.1, bf16[512,2048]{1,0:T(8,128)(2,1)} %wo_in.1, bf16[1024,2048]{1,0:T(8,128)(2,1)} %stream_in.1, ...), custom_call_target="tpu_custom_call" | custom-call | flops 28999999488 | bytes 16000000 | tf_op jit(solution)/shard_map/layer/pallas_call | solution.py:765
  150.9 2.3 %copy.17 = bf16[256,2048]{1,0:T(8,128)(2,1)} copy(bf16[256,2048]{1,0:T(8,128)(2,1)} %layer.1) | data formatting | bytes 2097152

commit v6 on v5

--- a/solution.py
+++ b/solution.py
@@ -225,9 +225,12 @@
             self.hop(way, False).start()
 
     def near(self):
-        for i, way in enumerate((1, -1)):
+        for way in (1, -1):
             self.landing(way, False).wait_recv()
             self.hop(way, True).start()
+
+    def near_hand(self):
+        for i in range(2):
             self.hand(i).start()
 
     def far(self):
@@ -238,6 +241,8 @@
     def finish(self):
         for i in range(3):
             self.hand(i, True).wait_recv()
+
+    def drain(self):
         for way in (1, -1):
             for forward in (False, True):
                 self.hop(way, forward).wait_send()
@@ -251,7 +256,7 @@
 
 def layer_kernel(
     q_in, k_in, v_in, lg_in, gate_in, wo_in, stream_in, wg_in, wu_in, wd_in,
-    bias_ref, rows_ref, gain_ref, ff_gain_ref,
+    bias_ref, extra_ref, doc_ref, gains_ref,
     out_ref,
     q_ref, k_ref, v_ref, lg_ref, gate_ref, aux_ref, wg_ref, wu_ref, shard_ref, wd_ref,
     cum_ref, blk_ref, off_ref, states_ref, before_ref, run_ref, local_ref,
@@ -338,7 +343,8 @@
     def columns(g, _):
         at = pl.multiple_of(g * GR, GR)
         for j in range(3):
-            row = rows_ref[pl.ds(j * groups + g, 1), :]
+            lanes = pl.ds(pl.multiple_of(g * GR, GR), GR)
+            row = doc_ref[:, lanes].astype(F32) if j == 2 else extra_ref[j : j + 1, lanes]
             col = jnp.sum(jnp.where(ri == ci, row, 0.0), axis=1, keepdims=True)
             aux_ref[pl.ds(at, GR), j : j + 1] = col
         return 0
@@ -468,7 +474,7 @@
         at = pl.multiple_of(g * GR, GR)
         same_block = (ri & (GR - BL)) == (ci & (GR - BL))
         doc = aux_ref[pl.ds(at, GR), 2:3]
-        same = same_block & (doc == rows_ref[pl.ds(2 * groups + g, 1), :])
+        same = same_block & (doc == doc_ref[:, pl.ds(at, GR)].astype(F32))
         below = same & (ci <= ri)
         above = same & (ci >= ri)
         cum3 = cum_ref[pl.ds(at, GR), :].reshape(per, BL, 2 * DK)
@@ -508,12 +514,12 @@
 
     lax.fori_loop(0, groups // 2, inside, 0)
     g2.near()
+    g1.column(0)
     lax.fori_loop(groups // 2, groups, inside, 0)
-    g1.far()
-    ring.near()
 
     for s in sends:
         s.wait()
+    ring.near()
     run_ref[0] = jnp.zeros_like(run_ref[0])
 
     def earlier(j, _):
@@ -551,6 +557,8 @@
         send_c, part_c, core_send.at[2], core_recv.at[2],
         device_id=partner, device_id_type=MESH)
     swap_c.start()
+    ring.near_hand()
+    g2.column(0)
     enter_f = jnp.where(is0, before_doc, e0[2:3])[:, 0:1]
     enter_b = jnp.where(is0, e1[1:2], after_doc)[:, 0:1]
     swap_c.wait()
@@ -567,7 +575,7 @@
         qf = q_ref[pl.ds(at, GR), :].astype(F32) * scale
         q_fwd = (qf * jnp.exp(glob) * hit_f).astype(BF16)
         q_bwd = (qf * jnp.exp(sum_ref[...] - glob) * hit_b).astype(BF16)
-        gain = gain_ref[...].astype(F32)
+        gain = gains_ref[:, :DV]
         for h in range(2):
             c = slice(h * DK, (h + 1) * DK)
             both = jnp.concatenate([q_fwd[:, c], q_bwd[:, c]], axis=1)
@@ -575,7 +583,7 @@
             out = local_ref[pl.ds(at, GR), h * DV : (h + 1) * DV] + nt_dot(both, carry)
             out = out * lax.rsqrt(jnp.mean(out * out, axis=-1, keepdims=True) + EPS) * gain
             u = gate_ref[pl.ds(at, GR), h * DV : (h + 1) * DV].astype(F32)
-            hm[me, pl.ds(at, GR), h * DV : (h + 1) * DV] = (
+            hm[pl.ds(at, GR), pl.ds(pl.multiple_of(me * 2 * DV + h * DV, DV), DV)] = (
                 out * (u / (1.0 + jnp.exp(-u)))).astype(BF16)
 
     def three(i, _):
@@ -585,7 +593,9 @@
     lax.fori_loop(0, 3, three, 0)
 
     def piece(slot, r, part):
-        return hm.at[slot, pl.ds(pl.multiple_of(r * q_rows + part * half, half), half)]
+        return hm.at[
+            pl.ds(pl.multiple_of(r * q_rows + part * half, half), half),
+            pl.ds(pl.multiple_of(slot * 2 * DV, 2 * DV), 2 * DV)]
 
     def remote(ref, send, recv, target, dst=None):
         return pltpu.make_async_remote_copy(
@@ -594,8 +604,8 @@
     def wire(slot, quarter, part, send, recv, target):
         return remote(piece(slot, quarter, part), send, recv, target)
 
-    to_right = (((3, 0), (3, 1), (0, 0)), ((2, 0), (2, 1)), ((0, 1), (1, 0)), ((1, 1),))
-    to_left = (((1, 1), (1, 0), (0, 1)), ((0, 0), (3, 1)), ((2, 1), (2, 0)), ((3, 0),))
+    to_right = (((0, 0), (3, 0), (3, 1)), ((2, 0), (2, 1)), ((1, 0), (0, 1)), ((1, 1),))
+    to_left = (((0, 1), (1, 1), (1, 0)), ((3, 1), (0, 0)), ((2, 1), (2, 0)), ((3, 0),))
 
     def own_right(o, p):
         return wire(me, quarter_of(me, o), p, own_rs.at[o * 2 + p], left_in.at[o * 2 + p], right)
@@ -643,22 +653,26 @@
 
     send_own(0)
     last(quarter_of(me, 2))
-    g1.column(0)
-    pump(0)
-    send_own(1)
+    g1.far()
     for ja in (-1, 1):
         g1.column(ja)
     g2.far()
-    g2.column(0)
+    pump(0)
+    send_own(1)
     ring.far()
     g1.column(2)
+    for ja in (-1, 1):
+        g2.column(ja)
     ring.finish()
 
     dh = d // 2
     to_r_a = remote(s2.at[:, pl.ds(0, dh)], rs_send.at[0], rs_recv.at[0], right, ra)
     to_l_b = remote(s2.at[:, pl.ds(dh, dh)], rs_send.at[1], rs_recv.at[1], left, rb)
-    to_r = remote(s1, rs_send.at[2], rs_recv.at[2], right, rl)
-    to_l = remote(s3, rs_send.at[3], rs_recv.at[3], left, rr)
+    lo, up = pl.ds(0, dh), pl.ds(dh, dh)
+    to_r = remote(s1.at[:, up], rs_send.at[2], rs_recv.at[2], right, rl.at[:, up])
+    to_l = remote(s3.at[:, lo], rs_send.at[3], rs_recv.at[3], left, rr.at[:, lo])
+    to_r_sum = remote(s1.at[:, lo], rs_send.at[4], rs_recv.at[4], right, rl.at[:, lo])
+    to_l_sum = remote(s3.at[:, up], rs_send.at[5], rs_recv.at[5], left, rr.at[:, up])
 
     for i in range(n):
         q = quarter_of(me, order[i])
@@ -673,44 +687,52 @@
         load_stream(i).wait()
 
         def project(j, total):
-            cols = pl.ds(pl.multiple_of(j * 512, 512), 512)
-            acc = st[i % 2, :, cols].astype(F32)
-            for k in range(n):
-                acc = acc + nn_dot(hm[k, rows, :], wo_v[k * 512 : (k + 1) * 512, cols])
+            cols = pl.ds(pl.multiple_of(j * 1024, 1024), 1024)
+            acc = st[i % 2, :, cols].astype(F32) + nn_dot(hm[rows, :], wo_v[:, cols])
             resid[:, cols] = acc
             return total + jnp.sum(acc * acc, axis=-1, keepdims=True)
 
-        squares = lax.fori_loop(0, d // 512, project, jnp.zeros((q_rows, 1), F32))
-        if i < n - 1:
-            pump(i + 1)
+        squares = lax.fori_loop(0, d // 1024, project, jnp.zeros((q_rows, 1), F32))
+        if i == 0:
+            pump(1)
+            send_own(2)
+            send_own(3)
         if i < n - 2:
-            send_own(i + 2)
             load_stream(i + 2).start()
         if i == 0:
-            for ja in (-1, 1, 2):
-                g2.column(ja)
+            g2.column(2)
             for ja in PlaneGather.OFFS:
                 g1.column_far(ja)
             g1.finish()
         factor = lax.rsqrt(squares / d + EPS)
-        normed[...] = (resid[...] * factor * ff_gain_ref[...].astype(F32)).astype(BF16)
-
-        def gate_up(j, _):
-            both = nn_dot(normed[...], w_v[:, pl.ds(pl.multiple_of(j * 256, 256), 256)])
-            g, u = both[:, :128], both[:, 128:]
-            hidden[:, pl.ds(pl.multiple_of(j * 128, 128), 128)] = (
-                g / (1.0 + jnp.exp(-g)) * u).astype(BF16)
+        normed[...] = (resid[...] * factor * gains_ref[:, DV:]).astype(BF16)
+
+        def gate_up(at, width):
+            both = nn_dot(normed[...], w_v[:, pl.ds(pl.multiple_of(at * 2, 256), 2 * width)])
+            for b in range(width // 128):
+                g = both[:, b * 256 : b * 256 + 128]
+                u = both[:, b * 256 + 128 : (b + 1) * 256]
+                hidden[:, pl.ds(pl.multiple_of(at + b * 128, 128), 128)] = (
+                    g / (1.0 + jnp.exp(-g)) * u).astype(BF16)
+
+        def gate_up_pair(j, _):
+            gate_up(j * 256, 256)
             return 0
 
-        lax.fori_loop(0, units // 128, gate_up, 0)
+        lax.fori_loop(0, units // 256, gate_up_pair, 0)
+        gate_up(units // 256 * 256, units % 256)
         if i == 0:
             for ja in PlaneGather.OFFS:
                 g2.column_far(ja)
             g2.finish()
+        if i == 2:
+            to_r_a.wait_recv()
+            s1[:, :dh] = (s1[:, :dh].astype(F32) + ra[...].astype(F32)).astype(BF16)
+            to_r_sum.start()
         target = (s2, s1, s3, resid)[i]
 
         def down(j, _):
-            cols = pl.ds(pl.multiple_of(j * 256, 256), 256)
+            cols = pl.ds(pl.multiple_of(j * 512, 512), 512)
             part = nt_dot(hidden[...], down_v[cols, :]).astype(BF16)
             if i < n - 1:
                 target[:, cols] = part
@@ -718,20 +740,24 @@
                 target[:, cols] = target[:, cols] + part.astype(F32)
             return 0
 
-        lax.fori_loop(0, d // 256, down, 0)
+        lax.fori_loop(0, d // 512, down, 0)
         if i == 0:
+            pump(2)
+            pump(3)
             to_r_a.start()
             to_l_b.start()
+        if i == 1:
+            to_r.start()
         if i == 2:
-            to_r_a.wait_recv()
-            s1[:, :dh] = (s1[:, :dh].astype(F32) + ra[...].astype(F32)).astype(BF16)
-            to_r.start()
+            to_l.start()
             to_l_b.wait_recv()
             s3[:, dh:] = (s3[:, dh:].astype(F32) + rb[...].astype(F32)).astype(BF16)
-            to_l.start()
+            to_l_sum.start()
 
     to_r.wait_recv()
     to_l.wait_recv()
+    to_r_sum.wait_recv()
+    to_l_sum.wait_recv()
     out_ref[...] = (resid[...] + rl[...].astype(F32) + rr[...].astype(F32)).astype(BF16)
 
     for o in range(n):
@@ -743,17 +769,19 @@
         fwd_left(i).wait_send()
     g1.drain()
     g2.drain()
+    ring.drain()
     to_r_a.wait_send()
     to_l_b.wait_send()
     to_r.wait_send()
     to_l.wait_send()
+    to_r_sum.wait_send()
+    to_l_sum.wait_send()
 
 
 def layer(q, k, v, lg, bias, extra, doc, gate, gain, wo, stream, ff_gain, wg, wu, wd):
     rows, d = stream.shape
     units = wg.shape[1]
-    groups = rows // GR
-    table = jnp.concatenate([extra.T, doc.astype(F32)[None]], axis=0).reshape(3 * groups, GR)
+    gains = jnp.concatenate([gain, ff_gain]).astype(F32).reshape(1, -1)
     vm = pl.BlockSpec(memory_space=pltpu.VMEM)
     hbm = pl.BlockSpec(memory_space=pl.ANY)
     blocks = rows // BL
@@ -784,14 +812,14 @@
             buf(NCHIP, DV, DK), buf(NCHIP, 8, DK, dtype=F32),
             buf(DV, 2 * DK), buf(DV, 2 * DK), buf(DV, 2 * DK),
             buf(1, 2 * DK, dtype=F32),
-            buf(4, rows, 2 * DV), buf(2, GR, d), buf(4 * wo.shape[0], d),
+            buf(rows, 4 * 2 * DV), buf(2, GR, d), buf(4 * wo.shape[0], d),
             buf(2 * NCHIP * wg.shape[0], 2 * units), buf(2 * NCHIP * wd.shape[0], units),
             buf(GR, d, dtype=F32), buf(GR, d), buf(GR, units),
             buf(GR, d), buf(GR, d), buf(GR, d), buf(GR, d // 2), buf(GR, d // 2), buf(GR, d), buf(GR, d),
             dma((13,)), dma((3,)), dma((3,)),
             dma((NCHIP,)), dma((NCHIP,)), dma((NCHIP,)), dma((NCHIP,)),
             dma((8,)), dma((8,)), dma((4,)), dma((4,)),
-            dma((8,)), dma((8,)), dma((4,)), dma((4,)), dma((4,)), dma((4,)),
+            dma((8,)), dma((8,)), dma((4,)), dma((4,)), dma((6,)), dma((6,)),
         ] + plane_sems() + plane_sems() + [dma((k,)) for k in RowGather.SEMS],
         compiler_params=pltpu.CompilerParams(
             collective_id=0, has_side_effects=True, vmem_limit_bytes=67_043_328),
@@ -799,7 +827,7 @@
             flops=29_000_000_000, bytes_accessed=16_000_000, transcendentals=0),
         name="layer",
     )(q, k, v, lg, gate, wo, stream, wg, wu, wd,
-      bias.reshape(1, -1), table, gain.reshape(1, -1), ff_gain.reshape(1, -1))
+      bias.reshape(1, -1), extra.T, doc.reshape(1, -1), gains)
 
 
 def per_device(

time: 155 us -> 128 us (0.83)
  Pallas kernels: 146 us -> 123 us
  local copies, waits for them, and re-layouts: 5.45 us -> 3.66 us
    pallas_call x1, Pallas kernels: 146 us -> 123 us  [layer(): pl.pallas_call(layer_kernel, out_shape=jax.ShapeDtypeStruct((GR, d), BF16...]
    reshape x3 -> x0, local copies, waits for them, and re-layouts: 3.15 us -> none  [the longest x1 1.28 us: layer(): ff_gain.reshape(1, -1)]
where the time goes in v6:
time: 128 us; the launch traced here: 127 us
  Pallas kernels  123 us (96%)
  local copies, waits for them, and re-layouts  3.66 us (3%)
    pallas_call x1, Pallas kernels, layer(): pl.pallas_call(layer_kernel, out_shape=jax.ShapeDtypeStruct((GR, d), BF16...  123 us

profile of v6, /device:TPU:6, one launch (start us, length us, event | category | flops | bytes accessed | tf_op | source)
XLA Modules:
  0.0 127.2 jit_solution(642278979371319484)
XLA Ops:
  0.0 0.7 concatenate.14
  0.7 0.7 concatenate.15
  1.4 0.6 maximum_convert_fusion.gains_ref
  2.0 122.9 %layer.1 = bf16[256,2048]{1,0:T(8,128)(2,1)} custom-call(bf16[1024,256]{1,0:T(8,128)(2,1)} %q_in.1, bf16[1024,256]{1,0:T(8,128)(2,1)} %k_in.1, bf16[1024,512]{1,0:T(8,128)(2,1)} %v_in.1, bf16[1024,256]{1,0:T(8,128)(2,1)} %lg_in.1, bf16[1024,512]{1,0:T(8,128)(2,1)} %gate_in.1, bf16[512,2048]{1,0:T(8,128)(2,1)} %wo_in.1, bf16[1024,2048]{1,0:T(8,128)(2,1)} %stream_in.1, ...), custom_call_target="tpu_custom_call" | custom-call | flops 28999999488 | bytes 16000000 | tf_op jit(solution)/shard_map/layer/pallas_call | solution.py:793
  124.9 2.3 %copy.17 = bf16[256,2048]{1,0:T(8,128)(2,1)} copy(bf16[256,2048]{1,0:T(8,128)(2,1)} %layer.1) | data formatting | bytes 2097152

commit v7 on v6

--- a/solution.py
+++ b/solution.py
@@ -138,7 +138,10 @@
             for hf in range(2):
                 self.landing(hf, 0, 0, way, False).wait_recv()
                 self.hop(hf, 0, 0, way, True).start()
-                self.second(hf, -way)
+
+    def near_second(self, hf):
+        for way in (1, -1):
+            self.second(hf, -way)
 
     def far(self):
         for hf in range(2):
@@ -179,7 +182,7 @@
 
 
 class RowGather:
-    SEMS = (4, 4, 3, 3)
+    SEMS = (6, 6, 3, 3)
 
     def __init__(self, rows, dst, sems):
         self.dst = dst
@@ -199,20 +202,27 @@
     def side(self, way):
         return (self.z, self.y, self.core, lax.rem(self.x + (way + 4), 4))
 
-    def hop(self, way, forward):
-        k = (0 if way > 0 else 1) + (2 if forward else 0)
-        if forward:
-            dst = self.piece(-way, self.core, 0 if way > 0 else 1)
-            src = dst
+    def copy(self, ref, k, way):
+        return remote_copy(ref, ref, self.send.at[k], self.recv.at[k], self.side(way))
+
+    def key(self, way, part):
+        return (0 if way > 0 else 1) + 2 * part
+
+    def hop(self, way, part):
+        first = 0 if way > 0 else 1
+        if part == 2:
+            ref = self.piece(-way, self.core, first)
         else:
-            dst = self.piece(0, self.core)
-            src = dst
-        return remote_copy(src, dst, self.send.at[k], self.recv.at[k], self.side(way))
-
-    def landing(self, way, forward):
-        k = (0 if way > 0 else 1) + (2 if forward else 0)
-        ref = self.piece(2, self.core, 0 if way > 0 else 1) if forward else self.piece(-way, self.core)
-        return remote_copy(ref, ref, self.send.at[k], self.recv.at[k], self.side(way))
+            ref = self.piece(0, self.core, first if part == 0 else 1 - first)
+        return self.copy(ref, self.key(way, part), way)
+
+    def landing(self, way, part):
+        first = 0 if way > 0 else 1
+        if part == 2:
+            ref = self.piece(2, self.core, first)
+        else:
+            ref = self.piece(-way, self.core, first if part == 0 else 1 - first)
+        return self.copy(ref, self.key(way, part), way)
 
     def hand(self, i, arriving=False):
         k = (-1, 1, 2)[i]
@@ -221,21 +231,23 @@
             ref, ref, self.core_send.at[i], self.core_recv.at[i], (self.z, self.y, 1 - self.core, self.x))
 
     def start(self):
-        for way in (1, -1):
-            self.hop(way, False).start()
+        for part in range(2):
+            for way in (1, -1):
+                self.hop(way, part).start()
 
     def near(self):
         for way in (1, -1):
-            self.landing(way, False).wait_recv()
-            self.hop(way, True).start()
+            self.landing(way, 0).wait_recv()
+            self.hop(way, 2).start()
 
     def near_hand(self):
-        for i in range(2):
+        for i, way in enumerate((1, -1)):
+            self.landing(way, 1).wait_recv()
             self.hand(i).start()
 
     def far(self):
         for way in (1, -1):
-            self.landing(way, True).wait_recv()
+            self.landing(way, 2).wait_recv()
         self.hand(2).start()
 
     def finish(self):
@@ -244,8 +256,8 @@
 
     def drain(self):
         for way in (1, -1):
-            for forward in (False, True):
-                self.hop(way, forward).wait_send()
+            for part in range(3):
+                self.hop(way, part).wait_send()
         for i in range(3):
             self.hand(i).wait_send()
 
@@ -260,7 +272,7 @@
     out_ref,
     q_ref, k_ref, v_ref, lg_ref, gate_ref, aux_ref, wg_ref, wu_ref, shard_ref, wd_ref,
     cum_ref, blk_ref, off_ref, states_ref, before_ref, run_ref, local_ref,
-    own_t, own_e, part_t, part_e, chip_t, chip_e, recv_t, recv_e, mine_c, send_c, part_c, sum_ref,
+    own_t, own_e, part_t, part_e, chip_t, chip_e, ry_t, ry_e, row_t, row_e, rz_t, rz_e, mine_c, send_c, part_c, sum_ref,
     hm, st, wo_v, w_v, down_v, resid, normed, hidden, s2, s1, s3, ra, rb, rl, rr,
     local_sem, core_send, core_recv, t_send, t_recv, e_send, e_recv,
     own_rs, own_ls, fwd_rs, fwd_ls, left_in, right_in, opp_l, opp_r, rs_send, rs_recv,
@@ -272,7 +284,6 @@
     per = GR // BL
     z, y = lax.axis_index("sp_0"), lax.axis_index("sp_1")
     core, me = lax.axis_index("sp_2"), lax.axis_index("tp")
-    chip = z * NY + y
     scale = DK ** (-0.5)
     n = 4
     q_rows = GR
@@ -287,9 +298,11 @@
     def quarter_of(owner, offset):
         return lax.rem(owner + offset, n)
 
-    def chip_peer(k):
-        other = lax.rem(chip + k, NCHIP)
-        return other, (other // NY, lax.rem(other, NY), core, me)
+    def along_y(k):
+        return (z, lax.rem(y + k, NY), core, me)
+
+    def along_z(k):
+        return (lax.rem(z + k, NZ), y, core, me)
 
     wo_own = wo_in.shape[0]
     loads = {
@@ -312,14 +325,15 @@
     load_stream(0).start()
     load_stream(1).start()
 
-    recv_t[pl.ds(chip, 1)] = jnp.zeros((1, DV, DK), BF16)
+    rz_t[pl.ds(z, 1)] = jnp.zeros((1, DV, DK), BF16)
 
     barrier = pltpu.get_barrier_semaphore()
     pl.semaphore_signal(barrier, inc=1, device_id=partner, device_id_type=MESH)
     pl.semaphore_signal(barrier, inc=1, device_id=right, device_id_type=MESH)
     pl.semaphore_signal(barrier, inc=1, device_id=left, device_id_type=MESH)
-    for k in range(1, NCHIP):
-        pl.semaphore_signal(barrier, inc=1, device_id=chip_peer(k)[1], device_id_type=MESH)
+    for k in range(1, NY):
+        pl.semaphore_signal(barrier, inc=1, device_id=along_y(k), device_id_type=MESH)
+        pl.semaphore_signal(barrier, inc=1, device_id=along_z(k), device_id_type=MESH)
 
     loads["wg"].wait()
     loads["wu"].wait()
@@ -329,13 +343,12 @@
     loads["wd"].wait()
     loads["wo"].wait()
 
-    pl.semaphore_wait(barrier, NCHIP + 2)
+    pl.semaphore_wait(barrier, 9)
     g1 = PlaneGather(shard_ref, w_v, gather_sems[:5])
     g2 = PlaneGather(wd_ref, down_v, gather_sems[5:10])
     ring = RowGather(wo_own, wo_v, gather_sems[10:])
     ring.start()
     g1.start()
-    g2.start()
 
     ri = lax.broadcasted_iota(jnp.int32, (GR, GR), 0)
     ci = lax.broadcasted_iota(jnp.int32, (GR, GR), 1)
@@ -427,6 +440,7 @@
         own_e[h, 2:3] = last_doc
         own_e[h, 3:8] = jnp.zeros((5, DK), F32)
 
+    g1.near()
     swap_t = pltpu.make_async_remote_copy(
         own_t.at[1 - core], part_t, core_send.at[0], core_recv.at[0],
         device_id=partner, device_id_type=MESH)
@@ -453,21 +467,17 @@
     chip_row = jnp.concatenate(
         [e0[0:1] + e1[0:1], e0[1:2], e1[2:3], jnp.zeros((5, DK), F32)], axis=0)
     chip_e[...] = chip_row
-    recv_e[pl.ds(chip, 1)] = chip_row[None]
-
-    sends = []
-    for k in range(1, NCHIP):
-        other, target = chip_peer(k)
-        back = jnp.where(other > chip, 0, 1)
-        sends.append(pltpu.make_async_remote_copy(
-            chip_e, recv_e.at[chip], e_send.at[k], e_recv.at[k],
-            device_id=target, device_id_type=MESH))
-        sends.append(pltpu.make_async_remote_copy(
-            chip_t.at[back], recv_t.at[chip], t_send.at[k], t_recv.at[k],
-            device_id=target, device_id_type=MESH))
-    for s in sends:
+    ry_e[pl.ds(y, 1)] = chip_row[None]
+    ry_t[pl.ds(y, 1)] = chip_t[...][None]
+
+    y_sends = []
+    for k in range(1, NY):
+        y_sends.append(remote_copy(chip_e, ry_e.at[y], e_send.at[k], e_recv.at[k], along_y(k)))
+        y_sends.append(remote_copy(chip_t, ry_t.at[y], t_send.at[k], t_recv.at[k], along_y(k)))
+    for s in y_sends:
         s.start()
-    g1.near()
+    g1.near_second(0)
+    g2.start()
     loads["q"].wait()
 
     def inside(g, _):
@@ -513,36 +523,89 @@
         return 0
 
     lax.fori_loop(0, groups // 2, inside, 0)
-    g2.near()
     g1.column(0)
     lax.fori_loop(groups // 2, groups, inside, 0)
 
-    for s in sends:
+    ring.near()
+    for s in y_sends:
         s.wait()
-    ring.near()
     run_ref[0] = jnp.zeros_like(run_ref[0])
 
-    def earlier(j, _):
-        e = recv_e[j]
-        p = recv_e[jnp.maximum(j - 1, 0)]
-        keep = jnp.exp(e[0:1]) * jnp.where(e[2:3] == p[2:3], 1.0, 0.0)
-        run_ref[0, :, :DK] = recv_t[j].astype(F32) + run_ref[0, :, :DK] * keep
-        return 0
-
-    def later(i, _):
-        j = NCHIP - 1 - i
-        e = recv_e[j]
-        p = recv_e[jnp.minimum(j + 1, NCHIP - 1)]
-        keep = jnp.exp(e[0:1]) * jnp.where(e[1:2] == p[1:2], 1.0, 0.0)
-        run_ref[0, :, DK:] = recv_t[j].astype(F32) + run_ref[0, :, DK:] * keep
-        return 0
-
-    lax.fori_loop(0, chip, earlier, 0)
-    lax.fori_loop(0, NCHIP - 1 - chip, later, 0)
-    cf, cb = run_ref[0, :, :DK], run_ref[0, :, DK:]
-    before_doc = jnp.where(chip > 0, recv_e[jnp.maximum(chip - 1, 0)][2:3], -1.0)
-    after_doc = jnp.where(
-        chip < NCHIP - 1, recv_e[jnp.minimum(chip + 1, NCHIP - 1)][1:2], -1.0)
+    def earlier(states, table):
+        def body(j, _):
+            e = table[j]
+            p = table[jnp.maximum(j - 1, 0)]
+            keep = jnp.exp(e[0:1]) * jnp.where(e[2:3] == p[2:3], 1.0, 0.0)
+            run_ref[0, :, :DK] = states(j, 0).astype(F32) + run_ref[0, :, :DK] * keep
+            return 0
+        return body
+
+    def later(states, table):
+        def body(i, _):
+            j = NY - 1 - i
+            e = table[j]
+            p = table[jnp.minimum(j + 1, NY - 1)]
+            keep = jnp.exp(e[0:1]) * jnp.where(e[1:2] == p[1:2], 1.0, 0.0)
+            run_ref[0, :, DK:] = states(j, 1).astype(F32) + run_ref[0, :, DK:] * keep
+            return 0
+        return body
+
+    def row_state(j, way):
+        return ry_t[j, way]
+
+    def column_state(j, way):
+        return rz_t[j]
+
+    lax.fori_loop(0, y, earlier(row_state, ry_e), 0)
+    lax.fori_loop(0, NY - 1 - y, later(row_state, ry_e), 0)
+    run_ref[1] = run_ref[0]
+    lax.fori_loop(y, NY, earlier(row_state, ry_e), 0)
+    lax.fori_loop(NY - 1 - y, NY, later(row_state, ry_e), 0)
+    row_t[0] = run_ref[0, :, :DK].astype(BF16)
+    row_t[1] = run_ref[0, :, DK:].astype(BF16)
+    in_row = [ry_e[j] for j in range(NY)]
+    row_sum = in_row[0][0:1] + in_row[1][0:1] + in_row[2][0:1] + in_row[3][0:1]
+    sum_before = jnp.zeros((1, DK), F32)
+    sum_after = jnp.zeros((1, DK), F32)
+    for j in range(NY):
+        sum_before = sum_before + jnp.where(j < y, in_row[j][0:1], 0.0)
+        sum_after = sum_after + jnp.where(j > y, in_row[j][0:1], 0.0)
+    last_before = ry_e[jnp.maximum(y - 1, 0)][2:3]
+    first_after = ry_e[jnp.minimum(y + 1, NY - 1)][1:2]
+    row_row = jnp.concatenate(
+        [row_sum, in_row[0][1:2], in_row[NY - 1][2:3], jnp.zeros((5, DK), F32)], axis=0)
+    row_e[...] = row_row
+    rz_e[pl.ds(z, 1)] = row_row[None]
+    z_sends = []
+    for k in range(1, NZ):
+        back = jnp.where(lax.rem(z + k, NZ) > z, 0, 1)
+        z_sends.append(
+            remote_copy(row_e, rz_e.at[z], e_send.at[4 + k], e_recv.at[4 + k], along_z(k)))
+        z_sends.append(
+            remote_copy(row_t.at[back], rz_t.at[z], t_send.at[4 + k], t_recv.at[4 + k], along_z(k)))
+    for s in z_sends:
+        s.start()
+    g1.near_second(1)
+    g1.far()
+    for s in z_sends:
+        s.wait()
+    g2.near()
+    g2.near_second(0)
+    g2.near_second(1)
+
+    run_ref[0] = jnp.zeros_like(run_ref[0])
+    lax.fori_loop(0, z, earlier(column_state, rz_e), 0)
+    lax.fori_loop(0, NZ - 1 - z, later(column_state, rz_e), 0)
+    prev_last = jnp.where(z > 0, rz_e[jnp.maximum(z - 1, 0)][2:3], -1.0)
+    next_first = jnp.where(z < NZ - 1, rz_e[jnp.minimum(z + 1, NZ - 1)][1:2], -1.0)
+    pass_f = jnp.exp(sum_before) * jnp.where(
+        y == 0, 1.0, jnp.where(prev_last == last_before, 1.0, 0.0))
+    pass_b = jnp.exp(sum_after) * jnp.where(
+        y == NY - 1, 1.0, jnp.where(next_first == first_after, 1.0, 0.0))
+    cf = run_ref[1, :, :DK] + pass_f * run_ref[0, :, :DK]
+    cb = run_ref[1, :, DK:] + pass_b * run_ref[0, :, DK:]
+    before_doc = jnp.where(y > 0, last_before, prev_last)
+    after_doc = jnp.where(y < NY - 1, first_after, next_first)
     pass0 = jnp.exp(e0[0:1]) * jnp.where(before_doc == e0[2:3], 1.0, 0.0)
     pass1 = jnp.exp(e1[0:1]) * jnp.where(after_doc == e1[1:2], 1.0, 0.0)
     mine_t = own_t[pl.ds(core, 1)][0].astype(F32)
@@ -558,7 +621,6 @@
         device_id=partner, device_id_type=MESH)
     swap_c.start()
     ring.near_hand()
-    g2.column(0)
     enter_f = jnp.where(is0, before_doc, e0[2:3])[:, 0:1]
     enter_b = jnp.where(is0, e1[1:2], after_doc)[:, 0:1]
     swap_c.wait()
@@ -653,14 +715,15 @@
 
     send_own(0)
     last(quarter_of(me, 2))
-    g1.far()
     for ja in (-1, 1):
         g1.column(ja)
-    g2.far()
+    g2.column(0)
+    ring.far()
     pump(0)
     send_own(1)
-    ring.far()
     g1.column(2)
+    g2.far()
+    send_own(2)
     for ja in (-1, 1):
         g2.column(ja)
     ring.finish()
@@ -674,16 +737,14 @@
     to_r_sum = remote(s1.at[:, lo], rs_send.at[4], rs_recv.at[4], right, rl.at[:, lo])
     to_l_sum = remote(s3.at[:, up], rs_send.at[5], rs_recv.at[5], left, rr.at[:, up])
 
-    for i in range(n):
-        q = quarter_of(me, order[i])
-        at = pl.multiple_of(q * q_rows, q_rows)
+    def prepare(i):
+        at = pl.multiple_of(quarter_of(me, order[i]) * q_rows, q_rows)
         rows = pl.ds(at, q_rows)
         for p in range(2):
             arrived("l", (1 + order[i]) % n, p)
             arrived("r", (n - 1 + order[i]) % n, p)
         came_opp_l(i).wait_recv()
         came_opp_r(i).wait_recv()
-
         load_stream(i).wait()
 
         def project(j, total):
@@ -693,19 +754,22 @@
             return total + jnp.sum(acc * acc, axis=-1, keepdims=True)
 
         squares = lax.fori_loop(0, d // 1024, project, jnp.zeros((q_rows, 1), F32))
-        if i == 0:
-            pump(1)
-            send_own(2)
-            send_own(3)
         if i < n - 2:
             load_stream(i + 2).start()
+        factor = lax.rsqrt(squares / d + EPS)
+        normed[...] = (resid[...] * factor * gains_ref[:, DV:]).astype(BF16)
+
+    prepare(0)
+    pump(1)
+    send_own(3)
+    g2.column(2)
+    for i in range(n):
         if i == 0:
-            g2.column(2)
             for ja in PlaneGather.OFFS:
                 g1.column_far(ja)
             g1.finish()
-        factor = lax.rsqrt(squares / d + EPS)
-        normed[...] = (resid[...] * factor * gains_ref[:, DV:]).astype(BF16)
+        else:
+            prepare(i)
 
         def gate_up(at, width):
             both = nn_dot(normed[...], w_v[:, pl.ds(pl.multiple_of(at * 2, 256), 2 * width)])
@@ -809,7 +873,9 @@
             buf(2, 2 * DV, DK), buf(2, 8, DK, dtype=F32),
             buf(2 * DV, DK), buf(8, DK, dtype=F32),
             buf(2, DV, DK), buf(8, DK, dtype=F32),
-            buf(NCHIP, DV, DK), buf(NCHIP, 8, DK, dtype=F32),
+            buf(NY, 2, DV, DK), buf(NY, 8, DK, dtype=F32),
+            buf(2, DV, DK), buf(8, DK, dtype=F32),
+            buf(NZ, DV, DK), buf(NZ, 8, DK, dtype=F32),
             buf(DV, 2 * DK), buf(DV, 2 * DK), buf(DV, 2 * DK),
             buf(1, 2 * DK, dtype=F32),
             buf(rows, 4 * 2 * DV), buf(2, GR, d), buf(4 * wo.shape[0], d),
@@ -817,7 +883,7 @@
             buf(GR, d, dtype=F32), buf(GR, d), buf(GR, units),
             buf(GR, d), buf(GR, d), buf(GR, d), buf(GR, d // 2), buf(GR, d // 2), buf(GR, d), buf(GR, d),
             dma((13,)), dma((3,)), dma((3,)),
-            dma((NCHIP,)), dma((NCHIP,)), dma((NCHIP,)), dma((NCHIP,)),
+            dma((8,)), dma((8,)), dma((8,)), dma((8,)),
             dma((8,)), dma((8,)), dma((4,)), dma((4,)),
             dma((8,)), dma((8,)), dma((4,)), dma((4,)), dma((6,)), dma((6,)),
         ] + plane_sems() + plane_sems() + [dma((k,)) for k in RowGather.SEMS],

time: 128 us -> 123 us (0.961)
  Pallas kernels: 123 us -> 118 us
    pallas_call x1, Pallas kernels: 123 us -> 118 us  [layer(): pl.pallas_call(layer_kernel, out_shape=jax.ShapeDtypeStruct((GR, d), BF16...]
where the time goes in v7:
time: 123 us
  Pallas kernels  118 us (96%)
  local copies, waits for them, and re-layouts  3.66 us (3%)
    pallas_call x1, Pallas kernels, layer(): pl.pallas_call(layer_kernel, out_shape=jax.ShapeDtypeStruct((GR, d), BF16...  118 us

profile of v7, /device:TPU:6, one launch (start us, length us, event | category | flops | bytes accessed | tf_op | source)
XLA Modules:
  0.0 122.7 jit_solution(8993064873150503024)
XLA Ops:
  0.0 0.7 concatenate.14
  0.7 0.7 concatenate.15
  1.4 0.6 maximum_convert_fusion.gains_ref
  2.0 118.4 %layer.1 = bf16[256,2048]{1,0:T(8,128)(2,1)} custom-call(bf16[1024,256]{1,0:T(8,128)(2,1)} %q_in.1, bf16[1024,256]{1,0:T(8,128)(2,1)} %k_in.1, bf16[1024,512]{1,0:T(8,128)(2,1)} %v_in.1, bf16[1024,256]{1,0:T(8,128)(2,1)} %lg_in.1, bf16[1024,512]{1,0:T(8,128)(2,1)} %gate_in.1, bf16[512,2048]{1,0:T(8,128)(2,1)} %wo_in.1, bf16[1024,2048]{1,0:T(8,128)(2,1)} %stream_in.1, ...), custom_call_target="tpu_custom_call" | custom-call | flops 28999999488 | bytes 16000000 | tf_op jit(solution)/shard_map/layer/pallas_call | solution.py:857
  120.4 2.3 %copy.17 = bf16[256,2048]{1,0:T(8,128)(2,1)} copy(bf16[256,2048]{1,0:T(8,128)(2,1)} %layer.1) | data formatting | bytes 2097152

commit v8 on v7

--- a/solution.py
+++ b/solution.py
@@ -268,7 +268,7 @@
 
 def layer_kernel(
     q_in, k_in, v_in, lg_in, gate_in, wo_in, stream_in, wg_in, wu_in, wd_in,
-    bias_ref, extra_ref, doc_ref, gains_ref,
+    bias_ref, extra_ref, doc_ref, gain_ref, ff_gain_ref,
     out_ref,
     q_ref, k_ref, v_ref, lg_ref, gate_ref, aux_ref, wg_ref, wu_ref, shard_ref, wd_ref,
     cum_ref, blk_ref, off_ref, states_ref, before_ref, run_ref, local_ref,
@@ -637,7 +637,7 @@
         qf = q_ref[pl.ds(at, GR), :].astype(F32) * scale
         q_fwd = (qf * jnp.exp(glob) * hit_f).astype(BF16)
         q_bwd = (qf * jnp.exp(sum_ref[...] - glob) * hit_b).astype(BF16)
-        gain = gains_ref[:, :DV]
+        gain = gain_ref[...].astype(F32).reshape(1, DV)
         for h in range(2):
             c = slice(h * DK, (h + 1) * DK)
             both = jnp.concatenate([q_fwd[:, c], q_bwd[:, c]], axis=1)
@@ -724,6 +724,8 @@
     g1.column(2)
     g2.far()
     send_own(2)
+    for ja in (0, -1, 1):
+        g1.column_far(ja)
     for ja in (-1, 1):
         g2.column(ja)
     ring.finish()
@@ -757,16 +759,17 @@
         if i < n - 2:
             load_stream(i + 2).start()
         factor = lax.rsqrt(squares / d + EPS)
-        normed[...] = (resid[...] * factor * gains_ref[:, DV:]).astype(BF16)
+        normed[...] = (resid[...] * factor * ff_gain_ref[...].astype(F32).reshape(1, d)).astype(BF16)
 
     prepare(0)
     pump(1)
     send_own(3)
     g2.column(2)
+    g1.column_far(2)
+    for ja in (0, -1, 1):
+        g2.column_far(ja)
     for i in range(n):
         if i == 0:
-            for ja in PlaneGather.OFFS:
-                g1.column_far(ja)
             g1.finish()
         else:
             prepare(i)
@@ -786,8 +789,9 @@
         lax.fori_loop(0, units // 256, gate_up_pair, 0)
         gate_up(units // 256 * 256, units % 256)
         if i == 0:
-            for ja in PlaneGather.OFFS:
-                g2.column_far(ja)
+            g2.column_far(2)
+            pump(2)
+            pump(3)
             g2.finish()
         if i == 2:
             to_r_a.wait_recv()
@@ -804,16 +808,20 @@
                 target[:, cols] = target[:, cols] + part.astype(F32)
             return 0
 
-        lax.fori_loop(0, d // 512, down, 0)
+        tiles = d // 1024
+        first_half, second_half = ((tiles, 2 * tiles), (0, tiles)) if i == 1 else (
+            (0, tiles), (tiles, 2 * tiles))
+        lax.fori_loop(*first_half, down, 0)
         if i == 0:
-            pump(2)
-            pump(3)
             to_r_a.start()
-            to_l_b.start()
         if i == 1:
             to_r.start()
         if i == 2:
             to_l.start()
+        lax.fori_loop(*second_half, down, 0)
+        if i == 0:
+            to_l_b.start()
+        if i == 2:
             to_l_b.wait_recv()
             s3[:, dh:] = (s3[:, dh:].astype(F32) + rb[...].astype(F32)).astype(BF16)
             to_l_sum.start()
@@ -845,7 +853,6 @@
 def layer(q, k, v, lg, bias, extra, doc, gate, gain, wo, stream, ff_gain, wg, wu, wd):
     rows, d = stream.shape
     units = wg.shape[1]
-    gains = jnp.concatenate([gain, ff_gain]).astype(F32).reshape(1, -1)
     vm = pl.BlockSpec(memory_space=pltpu.VMEM)
     hbm = pl.BlockSpec(memory_space=pl.ANY)
     blocks = rows // BL
@@ -857,7 +864,7 @@
     return pl.pallas_call(
         layer_kernel,
         out_shape=jax.ShapeDtypeStruct((GR, d), BF16),
-        in_specs=[hbm] * 10 + [vm] * 4,
+        in_specs=[hbm] * 10 + [vm] * 5,
         out_specs=vm,
         scratch_shapes=[
             buf(rows, 2 * DK), buf(rows, 2 * DK), buf(rows, 2 * DV), buf(rows, 2 * DK),
@@ -893,7 +900,7 @@
             flops=29_000_000_000, bytes_accessed=16_000_000, transcendentals=0),
         name="layer",
     )(q, k, v, lg, gate, wo, stream, wg, wu, wd,
-      bias.reshape(1, -1), extra.T, doc.reshape(1, -1), gains)
+      bias.reshape(1, -1), extra.T, doc.reshape(1, -1), gain, ff_gain)
 
 
 def per_device(

time: 123 us -> 120 us (0.976)
  local copies, waits for them, and re-layouts: 3.66 us -> 2.3 us
    concatenate x2 -> x0, local copies, waits for them, and re-layouts: 1.35 us -> none  [layer(): gains = jnp.concatenate([gain, ff_gain]).astype(F32).reshape(1, -1)]
where the time goes in v8:
time: 120 us
  Pallas kernels  118 us (98%)
  local copies, waits for them, and re-layouts  2.3 us (2%)
    pallas_call x1, Pallas kernels, layer(): pl.pallas_call(layer_kernel, out_shape=jax.ShapeDtypeStruct((GR, d), BF16...  118 us

profile of v8, /device:TPU:6, one launch (start us, length us, event | category | flops | bytes accessed | tf_op | source)
XLA Modules:
  0.0 120.1 jit_solution(5148681494453958487)
XLA Ops:
  0.0 117.7 %layer.1 = bf16[256,2048]{1,0:T(8,128)(2,1)} custom-call(bf16[1024,256]{1,0:T(8,128)(2,1)} %q_in.1, bf16[1024,256]{1,0:T(8,128)(2,1)} %k_in.1, bf16[1024,512]{1,0:T(8,128)(2,1)} %v_in.1, bf16[1024,256]{1,0:T(8,128)(2,1)} %lg_in.1, bf16[1024,512]{1,0:T(8,128)(2,1)} %gate_in.1, bf16[512,2048]{1,0:T(8,128)(2,1)} %wo_in.1, bf16[1024,2048]{1,0:T(8,128)(2,1)} %stream_in.1, ...), custom_call_target="tpu_custom_call" | custom-call | flops 28999999488 | bytes 16000000 | tf_op jit(solution)/shard_map/layer/pallas_call | solution.py:864
  117.7 2.3 %copy.17 = bf16[256,2048]{1,0:T(8,128)(2,1)} copy(bf16[256,2048]{1,0:T(8,128)(2,1)} %layer.1) | data formatting | bytes 2097152

commit v9 on v8

--- a/solution.py
+++ b/solution.py
@@ -793,10 +793,6 @@
             pump(2)
             pump(3)
             g2.finish()
-        if i == 2:
-            to_r_a.wait_recv()
-            s1[:, :dh] = (s1[:, :dh].astype(F32) + ra[...].astype(F32)).astype(BF16)
-            to_r_sum.start()
         target = (s2, s1, s3, resid)[i]
 
         def down(j, _):
@@ -818,6 +814,9 @@
             to_r.start()
         if i == 2:
             to_l.start()
+            to_r_a.wait_recv()
+            s1[:, :dh] = (s1[:, :dh].astype(F32) + ra[...].astype(F32)).astype(BF16)
+            to_r_sum.start()
         lax.fori_loop(*second_half, down, 0)
         if i == 0:
             to_l_b.start()

time: 120 us -> 119 us (level); the launches traced: 120 us -> 117 us
  Pallas kernels: 118 us -> 115 us
    pallas_call x1, Pallas kernels: 118 us -> 115 us  [layer(): pl.pallas_call(layer_kernel, out_shape=jax.ShapeDtypeStruct((GR, d), BF16...]
where the time goes in v9:
time: 119 us; the launch traced here: 117 us
  Pallas kernels  115 us (97%)
  local copies, waits for them, and re-layouts  2.3 us (2%)
    pallas_call x1, Pallas kernels, layer(): pl.pallas_call(layer_kernel, out_shape=jax.ShapeDtypeStruct((GR, d), BF16...  115 us

profile of v9, /device:TPU:6, one launch (start us, length us, event | category | flops | bytes accessed | tf_op | source)
XLA Modules:
  0.0 116.9 jit_solution(15238225930965599015)
XLA Ops:
  0.0 114.6 %layer.1 = bf16[256,2048]{1,0:T(8,128)(2,1)} custom-call(bf16[1024,256]{1,0:T(8,128)(2,1)} %q_in.1, bf16[1024,256]{1,0:T(8,128)(2,1)} %k_in.1, bf16[1024,512]{1,0:T(8,128)(2,1)} %v_in.1, bf16[1024,256]{1,0:T(8,128)(2,1)} %lg_in.1, bf16[1024,512]{1,0:T(8,128)(2,1)} %gate_in.1, bf16[512,2048]{1,0:T(8,128)(2,1)} %wo_in.1, bf16[1024,2048]{1,0:T(8,128)(2,1)} %stream_in.1, ...), custom_call_target="tpu_custom_call" | custom-call | flops 28999999488 | bytes 16000000 | tf_op jit(solution)/shard_map/layer/pallas_call | solution.py:863
  114.6 2.3 %copy.17 = bf16[256,2048]{1,0:T(8,128)(2,1)} copy(bf16[256,2048]{1,0:T(8,128)(2,1)} %layer.1) | data formatting | bytes 2097152

commit v10 on v9

--- a/solution.py
+++ b/solution.py
@@ -440,7 +440,6 @@
         own_e[h, 2:3] = last_doc
         own_e[h, 3:8] = jnp.zeros((5, DK), F32)
 
-    g1.near()
     swap_t = pltpu.make_async_remote_copy(
         own_t.at[1 - core], part_t, core_send.at[0], core_recv.at[0],
         device_id=partner, device_id_type=MESH)
@@ -449,6 +448,7 @@
         device_id=partner, device_id_type=MESH)
     swap_t.start()
     swap_e.start()
+    g1.near()
     swap_t.wait()
     swap_e.wait()
     is0 = core == 0

time: 119 us -> 119 us (level)
  no operation moved by 1% of the time
where the time goes in v10:
time: 119 us; the launch traced here: 117 us
  Pallas kernels  115 us (97%)
  local copies, waits for them, and re-layouts  2.3 us (2%)
    pallas_call x1, Pallas kernels, layer(): pl.pallas_call(layer_kernel, out_shape=jax.ShapeDtypeStruct((GR, d), BF16...  115 us

profile of v10, /device:TPU:6, one launch (start us, length us, event | category | flops | bytes accessed | tf_op | source)
XLA Modules:
  0.0 117.1 jit_solution(13242020883466275521)
XLA Ops:
  0.0 114.8 %layer.1 = bf16[256,2048]{1,0:T(8,128)(2,1)} custom-call(bf16[1024,256]{1,0:T(8,128)(2,1)} %q_in.1, bf16[1024,256]{1,0:T(8,128)(2,1)} %k_in.1, bf16[1024,512]{1,0:T(8,128)(2,1)} %v_in.1, bf16[1024,256]{1,0:T(8,128)(2,1)} %lg_in.1, bf16[1024,512]{1,0:T(8,128)(2,1)} %gate_in.1, bf16[512,2048]{1,0:T(8,128)(2,1)} %wo_in.1, bf16[1024,2048]{1,0:T(8,128)(2,1)} %stream_in.1, ...), custom_call_target="tpu_custom_call" | custom-call | flops 28999999488 | bytes 16000000 | tf_op jit(solution)/shard_map/layer/pallas_call | solution.py:863
  114.8 2.3 %copy.17 = bf16[256,2048]{1,0:T(8,128)(2,1)} copy(bf16[256,2048]{1,0:T(8,128)(2,1)} %layer.1) | data formatting | bytes 2097152
